TPU v7x, 32 devices: a whole 2x2x4 slice. The times are simulated.
32 devices in a mesh: fs: 16 (over z, y, x), tp: 2 (over core).
Axes of the slice: x: 2, y: 2, z: 4, core: 2. Of those that a mesh axis runs over, the one named last changes fastest.
Arguments:
- tokens: bfloat16 [2048, 2048], P('fs', 'tp'), may hold values from -300 to 300
- norm_gain: float32 [2048], P('fs'), may hold values from 0.1 to 1.9
- gate_weight: float32 [16, 2048, 1024], P(None, 'fs', 'tp'), may hold values from -1.3258252 to 1.3258252
- up_weight: float32 [16, 2048, 1024], P(None, 'fs', 'tp'), may hold values from -1.3258252 to 1.3258252
- down_weight: float32 [16, 1024, 2048], P(None, 'fs', 'tp'), may hold values from -0.1875 to 0.1875
- routes: int32 [2048, 4], P('fs'), may hold values from 0 to 15, all different within a row; in each aligned block of 128 rows (0 to 127, 128 to 255, ...) at most 64 rows name the same one
- route_weights: float32 [2048, 4], P('fs'), may hold values from 0.05 to 1
Outputs:
- mixed: bfloat16 [2048, 2048], P('fs', 'tp')
- gate_ready: bfloat16 [16, 2048, 1024], P('fs', None, 'tp')
- up_ready: bfloat16 [16, 2048, 1024], P('fs', None, 'tp')
- down_ready: bfloat16 [16, 1024, 2048], P('fs', None, 'tp')
Inputs may be any that keep to these rules, and one draw needn't show every extreme that they name: `routes`: each row names 4 different experts. In each aligned block of 128 rows no expert is named more than 64 times, a bound that some block reaches.
All inputs are finite; a program needn't handle non-finite values.
Results may differ from a plain program's by a relative error of at most 0.0089.
Values may be sent and summed in bfloat16 or wider, within the bound.
No kernel may reach another device: no remote copies, remote signals or barrier semaphores. Data moves between devices by JAX's collectives and lax.ppermute only.
A program may use at most 64 MiB of HBM per device.

v0:
```python
import jax
import jax.numpy as jnp
from jax import lax
from jax.sharding import PartitionSpec as P

epsilon = 1e-05


def activate(gate_pre, up_pre):
    gated = jnp.minimum(gate_pre, 7.0)
    upper = jnp.clip(up_pre, -7.0, 7.0)
    return (upper + 1.0) * gated * jax.nn.sigmoid(1.702 * gated)


def shards(tokens, norm_gain, gate_weight, up_weight, down_weight, routes, route_weights):
    gate_send = (norm_gain[None, :, None] * gate_weight).astype(jnp.bfloat16)
    up_send = (norm_gain[None, :, None] * up_weight).astype(jnp.bfloat16)
    down_send = down_weight.astype(jnp.bfloat16)
    gate_ready, up_ready, down_ready = (
        lax.all_to_all(gate_send, "fs", split_axis=0, concat_axis=1, tiled=True),
        lax.all_to_all(up_send, "fs", split_axis=0, concat_axis=1, tiled=True),
        lax.all_to_all(down_send, "fs", split_axis=0, concat_axis=1, tiled=True),
    )
    experts = gate_weight.shape[0]
    tok_rows = tokens.shape[0]
    top_count = routes.shape[1]
    pairs = tok_rows * top_count
    capacity = 2 * pairs // experts
    chosen = routes.reshape(pairs)
    onehot = (chosen[:, None] == jnp.arange(experts, dtype=jnp.int32)[None, :]).astype(jnp.int32)
    position = jnp.sum(jnp.cumsum(onehot, axis=0) * onehot, axis=1) - 1
    slot_index = chosen * capacity + position
    token_index = jnp.arange(pairs, dtype=jnp.int32) // top_count
    values = tokens.astype(jnp.float32)
    squared = lax.psum(jnp.sum(values * values, axis=1), "tp")
    width = values.shape[1] * lax.axis_size("tp")
    normed = (values * lax.rsqrt(squared / width + epsilon)[:, None]).astype(jnp.bfloat16)
    outbound = jnp.zeros((experts * capacity, normed.shape[1]), jnp.bfloat16)
    outbound = (
        outbound.at[slot_index].set(normed[token_index]).reshape(experts, capacity, normed.shape[1])
    )
    gate_matrix = gate_ready[0]
    up_matrix = up_ready[0]
    down_matrix = down_ready[0]
    arrived = lax.all_to_all(outbound, "fs", split_axis=0, concat_axis=0, tiled=True)
    arrived = lax.all_gather(arrived, "tp", axis=2, tiled=True)
    sources = arrived.shape[0]
    items = arrived.shape[1]
    arrived_rows = arrived.reshape(sources * items, arrived.shape[2])
    gate_pre = jnp.dot(arrived_rows, gate_matrix, preferred_element_type=jnp.float32)
    up_pre = jnp.dot(arrived_rows, up_matrix, preferred_element_type=jnp.float32)
    hidden = activate(gate_pre, up_pre).astype(jnp.bfloat16)
    summed = jnp.dot(
        lax.all_gather(hidden, "tp", axis=1, tiled=True),
        down_matrix,
        preferred_element_type=jnp.float32,
    )
    results = summed.astype(jnp.bfloat16).reshape(sources, items, down_matrix.shape[1])
    returned = lax.all_to_all(results, "fs", split_axis=0, concat_axis=0, tiled=True)
    flat_back = returned.reshape(experts * capacity, returned.shape[2])
    picked = (
        flat_back[slot_index].astype(jnp.float32).reshape(tok_rows, top_count, returned.shape[2])
    )
    mixed = jnp.sum(picked * route_weights[:, :, None], axis=1).astype(jnp.bfloat16)
    return (mixed, gate_ready, up_ready, down_ready)


def solution(mesh):
    placed = (
        P("fs", "tp"),
        P("fs"),
        P(None, "fs", "tp"),
        P(None, "fs", "tp"),
        P(None, "fs", "tp"),
        P("fs", None),
        P("fs", None),
    )
    return jax.shard_map(
        shards,
        mesh=mesh,
        in_specs=placed,
        out_specs=(P("fs", "tp"), P("fs", None, "tp"), P("fs", None, "tp"), P("fs", None, "tp")),
        check_vma=False,
    )
```

profile of v0, /device:TPU:12, one launch (start us, length us, event | category | flops | bytes accessed | tf_op | source)
XLA Modules:
  0.0 313.8 jit_solution(14182321171666740326)
XLA Ops:
  7.2 0.8 copy.13
  8.0 0.1 eq.29
  8.1 0.1 eq.25
  8.2 0.7 broadcast_multiply_fusion
  8.9 1.2 reduce-window.6
  10.0 0.2 slice_reduce_fusion
  10.3 0.1 fusion.6
  10.4 0.1 copy.12
  10.5 0.1 mul.66
  10.6 1.1 fusion.3
  11.7 2.5 psum.7
  14.2 1.1 fusion.4
  15.3 7.7 %scatter_custom_fusion = bf16[1024,1024]{1,0:T(8,128)(2,1)} fusion(s32[512]{0:T(512)S(1)} %bitcast.38, bf16[128,1024]{1,0:T(8,128)(2,1)S(1)} %fusion.4, s32[1024]{0:T(1024)S(1)} %pad_clamp_fusion.1, bf16[]{:T(256)} %constant.15.clone.1), kind=kCustom, calls=%fused_computation.8 | custom fusion | bytes 2097154 | tf_op jit(solution)/shard_map/scatter | solution.py:40
  23.0 0.0 copy-start.3
  23.0 7.3 %all-to-all-start = ((bf16[16,64,1024]{2,1,0:T(8,128)(2,1)}), bf16[16,64,1024]{2,1,0:T(8,128)(2,1)}, u32[]{:S(2)}, u32[]{:S(2)}) async-start(bf16[16,64,1024]{2,1,0:T(8,128)(2,1)} %bitcast.4), calls=%async_computation | async-start | bytes 4194304 | tf_op jit(solution)/shard_map/all_to_all | solution.py:45
  30.3 0.0 copy-done.3
  30.3 6.1 %multiply_convert_fusion = (bf16[16,128,512]{2,1,0:T(8,128)(2,1)}, bf16[16,128,512]{2,1,0:T(8,128)(2,1)S(1)}) fusion(f32[16,128,512]{2,1,0:T(8,128)} %param.9, f32[128]{0:T(128)S(1)} %copy-done.3, f32[16,128,512]{2,1,0:T(8,128)} %param.10), kind=kLoop, calls=%fused_computation.3 | loop fusion | flops 4194304 | bytes 12583424 | tf_op jit(solution)/shard_map/convert_element_type | solution.py:16
  36.4 42.3 %all-to-all-done = bf16[16,64,1024]{2,1,0:T(8,128)(2,1)} async-done(((bf16[16,64,1024]{2,1,0:T(8,128)(2,1)}), bf16[16,64,1024]{2,1,0:T(8,128)(2,1)}, u32[]{:S(2)}, u32[]{:S(2)}) %all-to-all-start) | async-done | bytes 2097184 | tf_op jit(solution)/shard_map/all_to_all | solution.py:45
  78.8 52.0 %all_to_all.46 = bf16[16,128,512]{2,1,0:T(8,128)(2,1)} all-to-all(bf16[16,128,512]{2,1,0:T(8,128)(2,1)S(1)} %get-tuple-element.5), channel_id=1, replica_groups=mesh['fs'=16,'tp'=2] {'fs'}, dimensions={0} | all-to-all | bytes 4194304 | tf_op jit(solution)/shard_map/all_to_all | solution.py:21
  130.8 5.5 %all-to-all-start.2 = ((bf16[16,128,512]{2,1,0:T(8,128)(2,1)}), bf16[16,128,512]{2,1,0:T(8,128)(2,1)}, u32[]{:S(2)}, u32[]{:S(2)}) async-start(bf16[16,128,512]{2,1,0:T(8,128)(2,1)} %get-tuple-element.4), calls=%async_computation.2 | async-start | bytes 4194304 | tf_op jit(solution)/shard_map/all_to_all | solution.py:20
  136.2 0.0 all-gather.3.cloned.1.call-start
  136.3 0.7 all-gather.3.cloned.1.call-update
  137.0 3.8 %convert_element_type.42 = bf16[16,64,1024]{2,1,0:T(8,128)(2,1)} convert(f32[16,64,1024]{2,1,0:T(8,128)} %param.11) | non-fusion elementwise | flops 1048576 | bytes 6291456 | tf_op jit(solution)/shard_map/convert_element_type | solution.py:18
  140.8 0.0 copy-start
  140.8 42.9 %all-to-all-done.2 = bf16[16,128,512]{2,1,0:T(8,128)(2,1)} async-done(((bf16[16,128,512]{2,1,0:T(8,128)(2,1)}), bf16[16,128,512]{2,1,0:T(8,128)(2,1)}, u32[]{:S(2)}, u32[]{:S(2)}) %all-to-all-start.2) | async-done | bytes 2097184 | tf_op jit(solution)/shard_map/all_to_all | solution.py:20
  183.7 4.7 %all-to-all-start.3 = ((bf16[16,64,1024]{2,1,0:T(8,128)(2,1)}), bf16[16,64,1024]{2,1,0:T(8,128)(2,1)}, u32[]{:S(2)}, u32[]{:S(2)}) async-start(bf16[16,64,1024]{2,1,0:T(8,128)(2,1)} %convert_element_type.42), calls=%async_computation.3 | async-start | bytes 4194304 | tf_op jit(solution)/shard_map/all_to_all | solution.py:22
  188.4 0.2 all-gather.5.cloned.1.call-start
  188.6 0.0 all-gather.3.cloned.1.call-done
  188.7 0.0 copy-done
  188.7 0.0 copy-start.4
  188.7 4.7 %fusion.8 = f32[1024,512]{1,0:T(8,128)S(1)} fusion(bf16[1024,2048]{1,0:T(8,128)(2,1)} %bitcast.42, bf16[2048,512]{1,0:T(8,128)(2,1)S(1)} %bitcast.35), kind=kOutput, calls=%fused_computation.34 | convolution fusion | flops 2147483648 | bytes 8388608 | tf_op jit(solution)/shard_map/dot_general | solution.py:51
  193.4 0.0 copy-done.4
  193.4 5.4 %multiply_convert_fusion.2 = bf16[1024,512]{1,0:T(8,128)(2,1)} fusion(f32[1024,512]{1,0:T(8,128)S(1)} %fusion.8, bf16[1024,2048]{1,0:T(8,128)(2,1)S(1)} %bitcast.43, bf16[2048,512]{1,0:T(8,128)(2,1)} %bitcast.7), kind=kOutput, calls=%fused_computation.6 | convolution fusion | flops 2152726528 | bytes 9437184 | tf_op jit(solution)/shard_map/dot_general | solution.py:50
  198.8 0.0 all-gather.5.cloned.1.call-update
  198.8 37.4 %all-to-all-done.3 = bf16[16,64,1024]{2,1,0:T(8,128)(2,1)} async-done(((bf16[16,64,1024]{2,1,0:T(8,128)(2,1)}), bf16[16,64,1024]{2,1,0:T(8,128)(2,1)}, u32[]{:S(2)}, u32[]{:S(2)}) %all-to-all-start.3) | async-done | bytes 2097184 | tf_op jit(solution)/shard_map/all_to_all | solution.py:22
  236.2 0.0 all-gather.5.cloned.1.call-done
  236.2 5.9 %convolution_convert_fusion = bf16[1024,1024]{1,0:T(8,128)(2,1)} fusion(bf16[1024,1024]{1,0:T(8,128)(2,1)} %all-gather.5.cloned.1.call-done, bf16[1024,1024]{1,0:T(8,128)(2,1)} %bitcast.8), kind=kOutput, calls=%fused_computation.7 | convolution fusion | flops 2148532224 | bytes 6291456 | tf_op jit(solution)/shard_map/dot_general | solution.py:53
  242.1 0.0 copy-start.2
  242.1 4.8 %all-to-all-start.4 = ((bf16[16,64,1024]{2,1,0:T(8,128)(2,1)}), bf16[16,64,1024]{2,1,0:T(8,128)(2,1)S(1)}, u32[]{:S(2)}, u32[]{:S(2)}) async-start(bf16[16,64,1024]{2,1,0:T(8,128)(2,1)} %bitcast.37), calls=%async_computation.4 | async-start | bytes 4194304 | tf_op jit(solution)/shard_map/all_to_all | solution.py:59
  246.9 0.0 copy-done.2
  246.9 0.1 copy.16
  247.0 47.5 %all-to-all-done.4 = bf16[16,64,1024]{2,1,0:T(8,128)(2,1)S(1)} async-done(((bf16[16,64,1024]{2,1,0:T(8,128)(2,1)}), bf16[16,64,1024]{2,1,0:T(8,128)(2,1)S(1)}, u32[]{:S(2)}, u32[]{:S(2)}) %all-to-all-start.4) | async-done | bytes 2097184 | tf_op jit(solution)/shard_map/all_to_all | solution.py:59
  294.6 2.0 gather_fusion
  296.6 0.7 reshape.141
  297.3 2.1 multiply_reduce_fusion
  299.4 0.0 copy-start.1
  299.4 3.2 %copy.22 = bf16[1,2048,512]{2,1,0:T(8,128)(2,1)} copy(bf16[1,2048,512]{2,1,0:T(8,128)(2,1)} %bitcast.11) | data formatting | bytes 4194304
  302.6 0.0 copy-done.1
  302.6 1.3 copy.23
  303.9 3.1 copy.24
  (9 shorter events, 0.1 us)
Async XLA Ops:
  23.0 7.3 %copy-start.3 = (f32[128]{0:T(128)S(1)}, f32[128]{0:T(128)}, u32[]{:S(2)}) copy-start(f32[128]{0:T(128)} %param.8) | copy-start | bytes 1540
  23.0 55.8 %all-to-all-start = ((bf16[16,64,1024]{2,1,0:T(8,128)(2,1)}), bf16[16,64,1024]{2,1,0:T(8,128)(2,1)}, u32[]{:S(2)}, u32[]{:S(2)}) async-start(bf16[16,64,1024]{2,1,0:T(8,128)(2,1)} %bitcast.4), calls=%async_computation | async-start | bytes 4194304 | tf_op jit(solution)/shard_map/all_to_all | solution.py:45
  130.8 52.9 %all-to-all-start.2 = ((bf16[16,128,512]{2,1,0:T(8,128)(2,1)}), bf16[16,128,512]{2,1,0:T(8,128)(2,1)}, u32[]{:S(2)}, u32[]{:S(2)}) async-start(bf16[16,128,512]{2,1,0:T(8,128)(2,1)} %get-tuple-element.4), calls=%async_computation.2 | async-start | bytes 4194304 | tf_op jit(solution)/shard_map/all_to_all | solution.py:20
  136.2 52.4 %all-gather.3.cloned.1.call-start = ((), (), s32[]{:S(2)}) async-start(), calls=%async_computation.5 | async-start | bytes 6291456 | tf_op jit(solution)/shard_map/all_gather | solution.py:46
  140.8 47.9 %copy-start = (bf16[16,128,512]{2,1,0:T(8,128)(2,1)S(1)}, bf16[16,128,512]{2,1,0:T(8,128)(2,1)}, u32[]{:S(2)}) copy-start(bf16[16,128,512]{2,1,0:T(8,128)(2,1)} %all_to_all.46) | copy-start | bytes 6291460
  183.7 52.5 %all-to-all-start.3 = ((bf16[16,64,1024]{2,1,0:T(8,128)(2,1)}), bf16[16,64,1024]{2,1,0:T(8,128)(2,1)}, u32[]{:S(2)}, u32[]{:S(2)}) async-start(bf16[16,64,1024]{2,1,0:T(8,128)(2,1)} %convert_element_type.42), calls=%async_computation.3 | async-start | bytes 4194304 | tf_op jit(solution)/shard_map/all_to_all | solution.py:22
  188.4 47.8 %all-gather.5.cloned.1.call-start = ((), (), s32[]{:S(2)}) async-start(), calls=%async_computation.6 | async-start | bytes 3145728 | tf_op jit(solution)/shard_map/all_gather | solution.py:54
  188.7 4.7 %copy-start.4 = (bf16[16,64,2048]{2,1,0:T(8,128)(2,1)S(1)}, bf16[16,64,2048]{2,1,0:T(8,128)(2,1)}, u32[]{:S(2)}) copy-start(bf16[16,64,2048]{2,1,0:T(8,128)(2,1)} %all-gather.3.cloned.1.call-done) | copy-start | bytes 12582916
  242.1 4.8 %copy-start.2 = (f32[128,4]{0,1:T(4,128)S(1)}, f32[128,4]{0,1:T(4,128)}, u32[]{:S(2)}) copy-start(f32[128,4]{0,1:T(4,128)} %param.13) | copy-start | bytes 6148
  242.1 52.5 %all-to-all-start.4 = ((bf16[16,64,1024]{2,1,0:T(8,128)(2,1)}), bf16[16,64,1024]{2,1,0:T(8,128)(2,1)S(1)}, u32[]{:S(2)}, u32[]{:S(2)}) async-start(bf16[16,64,1024]{2,1,0:T(8,128)(2,1)} %bitcast.37), calls=%async_computation.4 | async-start | bytes 4194304 | tf_op jit(solution)/shard_map/all_to_all | solution.py:59
  299.4 3.2 %copy-start.1 = (bf16[16,128,512]{2,1,0:T(8,128)(2,1)S(1)}, bf16[16,128,512]{2,1,0:T(8,128)(2,1)}, u32[]{:S(2)}) copy-start(bf16[16,128,512]{2,1,0:T(8,128)(2,1)} %all_to_all.46) | copy-start | bytes 6291460
Sparse Core Ops, SparseCore 0:
  138.6 14.8 all-gather.2
  198.9 11.6 all-gather.4
where the time goes:
time: 314 us
  waiting for transfers between devices  171 us (54%)
  blocking collectives  54.4 us (17%)
  starting transfers between devices  22.6 us (7%)
  local copies, waits for them, and re-layouts  19.6 us (6%)
  other arithmetic  16.2 us (5%)
  matrix products  16 us (5%)
  between operations  14.2 us (5%)
    all_to_all x1, blocking collectives, shards(): lax.all_to_all(up_send, 'fs', split_axis=0, concat_axis=1, tiled=True)  52 us
    all_to_all x1, waiting for transfers between devices, shards(): lax.all_to_all(results, 'fs', split_axis=0, concat_axis=0, tiled=True)  47.5 us
    all_to_all x1, waiting for transfers between devices, shards(): lax.all_to_all(gate_send, 'fs', split_axis=0, concat_axis=1, tiled=True)  42.9 us
    all_to_all x1, waiting for transfers between devices, shards(): lax.all_to_all(outbound, 'fs', split_axis=0, concat_axis=0, tiled=True)  42.3 us
    all_to_all x1, waiting for transfers between devices, shards(): lax.all_to_all(down_send, 'fs', split_axis=0, concat_axis=1, tiled=True)  37.4 us
    unnamed x15, local copies, waits for them, and re-layouts  8.51 us
    scatter x1, local copies, waits for them, and re-layouts, shards(): outbound.at[slot_index].set(normed[token_index])  7.72 us
    all_to_all x1, starting transfers between devices, shards(): lax.all_to_all(outbound, 'fs', split_axis=0, concat_axis=0, tiled=True)  7.3 us
  transfers between devices with their start and end apart: 6, of which 4 were waited for; matrix products, arithmetic and copies ran while one was open for 6% of the time, Pallas kernels for 0%

commit v1 on v0

v1 whole, which is shorter than its diff:
```python
import math

import jax
import jax.numpy as jnp
from jax import lax
from jax.sharding import PartitionSpec as P

epsilon = 1e-05
bf16 = jnp.bfloat16
f32 = jnp.float32


def activate(gate_pre, up_pre):
    gated = jnp.minimum(gate_pre, 7.0)
    upper = jnp.clip(up_pre, -7.0, 7.0)
    return (upper + 1.0) * gated * jax.nn.sigmoid(1.702 * gated)


def parts_of(weights):
    first = lax.reduce_precision(weights, 8, 7)
    rest = weights - first
    second = lax.reduce_precision(rest, 8, 7)
    return [p.astype(bf16) for p in (first, second, rest - second)]


def over_tp(value):
    size, mine = lax.axis_size("tp"), lax.axis_index("tp")
    blocks = [(mine, value)]
    for j in range(1, size):
        pairs = [(s, (s + j) % size) for s in range(size)]
        blocks.append(((mine - j) % size, lax.ppermute(value, "tp", pairs)))
    return blocks


def product(blocks, matrix):
    total = 0.0
    for owner, value in blocks:
        depth = value.shape[1]
        rows = lax.dynamic_slice_in_dim(matrix, owner * depth, depth, 0)
        total = total + jnp.dot(value, rows, preferred_element_type=f32)
    return total


def shards(tokens, norm_gain, gate_weight, up_weight, down_weight, routes, route_weights):
    count, tp = lax.axis_size("fs"), lax.axis_size("tp")
    inner = math.gcd(count, 4)
    depth = count // inner
    me = lax.axis_index("fs")
    level, place = me // inner, me % inner
    rows, width = tokens.shape
    top = routes.shape[1]
    experts = gate_weight.shape[0]
    capacity = 2 * rows * top // experts

    gate_send = (norm_gain[None, :, None] * gate_weight).astype(bf16)
    up_send = (norm_gain[None, :, None] * up_weight).astype(bf16)
    down_send = down_weight.astype(bf16)
    gate_ready, up_ready, down_ready = (
        lax.all_to_all(sent, "fs", split_axis=0, concat_axis=1, tiled=True)
        for sent in (gate_send, up_send, down_send)
    )

    values = tokens.astype(f32)
    squared = lax.psum(jnp.sum(values * values, axis=1), "tp")
    normed = (values * lax.rsqrt(squared / (width * tp) + epsilon)[:, None]).astype(bf16)
    notes = jnp.concatenate([routes.T.astype(bf16)] + parts_of(route_weights.T), axis=0)
    notes = jnp.concatenate([notes[: 2 * top], notes[2 * top :]], axis=1)
    notes = jnp.pad(notes, ((0, 0), (0, width - 2 * rows)))
    payload = jnp.concatenate([normed, notes], axis=0)

    def shift(value, step, first):
        pairs = []
        for s in range(count):
            at = s // inner
            if 0 <= at + step < depth and (at >= first if step > 0 else at < depth - first):
                pairs.append((s, s + step * inner))
        return lax.ppermute(value, "fs", pairs)

    ups, downs = [payload], [payload]
    for r in range(1, depth):
        ups.append(shift(ups[-1], 1, r - 1))
        downs.append(shift(downs[-1], -1, r - 1))
    column = [payload]
    for q in range(1, depth):
        column.append(jnp.where(level + q < depth, downs[q], ups[depth - q]))
    column = jnp.stack(column)
    column_tokens = column[:, :rows]
    column_notes = column[:, rows:, : 2 * rows].astype(f32)
    column_routes = column_notes[:, :top, :rows]
    column_weights = (
        column_notes[:, top:, :rows] + column_notes[:, :top, rows:] + column_notes[:, top:, rows:]
    )

    targets = level * inner + jnp.bitwise_xor(place, jnp.arange(inner, dtype=jnp.int32))
    named = column_routes[:, None] == targets.astype(f32)[None, :, None, None]
    member = jnp.any(named, axis=2)
    share = jnp.sum(jnp.where(named, column_weights[:, None], 0.0), axis=2)
    before = (jnp.arange(rows)[:, None] < jnp.arange(rows)[None, :]).astype(bf16)
    position = jnp.einsum(
        "qrs,st->qrt", member.astype(bf16), before, preferred_element_type=f32
    )
    slots = jnp.arange(capacity, dtype=jnp.int32).astype(f32)
    chosen = member[:, :, None, :] & (position[:, :, None, :] == slots[None, None, :, None])
    picked = jnp.einsum(
        "qrct,qtd->rqcd", chosen.astype(bf16), column_tokens, preferred_element_type=f32
    ).astype(bf16)
    picked = picked.reshape(inner, depth * capacity, width)

    def swap(value, r):
        if r == 0:
            return value
        return lax.ppermute(value, "fs", [(s, s ^ r) for s in range(count)])

    arrived = jnp.concatenate([swap(picked[r], r) for r in range(inner)], axis=0)
    arrived = over_tp(arrived)
    gate_pre = product(arrived, gate_ready[0])
    up_pre = product(arrived, up_ready[0])
    hidden = over_tp(activate(gate_pre, up_pre).astype(bf16))
    results = product(hidden, down_ready[0]).astype(bf16)
    results = results.reshape(inner, depth * capacity, width)
    back = jnp.stack([swap(results[r], r) for r in range(inner)])
    back = back.reshape(inner, depth, capacity, width)
    scale = jnp.where(chosen, share[:, :, None, :], 0.0)
    partial = jnp.einsum(
        "qrct,rqcd->qtd",
        scale,
        back.astype(f32),
        preferred_element_type=f32,
        precision=lax.Precision.HIGHEST,
    )
    upward, downward = 0.0, 0.0
    for r in range(1, depth):
        def carried(value, step):
            pairs = []
            for s in range(count):
                at = s // inner
                if step > 0 and at + depth - r < depth or step < 0 and at - (depth - r) >= 0:
                    pairs.append((s, s + step * inner))
            return lax.ppermute(value.astype(bf16), "fs", pairs).astype(f32)

        upward = carried(partial[depth - r] + upward, 1)
        downward = carried(partial[r] + downward, -1)
    mixed = (partial[0] + upward + downward).astype(bf16)
    return (mixed, gate_ready, up_ready, down_ready)


def solution(mesh):
    placed = (
        P("fs", "tp"),
        P("fs"),
        P(None, "fs", "tp"),
        P(None, "fs", "tp"),
        P(None, "fs", "tp"),
        P("fs", None),
        P("fs", None),
    )
    return jax.shard_map(
        shards,
        mesh=mesh,
        in_specs=placed,
        out_specs=(P("fs", "tp"), P("fs", None, "tp"), P("fs", None, "tp"), P("fs", None, "tp")),
        check_vma=False,
    )
```

time: 314 us -> 295 us (0.939)
  blocking collectives: 54.4 us -> 2.46 us
  starting transfers between devices: 22.6 us -> 54.8 us
  waiting for transfers between devices: 171 us -> 195 us
  between operations: 14.2 us -> 1.04 us
  local copies, waits for them, and re-layouts: 19.6 us -> 9.27 us
  other arithmetic: 16.2 us -> 11.7 us
  matrix products: 16 us -> 19.8 us
    ppermute x0 -> x20, waiting for transfers between devices: none -> 115 us  [the longest x6 54.6 us: shift(): return lax.ppermute(value, 'fs', pairs)]
    all_to_all x4 -> x3, waiting for transfers between devices: 170 us -> 79.5 us  [shards(): lax.all_to_all(sent, 'fs', split_axis=0, concat_axis=1, tiled=True)]
    all_to_all x1 -> x0, blocking collectives: 52 us -> none  [shards(): lax.all_to_all(up_send, 'fs', split_axis=0, concat_axis=1, tiled=True)]
    ppermute x0 -> x20, starting transfers between devices: none -> 33.5 us  [the longest x6 14.6 us: shift(): return lax.ppermute(value, 'fs', pairs)]
    scatter x1 -> x0, local copies, waits for them, and re-layouts: 7.72 us -> none  [shards(): outbound.at[slot_index].set(normed[token_index])]
    dot_general x3 -> x9, matrix products: 16 us -> 19.8 us  [the longest x6 17.5 us: product(): total = total + jnp.dot(value, rows, preferred_element_type=f32)]
    convert_element_type x4 -> x11, other arithmetic: 11 us -> 9.72 us  [the longest x1 6.84 us: shards(): up_send = (norm_gain[None, :, None] * up_weight).astype(bf16)]
    all_to_all x4 -> x3, starting transfers between devices: 22.3 us -> 21.3 us  [shards(): lax.all_to_all(sent, 'fs', split_axis=0, concat_axis=1, tiled=True)]
  transfers between devices with their start and end apart: 6 -> 23, of which waited for: 4 -> 14; matrix products, arithmetic and copies ran while one was open for 6% -> 7% of each run, Pallas kernels for 0% -> 0%
where the time goes in v1:
time: 295 us; the launch traced here: 294 us
  waiting for transfers between devices  195 us (66%)
  starting transfers between devices  54.8 us (19%)
  matrix products  19.8 us (7%)
  other arithmetic  11.7 us (4%)
  local copies, waits for them, and re-layouts  9.27 us (3%)
    all_to_all x3, waiting for transfers between devices, shards(): lax.all_to_all(sent, 'fs', split_axis=0, concat_axis=1, tiled=True)  79.5 us
    ppermute x6, waiting for transfers between devices, shift(): return lax.ppermute(value, 'fs', pairs)  54.6 us
    ppermute x6, waiting for transfers between devices, swap(): return lax.ppermute(value, 'fs', [(s, s ^ r) for s in range(count)])  40.9 us
    all_to_all x3, starting transfers between devices, shards(): lax.all_to_all(sent, 'fs', split_axis=0, concat_axis=1, tiled=True)  21.3 us
    ppermute x6, waiting for transfers between devices, carried(): return lax.ppermute(value.astype(bf16), 'fs', pairs).astype(f32)  19.6 us
    dot_general x6, matrix products, product(): total = total + jnp.dot(value, rows, preferred_element_type=f32)  17.5 us
    ppermute x6, starting transfers between devices, shift(): return lax.ppermute(value, 'fs', pairs)  14.6 us
    ppermute x6, starting transfers between devices, carried(): return lax.ppermute(value.astype(bf16), 'fs', pairs).astype(f32)  11.8 us
  transfers between devices with their start and end apart: 23, of which 14 were waited for; matrix products, arithmetic and copies ran while one was open for 7% of the time, Pallas kernels for 0%

profile of v1, /device:TPU:12, one launch (start us, length us, event | category | flops | bytes accessed | tf_op | source)
XLA Modules:
  0.0 293.7 jit_solution(7040111068791807155)
XLA Ops:
  0.6 6.8 %multiply_convert_fusion.1 = (bf16[16,128,512]{2,1,0:T(8,128)(2,1)}, bf16[16,128,512]{2,1,0:T(8,128)(2,1)}) fusion(f32[16,128,512]{2,1,0:T(8,128)} %param.10, f32[128]{0:T(128)} %param.8, f32[16,128,512]{2,1,0:T(8,128)} %param.9), kind=kLoop, calls=%fused_computation.2 | loop fusion | flops 4194304 | bytes 12583424 | tf_op jit(solution)/shard_map/convert_element_type | solution.py:56
  7.5 7.3 %all-to-all-start.1 = ((bf16[16,128,512]{2,1,0:T(8,128)(2,1)}), bf16[16,128,512]{2,1,0:T(8,128)(2,1)S(1)}, u32[]{:S(2)}, u32[]{:S(2)}) async-start(bf16[16,128,512]{2,1,0:T(8,128)(2,1)} %get-tuple-element.26), calls=%async_computation.1 | async-start | bytes 4194304 | tf_op jit(solution)/shard_map/all_to_all | solution.py:59
  14.8 0.1 fusion.24
  14.9 2.5 psum.7
  17.4 0.1 fusion.25
  17.6 45.4 %all-to-all-done.1 = bf16[16,128,512]{2,1,0:T(8,128)(2,1)S(1)} async-done(((bf16[16,128,512]{2,1,0:T(8,128)(2,1)}), bf16[16,128,512]{2,1,0:T(8,128)(2,1)S(1)}, u32[]{:S(2)}, u32[]{:S(2)}) %all-to-all-start.1) | async-done | bytes 2097184 | tf_op jit(solution)/shard_map/all_to_all | solution.py:59
  62.9 1.3 copy-done
  64.3 4.9 %all-to-all-start = ((bf16[16,128,512]{2,1,0:T(8,128)(2,1)}), bf16[16,128,512]{2,1,0:T(8,128)(2,1)}, u32[]{:S(2)}, u32[]{:S(2)}) async-start(bf16[16,128,512]{2,1,0:T(8,128)(2,1)} %get-tuple-element.25), calls=%async_computation | async-start | bytes 4194304 | tf_op jit(solution)/shard_map/all_to_all | solution.py:59
  69.2 2.5 collective-permute-start
  71.7 3.4 %collective-permute-start.1 = (bf16[136,1024]{1,0:T(8,128)(2,1)S(1)}, bf16[136,1024]{1,0:T(8,128)(2,1)S(1)}, u32[]{:S(2)}, u32[]{:S(2)}) collective-permute-start(bf16[136,1024]{1,0:T(8,128)(2,1)S(1)} %get-tuple-element.19), channel_id=1, source_target_pairs={{0,8},{2,10},{4,12},{6,14},{8,16},{10,18},{12,20},{14,22},{16,24},... | collective-permute-start | bytes 835592 | tf_op jit(solution)/shard_map/ppermute | solution.py:77
  75.1 47.1 %collective-permute-done = bf16[136,1024]{1,0:T(8,128)(2,1)S(1)} collective-permute-done((bf16[136,1024]{1,0:T(8,128)(2,1)S(1)}, bf16[136,1024]{1,0:T(8,128)(2,1)S(1)}, u32[]{:S(2)}, u32[]{:S(2)}) %collective-permute-start) | collective-permute-done | bytes 278560 | tf_op jit(solution)/shard_map/ppermute | solution.py:77
  122.2 1.9 collective-permute-start.4
  124.1 3.9 %collective-permute-start.2 = (bf16[136,1024]{1,0:T(8,128)(2,1)S(1)}, bf16[136,1024]{1,0:T(8,128)(2,1)S(1)}, u32[]{:S(2)}, u32[]{:S(2)}) collective-permute-start(bf16[136,1024]{1,0:T(8,128)(2,1)S(1)} %collective-permute-done.1), channel_id=1, source_target_pairs={{8,16},{10,18},{12,20},{14,22},{16,24},{18,26},{20,28},{22,30},{9,... | collective-permute-start | bytes 835592 | tf_op jit(solution)/shard_map/ppermute | solution.py:77
  128.1 3.6 %collective-permute-done.4 = bf16[136,1024]{1,0:T(8,128)(2,1)S(1)} collective-permute-done((bf16[136,1024]{1,0:T(8,128)(2,1)S(1)}, bf16[136,1024]{1,0:T(8,128)(2,1)S(1)}, u32[]{:S(2)}, u32[]{:S(2)}) %collective-permute-start.4) | collective-permute-done | bytes 278560 | tf_op jit(solution)/shard_map/ppermute | solution.py:77
  131.8 2.2 collective-permute-start.5
  134.0 0.7 collective-permute-start.3
  134.7 3.8 %collective-permute-done.5 = bf16[136,1024]{1,0:T(8,128)(2,1)S(1)} collective-permute-done((bf16[136,1024]{1,0:T(8,128)(2,1)S(1)}, bf16[136,1024]{1,0:T(8,128)(2,1)S(1)}, u32[]{:S(2)}, u32[]{:S(2)}) %collective-permute-start.5) | collective-permute-done | bytes 278560 | tf_op jit(solution)/shard_map/ppermute | solution.py:77
  138.7 0.1 compare_reduce_fusion
  138.8 0.1 fusion.41
  138.9 0.7 convert_bitcast_fusion
  139.7 0.2 fusion.63
  139.9 0.5 collective-permute-start.8
  140.3 2.1 collective-permute-start.7
  142.4 1.0 collective-permute-start.6
  143.4 12.2 %collective-permute-done.8 = bf16[256,1024]{1,0:T(8,128)(2,1)S(1)} collective-permute-done((bf16[256,1024]{1,0:T(8,128)(2,1)S(1)}, bf16[256,1024]{1,0:T(8,128)(2,1)S(1)}, u32[]{:S(2)}, u32[]{:S(2)}) %collective-permute-start.8) | collective-permute-done | bytes 524320 | tf_op jit(solution)/shard_map/ppermute | solution.py:112
  155.6 7.5 %collective-permute-done.7 = bf16[256,1024]{1,0:T(8,128)(2,1)S(1)} collective-permute-done((bf16[256,1024]{1,0:T(8,128)(2,1)S(1)}, bf16[256,1024]{1,0:T(8,128)(2,1)S(1)}, u32[]{:S(2)}, u32[]{:S(2)}) %collective-permute-start.7) | collective-permute-done | bytes 524320 | tf_op jit(solution)/shard_map/ppermute | solution.py:112
  163.1 1.5 pad_maximum_fusion
  164.6 0.1 copy-done.7
  164.8 1.7 copy-done.3
  166.4 1.7 convert_element_type.119
  168.1 9.1 %all-to-all-start.2 = ((bf16[16,64,1024]{2,1,0:T(8,128)(2,1)}), bf16[16,64,1024]{2,1,0:T(8,128)(2,1)S(1)}, u32[]{:S(2)}, u32[]{:S(2)}) async-start(bf16[16,64,1024]{2,1,0:T(8,128)(2,1)} %convert_element_type.119), calls=%async_computation.2 | async-start | bytes 4194304 | tf_op jit(solution)/shard_map/all_to_all | solution.py:59
  177.2 2.8 fusion.22
  180.0 3.2 %fusion.20 = f32[1024,512]{1,0:T(8,128)S(1)} fusion(bf16[1024,1024]{1,0:T(8,128)(2,1)} %collective-permute-done.9, bf16[2048,512]{1,0:T(8,128)(2,1)} %bitcast.14, s32[]{:T(128)S(6)} %select_n.71), kind=kOutput, calls=%fused_computation.26 | convolution fusion | flops 1073741824 | bytes 5242884 | tf_op jit(solution)/shard_map/dot_general | solution.py:40
  183.3 2.9 fusion.17
  186.3 4.8 %multiply_convert_fusion.2 = bf16[1024,512]{1,0:T(8,128)(2,1)} fusion(f32[1024,512]{1,0:T(8,128)S(1)} %fusion.17, f32[1024,512]{1,0:T(8,128)S(1)} %fusion.22, f32[1024,512]{1,0:T(8,128)S(1)} %fusion.20, bf16[2048,512]{1,0:T(8,128)(2,1)S(1)} %bitcast.87, s32[]{:T(128)S(6)} %select_n.69, bf16[256,1024]{1,0:T(8,128)(2,1)S(1)} %collective-permute-done.8, ...), kind=kOutput, calls=%fused_computation.12 | convolution fusion | flops 1088421888 | bytes 10485764 | tf_op jit(solution)/shard_map/dot_general | solution.py:40
  191.1 34.1 %all-to-all-done.2 = bf16[16,64,1024]{2,1,0:T(8,128)(2,1)S(1)} async-done(((bf16[16,64,1024]{2,1,0:T(8,128)(2,1)}), bf16[16,64,1024]{2,1,0:T(8,128)(2,1)S(1)}, u32[]{:S(2)}, u32[]{:S(2)}) %all-to-all-start.2) | async-done | bytes 2097184 | tf_op jit(solution)/shard_map/all_to_all | solution.py:59
  225.2 2.5 fusion.15
  227.7 1.3 add_convert_fusion
  229.0 0.2 fusion.62
  229.2 0.3 collective-permute-start.13
  229.5 2.4 collective-permute-start.12
  231.9 0.9 collective-permute-start.11
  232.7 0.1 fusion.43
  232.8 12.1 %collective-permute-done.13 = bf16[256,1024]{1,0:T(8,128)(2,1)S(1)} collective-permute-done((bf16[256,1024]{1,0:T(8,128)(2,1)S(1)}, bf16[256,1024]{1,0:T(8,128)(2,1)S(1)}, u32[]{:S(2)}, u32[]{:S(2)}) %collective-permute-start.13) | collective-permute-done | bytes 524320 | tf_op jit(solution)/shard_map/ppermute | solution.py:112
  244.9 9.1 %collective-permute-done.12 = bf16[256,1024]{1,0:T(8,128)(2,1)S(1)} collective-permute-done((bf16[256,1024]{1,0:T(8,128)(2,1)S(1)}, bf16[256,1024]{1,0:T(8,128)(2,1)S(1)}, u32[]{:S(2)}, u32[]{:S(2)}) %collective-permute-start.12) | collective-permute-done | bytes 524320 | tf_op jit(solution)/shard_map/ppermute | solution.py:112
  254.0 1.3 fusion.8
  255.4 0.1 fusion.31
  255.4 1.3 collective-permute-start.14
  256.7 0.7 collective-permute-start.17
  257.4 7.8 %collective-permute-done.14 = bf16[128,1024]{1,0:T(8,128)(2,1)S(1)} collective-permute-done((bf16[128,1024]{1,0:T(8,128)(2,1)S(1)}, bf16[128,1024]{1,0:T(8,128)(2,1)S(1)}, u32[]{:S(2)}, u32[]{:S(2)}) %collective-permute-start.14) | collective-permute-done | bytes 262176 | tf_op jit(solution)/shard_map/ppermute | solution.py:139
  265.2 0.1 add_convert_fusion.4
  265.4 2.7 collective-permute-start.15
  268.1 1.3 collective-permute-start.18
  269.4 5.1 %collective-permute-done.15 = bf16[128,1024]{1,0:T(8,128)(2,1)S(1)} collective-permute-done((bf16[128,1024]{1,0:T(8,128)(2,1)S(1)}, bf16[128,1024]{1,0:T(8,128)(2,1)S(1)}, u32[]{:S(2)}, u32[]{:S(2)}) %collective-permute-start.15) | collective-permute-done | bytes 262176 | tf_op jit(solution)/shard_map/ppermute | solution.py:139
  274.5 2.4 collective-permute-done.18
  276.8 0.2 add_convert_fusion.3
  277.0 1.9 collective-permute-start.19
  278.9 3.9 %collective-permute-start.16 = (bf16[128,1024]{1,0:T(8,128)(2,1)S(1)}, bf16[128,1024]{1,0:T(8,128)(2,1)S(1)}, u32[]{:S(2)}, u32[]{:S(2)}) collective-permute-start(bf16[128,1024]{1,0:T(8,128)(2,1)S(1)} %get-tuple-element.4), channel_id=1, source_target_pairs={{0,8},{2,10},{4,12},{6,14},{8,16},{10,18},{12,20},{14,22},{16,24},... | collective-permute-start | bytes 786440 | tf_op jit(solution)/shard_map/ppermute | solution.py:139
  282.9 2.4 collective-permute-done.19
  285.3 1.9 collective-permute-done.16
  287.2 0.8 fusion.28
  288.0 1.3 copy.24
  289.3 3.0 %copy.25 = bf16[1,2048,512]{2,1,0:T(8,128)(2,1)} copy(bf16[1,2048,512]{2,1,0:T(8,128)(2,1)} %bitcast.32) | data formatting | bytes 4194304
  292.4 1.3 copy.26
  (42 shorter events, 0.3 us)
Async XLA Ops:
  7.5 7.3 %copy-start.4 = (bf16[128,1024]{1,0:T(8,128)(2,1)S(1)}, bf16[128,1024]{1,0:T(8,128)(2,1)}, u32[]{:S(2)}) copy-start(bf16[128,1024]{1,0:T(8,128)(2,1)} %param.7) | copy-start | bytes 786436
  7.5 9.9 %copy-start.9 = (s32[128,4]{0,1:T(4,128)S(1)}, s32[128,4]{0,1:T(4,128)}, u32[]{:S(2)}) copy-start(s32[128,4]{0,1:T(4,128)} %param.12) | copy-start | bytes 6148
  7.5 9.9 %copy-start.10 = (f32[128,4]{0,1:T(4,128)S(1)}, f32[128,4]{0,1:T(4,128)}, u32[]{:S(2)}) copy-start(f32[128,4]{0,1:T(4,128)} %param.13) | copy-start | bytes 6148
  7.5 55.5 %all-to-all-start.1 = ((bf16[16,128,512]{2,1,0:T(8,128)(2,1)}), bf16[16,128,512]{2,1,0:T(8,128)(2,1)S(1)}, u32[]{:S(2)}, u32[]{:S(2)}) async-start(bf16[16,128,512]{2,1,0:T(8,128)(2,1)} %get-tuple-element.26), calls=%async_computation.1 | async-start | bytes 4194304 | tf_op jit(solution)/shard_map/all_to_all | solution.py:59
  62.9 1.3 copy-start
  64.3 103.9 %all-to-all-start = ((bf16[16,128,512]{2,1,0:T(8,128)(2,1)}), bf16[16,128,512]{2,1,0:T(8,128)(2,1)}, u32[]{:S(2)}, u32[]{:S(2)}) async-start(bf16[16,128,512]{2,1,0:T(8,128)(2,1)} %get-tuple-element.25), calls=%async_computation | async-start | bytes 4194304 | tf_op jit(solution)/shard_map/all_to_all | solution.py:59
  69.2 53.0 %collective-permute-start = (bf16[136,1024]{1,0:T(8,128)(2,1)S(1)}, bf16[136,1024]{1,0:T(8,128)(2,1)S(1)}, u32[]{:S(2)}, u32[]{:S(2)}) collective-permute-start(bf16[136,1024]{1,0:T(8,128)(2,1)S(1)} %get-tuple-element.19), channel_id=1, source_target_pairs={{8,0},{10,2},{12,4},{14,6},{16,8},{18,10},{20,12},{22,14},{24,16},... | collective-permute-start | bytes 835592 | tf_op jit(solution)/shard_map/ppermute | solution.py:77
  71.7 52.4 %collective-permute-start.1 = (bf16[136,1024]{1,0:T(8,128)(2,1)S(1)}, bf16[136,1024]{1,0:T(8,128)(2,1)S(1)}, u32[]{:S(2)}, u32[]{:S(2)}) collective-permute-start(bf16[136,1024]{1,0:T(8,128)(2,1)S(1)} %get-tuple-element.19), channel_id=1, source_target_pairs={{0,8},{2,10},{4,12},{6,14},{8,16},{10,18},{12,20},{14,22},{16,24},... | collective-permute-start | bytes 835592 | tf_op jit(solution)/shard_map/ppermute | solution.py:77
  122.2 9.6 %collective-permute-start.4 = (bf16[136,1024]{1,0:T(8,128)(2,1)S(1)}, bf16[136,1024]{1,0:T(8,128)(2,1)S(1)}, u32[]{:S(2)}, u32[]{:S(2)}) collective-permute-start(bf16[136,1024]{1,0:T(8,128)(2,1)S(1)} %collective-permute-done), channel_id=1, source_target_pairs={{8,0},{10,2},{12,4},{14,6},{16,8},{18,10},{20,12},{22,14},{9,1},{1... | collective-permute-start | bytes 835592 | tf_op jit(solution)/shard_map/ppermute | solution.py:77
  124.1 9.9 %collective-permute-start.2 = (bf16[136,1024]{1,0:T(8,128)(2,1)S(1)}, bf16[136,1024]{1,0:T(8,128)(2,1)S(1)}, u32[]{:S(2)}, u32[]{:S(2)}) collective-permute-start(bf16[136,1024]{1,0:T(8,128)(2,1)S(1)} %collective-permute-done.1), channel_id=1, source_target_pairs={{8,16},{10,18},{12,20},{14,22},{16,24},{18,26},{20,28},{22,30},{9,... | collective-permute-start | bytes 835592 | tf_op jit(solution)/shard_map/ppermute | solution.py:77
  131.8 6.8 %collective-permute-start.5 = (bf16[136,1024]{1,0:T(8,128)(2,1)S(1)}, bf16[136,1024]{1,0:T(8,128)(2,1)S(1)}, u32[]{:S(2)}, u32[]{:S(2)}) collective-permute-start(bf16[136,1024]{1,0:T(8,128)(2,1)S(1)} %collective-permute-done.4), channel_id=1, source_target_pairs={{8,0},{10,2},{12,4},{14,6},{9,1},{11,3},{13,5},{15,7}} | collective-permute-start | bytes 835592 | tf_op jit(solution)/shard_map/ppermute | solution.py:77
  134.0 4.6 %collective-permute-start.3 = (bf16[136,1024]{1,0:T(8,128)(2,1)S(1)}, bf16[136,1024]{1,0:T(8,128)(2,1)S(1)}, u32[]{:S(2)}, u32[]{:S(2)}) collective-permute-start(bf16[136,1024]{1,0:T(8,128)(2,1)S(1)} %collective-permute-done.2), channel_id=1, source_target_pairs={{16,24},{18,26},{20,28},{22,30},{17,25},{19,27},{21,29},{23,31}} | collective-permute-start | bytes 835592 | tf_op jit(solution)/shard_map/ppermute | solution.py:77
  139.9 15.8 %collective-permute-start.8 = (bf16[256,1024]{1,0:T(8,128)(2,1)S(1)}, bf16[256,1024]{1,0:T(8,128)(2,1)S(1)}, u32[]{:S(2)}, u32[]{:S(2)}) collective-permute-start(bf16[256,1024]{1,0:T(8,128)(2,1)S(1)} %bitcast.95), channel_id=1, source_target_pairs={{0,6},{2,4},{4,2},{6,0},{8,14},{10,12},{12,10},{14,8},{16,22},{18,... | collective-permute-start | bytes 1572872 | tf_op jit(solution)/shard_map/ppermute | solution.py:112
  140.3 22.8 %collective-permute-start.7 = (bf16[256,1024]{1,0:T(8,128)(2,1)S(1)}, bf16[256,1024]{1,0:T(8,128)(2,1)S(1)}, u32[]{:S(2)}, u32[]{:S(2)}) collective-permute-start(bf16[256,1024]{1,0:T(8,128)(2,1)S(1)} %bitcast.94), channel_id=1, source_target_pairs={{0,4},{2,6},{4,0},{6,2},{8,12},{10,14},{12,8},{14,10},{16,20},{18,... | collective-permute-start | bytes 1572872 | tf_op jit(solution)/shard_map/ppermute | solution.py:112
  142.4 20.7 %collective-permute-start.6 = (bf16[256,1024]{1,0:T(8,128)(2,1)S(1)}, bf16[256,1024]{1,0:T(8,128)(2,1)S(1)}, u32[]{:S(2)}, u32[]{:S(2)}) collective-permute-start(bf16[256,1024]{1,0:T(8,128)(2,1)S(1)} %bitcast.93), channel_id=1, source_target_pairs={{0,2},{2,0},{4,6},{6,4},{8,10},{10,8},{12,14},{14,12},{16,18},{18,... | collective-permute-start | bytes 1572872 | tf_op jit(solution)/shard_map/ppermute | solution.py:112
  163.1 1.5 copy-start.5
  163.1 1.6 copy-start.7
  163.1 3.3 %copy-start.3 = (f32[16,64,1024]{2,1,0:T(8,128)S(1)}, f32[16,64,1024]{2,1,0:T(8,128)}, u32[]{:S(2)}) copy-start(f32[16,64,1024]{2,1,0:T(8,128)} %param.11) | copy-start | bytes 12582916
  164.8 15.3 %collective-permute-start.9 = (bf16[1024,1024]{1,0:T(8,128)(2,1)}, bf16[1024,1024]{1,0:T(8,128)(2,1)}, u32[]{:S(2)}, u32[]{:S(2)}) collective-permute-start(bf16[1024,1024]{1,0:T(8,128)(2,1)} %pad_maximum_fusion), channel_id=1, source_target_pairs={{0,1},{1,0},{2,3},{3,2},{4,5},{5,4},{6,7},{7,6},{8,9},{9,8},{10,11... | collective-permute-start | bytes 6291464 | tf_op jit(solution)/shard_map/ppermute | solution.py:31
  168.1 57.1 %all-to-all-start.2 = ((bf16[16,64,1024]{2,1,0:T(8,128)(2,1)}), bf16[16,64,1024]{2,1,0:T(8,128)(2,1)S(1)}, u32[]{:S(2)}, u32[]{:S(2)}) async-start(bf16[16,64,1024]{2,1,0:T(8,128)(2,1)} %convert_element_type.119), calls=%async_computation.2 | async-start | bytes 4194304 | tf_op jit(solution)/shard_map/all_to_all | solution.py:59
  180.0 3.3 %copy-start.1 = (bf16[16,128,512]{2,1,0:T(8,128)(2,1)S(1)}, bf16[16,128,512]{2,1,0:T(8,128)(2,1)}, u32[]{:S(2)}) copy-start(bf16[16,128,512]{2,1,0:T(8,128)(2,1)} %copy-done) | copy-start | bytes 6291460
  183.3 2.9 %copy-start.6 = (bf16[256,1024]{1,0:T(8,128)(2,1)S(1)}, bf16[256,1024]{1,0:T(8,128)(2,1)}, u32[]{:S(2)}) copy-start(bf16[256,1024]{1,0:T(8,128)(2,1)} %copy-done.5) | copy-start | bytes 1572868
  183.3 2.9 %copy-start.8 = (bf16[256,1024]{1,0:T(8,128)(2,1)S(1)}, bf16[256,1024]{1,0:T(8,128)(2,1)}, u32[]{:S(2)}) copy-start(bf16[256,1024]{1,0:T(8,128)(2,1)} %copy-done.7) | copy-start | bytes 1572868
  191.1 36.6 %collective-permute-start.10 = (bf16[1024,512]{1,0:T(8,128)(2,1)}, bf16[1024,512]{1,0:T(8,128)(2,1)S(1)}, u32[]{:S(2)}, u32[]{:S(2)}) collective-permute-start(bf16[1024,512]{1,0:T(8,128)(2,1)} %multiply_convert_fusion.2), channel_id=1, source_target_pairs={{0,1},{1,0},{2,3},{3,2},{4,5},{5,4},{6,7},{7,6},{8,9},{9,8},{10,11... | collective-permute-start | bytes 3145736 | tf_op jit(solution)/shard_map/ppermute | solution.py:31
  229.2 15.8 %collective-permute-start.13 = (bf16[256,1024]{1,0:T(8,128)(2,1)S(1)}, bf16[256,1024]{1,0:T(8,128)(2,1)S(1)}, u32[]{:S(2)}, u32[]{:S(2)}) collective-permute-start(bf16[256,1024]{1,0:T(8,128)(2,1)S(1)} %get-tuple-element.11), channel_id=1, source_target_pairs={{0,6},{2,4},{4,2},{6,0},{8,14},{10,12},{12,10},{14,8},{16,22},{18,... | collective-permute-start | bytes 1572872 | tf_op jit(solution)/shard_map/ppermute | solution.py:112
  229.5 24.5 %collective-permute-start.12 = (bf16[256,1024]{1,0:T(8,128)(2,1)S(1)}, bf16[256,1024]{1,0:T(8,128)(2,1)S(1)}, u32[]{:S(2)}, u32[]{:S(2)}) collective-permute-start(bf16[256,1024]{1,0:T(8,128)(2,1)S(1)} %get-tuple-element.12), channel_id=1, source_target_pairs={{0,4},{2,6},{4,0},{6,2},{8,12},{10,14},{12,8},{14,10},{16,20},{18,... | collective-permute-start | bytes 1572872 | tf_op jit(solution)/shard_map/ppermute | solution.py:112
  231.9 22.2 %collective-permute-start.11 = (bf16[256,1024]{1,0:T(8,128)(2,1)S(1)}, bf16[256,1024]{1,0:T(8,128)(2,1)S(1)}, u32[]{:S(2)}, u32[]{:S(2)}) collective-permute-start(bf16[256,1024]{1,0:T(8,128)(2,1)S(1)} %get-tuple-element.13), channel_id=1, source_target_pairs={{0,2},{2,0},{4,6},{6,4},{8,10},{10,8},{12,14},{14,12},{16,18},{18,... | collective-permute-start | bytes 1572872 | tf_op jit(solution)/shard_map/ppermute | solution.py:112
  255.4 9.8 %collective-permute-start.14 = (bf16[128,1024]{1,0:T(8,128)(2,1)S(1)}, bf16[128,1024]{1,0:T(8,128)(2,1)S(1)}, u32[]{:S(2)}, u32[]{:S(2)}) collective-permute-start(bf16[128,1024]{1,0:T(8,128)(2,1)S(1)} %get-tuple-element.8), channel_id=1, source_target_pairs={{0,8},{2,10},{4,12},{6,14},{1,9},{3,11},{5,13},{7,15}} | collective-permute-start | bytes 786440 | tf_op jit(solution)/shard_map/ppermute | solution.py:139
  256.7 8.5 %collective-permute-start.17 = (bf16[128,1024]{1,0:T(8,128)(2,1)S(1)}, bf16[128,1024]{1,0:T(8,128)(2,1)S(1)}, u32[]{:S(2)}, u32[]{:S(2)}) collective-permute-start(bf16[128,1024]{1,0:T(8,128)(2,1)S(1)} %get-tuple-element.9), channel_id=1, source_target_pairs={{24,16},{26,18},{28,20},{30,22},{25,17},{27,19},{29,21},{31,23}} | collective-permute-start | bytes 786440 | tf_op jit(solution)/shard_map/ppermute | solution.py:139
  265.4 22.6 %copy-start.2 = (bf16[16,128,512]{2,1,0:T(8,128)(2,1)S(1)}, bf16[16,128,512]{2,1,0:T(8,128)(2,1)}, u32[]{:S(2)}) copy-start(bf16[16,128,512]{2,1,0:T(8,128)(2,1)} %copy-done) | copy-start | bytes 6291460
  265.4 9.1 %collective-permute-start.15 = (bf16[128,1024]{1,0:T(8,128)(2,1)S(1)}, bf16[128,1024]{1,0:T(8,128)(2,1)S(1)}, u32[]{:S(2)}, u32[]{:S(2)}) collective-permute-start(bf16[128,1024]{1,0:T(8,128)(2,1)S(1)} %get-tuple-element.6), channel_id=1, source_target_pairs={{0,8},{2,10},{4,12},{6,14},{8,16},{10,18},{12,20},{14,22},{1,9},{3... | collective-permute-start | bytes 786440 | tf_op jit(solution)/shard_map/ppermute | solution.py:139
  268.1 8.8 %collective-permute-start.18 = (bf16[128,1024]{1,0:T(8,128)(2,1)S(1)}, bf16[128,1024]{1,0:T(8,128)(2,1)S(1)}, u32[]{:S(2)}, u32[]{:S(2)}) collective-permute-start(bf16[128,1024]{1,0:T(8,128)(2,1)S(1)} %get-tuple-element.7), channel_id=1, source_target_pairs={{16,8},{18,10},{20,12},{22,14},{24,16},{26,18},{28,20},{30,22},{17... | collective-permute-start | bytes 786440 | tf_op jit(solution)/shard_map/ppermute | solution.py:139
  277.0 8.3 %collective-permute-start.19 = (bf16[128,1024]{1,0:T(8,128)(2,1)S(1)}, bf16[128,1024]{1,0:T(8,128)(2,1)S(1)}, u32[]{:S(2)}, u32[]{:S(2)}) collective-permute-start(bf16[128,1024]{1,0:T(8,128)(2,1)S(1)} %get-tuple-element.5), channel_id=1, source_target_pairs={{8,0},{10,2},{12,4},{14,6},{16,8},{18,10},{20,12},{22,14},{24,16},... | collective-permute-start | bytes 786440 | tf_op jit(solution)/shard_map/ppermute | solution.py:139
  278.9 8.3 %collective-permute-start.16 = (bf16[128,1024]{1,0:T(8,128)(2,1)S(1)}, bf16[128,1024]{1,0:T(8,128)(2,1)S(1)}, u32[]{:S(2)}, u32[]{:S(2)}) collective-permute-start(bf16[128,1024]{1,0:T(8,128)(2,1)S(1)} %get-tuple-element.4), channel_id=1, source_target_pairs={{0,8},{2,10},{4,12},{6,14},{8,16},{10,18},{12,20},{14,22},{16,24},... | collective-permute-start | bytes 786440 | tf_op jit(solution)/shard_map/ppermute | solution.py:139

commit v2 on v1

v2 whole, which is shorter than its diff:
```python
import math

import jax
import jax.numpy as jnp
from jax import lax
from jax.sharding import PartitionSpec as P


epsilon = 1e-05
bf16 = jnp.bfloat16
f32 = jnp.float32


def activate(gate_pre, up_pre):
    gated = jnp.minimum(gate_pre, 7.0)
    upper = jnp.clip(up_pre, -7.0, 7.0)
    return (upper + 1.0) * gated * jax.nn.sigmoid(1.702 * gated)


def parts_of(weights):
    first = lax.reduce_precision(weights, 8, 7)
    rest = weights - first
    second = lax.reduce_precision(rest, 8, 7)
    return [p.astype(bf16) for p in (first, second, rest - second)]


def layout_of(count):
    inner = math.gcd(count, 4)
    return inner, count // inner


def chunks_of(width):
    last = width // 4 if width % 512 == 0 else width // 2
    return [(0, width - last), (width - last, last)]


def far_first(depth):
    return [q for q in range(1, depth) if q != 1] + [1] * (depth > 1)


def over_tp(value):
    size, mine = lax.axis_size("tp"), lax.axis_index("tp")
    blocks = [(mine, value)]
    for j in range(1, size):
        pairs = [(s, (s + j) % size) for s in range(size)]
        blocks.append(((mine - j) % size, lax.ppermute(value, "tp", pairs)))
    return blocks


def product(blocks, matrix):
    total = 0.0
    for owner, value in blocks:
        depth = value.shape[1]
        rows = lax.dynamic_slice_in_dim(matrix, owner * depth, depth, 0)
        total = total + jnp.dot(value, rows, preferred_element_type=f32)
    return total


def take(array, index, axis):
    return lax.dynamic_index_in_dim(array, index, axis, keepdims=False)


def put(array, value, index, axis):
    return lax.dynamic_update_index_in_dim(array, value, index, axis)


def shards(tokens, norm_gain, gate_weight, up_weight, down_weight, routes, route_weights):
    count, tp = lax.axis_size("fs"), lax.axis_size("tp")
    inner, depth = layout_of(count)
    me = lax.axis_index("fs")
    level, place = me // inner, me % inner
    rows, width = tokens.shape
    top = routes.shape[1]
    experts = gate_weight.shape[0]
    capacity = 2 * rows * top // experts
    chunks = chunks_of(width)

    def plane(value, r):
        return lax.ppermute(value, "fs", [(s, s ^ r) for s in range(count)])

    def line(value, q):
        return lax.ppermute(value, "fs", [(s, s ^ (q * inner)) for s in range(count)])

    notes = jnp.concatenate([routes.T.astype(bf16)] + parts_of(route_weights.T), axis=0)
    notes = jnp.concatenate([notes[: 2 * top], notes[2 * top :]], axis=1)
    notes = jnp.pad(notes, ((0, 0), (0, width - 2 * rows)))
    payload = jnp.concatenate([tokens, notes], axis=0)

    def shift(value, step, first):
        pairs = []
        for s in range(count):
            at = s // inner
            if 0 <= at + step < depth and (at >= first if step > 0 else at < depth - first):
                pairs.append((s, s + step * inner))
        return lax.ppermute(value, "fs", pairs)

    ups, downs = [payload], [payload]
    for n in range(1, depth):
        ups.append(shift(ups[-1], 1, n - 1))
        downs.append(shift(downs[-1], -1, n - 1))
    column = [payload]
    for q in range(1, depth):
        column.append(jnp.where(level + q < depth, downs[q], ups[depth - q]))
    column = jnp.stack(column)

    def blocks_of(weight, gain):
        shaped = weight.reshape((depth, inner) + weight.shape[1:])

        def block(index, axis):
            part = take(shaped, index, axis)
            return (part * gain[None, :, None] if gain is not None else part).astype(bf16)

        return block

    def line_then_plane(block):
        stage = jnp.zeros((depth, inner) + block(0, 0).shape[1:], bf16)
        stage = put(stage, block(level, 0), level, 0)
        for q in far_first(depth):
            stage = put(stage, line(block(level ^ q, 0), q), level ^ q, 0)
        out = put(stage, take(stage, place, 1), place, 1)
        for r in range(1, inner):
            got = plane(take(stage, place ^ r, 1), r)
            out = put(out, got, place ^ r, 1)
        return out

    def plane_stage(block):
        stage = jnp.zeros((inner, depth) + block(0, 0).shape[1:], bf16)
        stage = put(stage, block(place, 1), place, 0)
        for r in range(1, inner):
            stage = put(stage, plane(block(place ^ r, 1), r), place ^ r, 0)
        return stage

    def line_stage(stage):
        out = jnp.zeros((depth, inner) + stage.shape[2:], bf16)
        out = put(out, take(stage, level, 1), level, 0)
        for q in far_first(depth):
            got = line(take(stage, level ^ q, 1), q)
            out = put(out, got, level ^ q, 0)
        return out

    gate_out = line_then_plane(blocks_of(gate_weight, norm_gain))
    gate_ready = gate_out.reshape(-1, gate_weight.shape[2])
    up_out = line_stage(plane_stage(blocks_of(up_weight, norm_gain)))
    up_ready = up_out.reshape(-1, up_weight.shape[2])
    down_stage = plane_stage(blocks_of(down_weight, None))
    down_parts = []
    for start, size in chunks:
        part = line_stage(down_stage[..., start : start + size])
        down_parts.append(part.reshape(-1, size))
    down_ready = jnp.concatenate(down_parts, axis=1)

    column_tokens = column[:, :rows]
    column_notes = column[:, rows:, : 2 * rows].astype(f32)
    column_routes = column_notes[:, :top, :rows]
    column_weights = (
        column_notes[:, top:, :rows] + column_notes[:, :top, rows:] + column_notes[:, top:, rows:]
    )
    targets = level * inner + jnp.bitwise_xor(place, jnp.arange(inner, dtype=jnp.int32))
    named = column_routes[:, None] == targets.astype(f32)[None, :, None, None]
    member = jnp.any(named, axis=2)
    share = jnp.sum(jnp.where(named, column_weights[:, None], 0.0), axis=2)
    before = (jnp.arange(rows)[:, None] < jnp.arange(rows)[None, :]).astype(bf16)
    position = jnp.einsum("qrs,st->qrt", member.astype(bf16), before, preferred_element_type=f32)
    slots = jnp.arange(capacity, dtype=jnp.int32).astype(f32)
    chosen = member[:, :, None, :] & (position[:, :, None, :] == slots[None, None, :, None])
    picked = jnp.einsum(
        "qrct,qtd->rqcd", chosen.astype(bf16), column_tokens, preferred_element_type=f32
    ).astype(bf16)
    picked = picked.reshape(inner, depth * capacity, width)

    arrived = [picked[0]] + [plane(picked[r], r) for r in range(1, inner)]
    arrived = over_tp(jnp.concatenate(arrived, axis=0))
    squared = sum(jnp.sum(jnp.square(x.astype(f32)), axis=1, keepdims=True) for _, x in arrived)
    factor = lax.rsqrt(squared / (width * tp) + epsilon)
    normed = [(owner, (x.astype(f32) * factor).astype(bf16)) for owner, x in arrived]
    hidden = activate(product(normed, gate_ready), product(normed, up_ready)).astype(bf16)
    hidden = over_tp(hidden)

    scale = jnp.where(chosen, share[:, :, None, :], 0.0)
    partials = []
    for c, (start, size) in enumerate(chunks):
        results = product(hidden, down_parts[c]).astype(bf16)
        results = results.reshape(inner, depth * capacity, size)
        back = [results[0]] + [plane(results[r], r) for r in range(1, inner)]
        back = jnp.stack(back).reshape(inner, depth, capacity, size)
        partials.append(
            jnp.einsum(
                "qrct,rqcd->qtd",
                scale,
                back.astype(f32),
                preferred_element_type=f32,
                precision=lax.Precision.HIGHEST,
            )
        )
    mixed = []
    for partial in partials:
        upward, downward = 0.0, 0.0
        for n in range(1, depth):
            reach = depth - n
            lift = [(s, s + inner) for s in range(count) if s // inner + reach < depth]
            drop = [(s, s - inner) for s in range(count) if s // inner >= reach]
            upward = lax.ppermute((partial[reach] + upward).astype(bf16), "fs", lift)
            downward = lax.ppermute((partial[n] + downward).astype(bf16), "fs", drop)
            upward, downward = upward.astype(f32), downward.astype(f32)
        mixed.append((partial[0] + upward + downward).astype(bf16))
    mixed = jnp.concatenate(mixed, axis=1)
    return (mixed, gate_ready[None], up_ready[None], down_ready[None])


def solution(mesh):
    placed = (
        P("fs", "tp"),
        P("fs"),
        P(None, "fs", "tp"),
        P(None, "fs", "tp"),
        P(None, "fs", "tp"),
        P("fs", None),
        P("fs", None),
    )

    def program(*arrays):
        return jax.shard_map(
            shards,
            mesh=mesh,
            in_specs=placed,
            out_specs=(P("fs", "tp"), P("fs", None, "tp"), P("fs", None, "tp"), P("fs", None, "tp")),
            check_vma=False,
        )(*arrays)

    return program
```

time: 295 us -> 316 us (1.071)
  starting transfers between devices: 54.8 us -> 77.1 us
  waiting for transfers between devices: 195 us -> 183 us
  local copies, waits for them, and re-layouts: 9.27 us -> 19.4 us
  matrix products: 19.8 us -> 13.8 us
  other arithmetic: 11.7 us -> 17.7 us
    ppermute x12 -> x42, waiting for transfers between devices: 60.5 us -> 183 us  [the longest x12 98.8 us: line(): return lax.ppermute(value, 'fs', [(s, s ^ q * inner) for s in range(count)])]
    all_to_all x3 -> x0, waiting for transfers between devices: 79.5 us -> none  [shards(): lax.all_to_all(sent, 'fs', split_axis=0, concat_axis=1, tiled=True)]
    ppermute x6, waiting for transfers between devices: 54.6 us -> 0.02 us  [shift(): return lax.ppermute(value, 'fs', pairs)]
    ppermute x12 -> x42, starting transfers between devices: 18.9 us -> 63.3 us  [the longest x18 23.3 us: plane(): return lax.ppermute(value, 'fs', [(s, s ^ r) for s in range(count)])]
    all_to_all x3 -> x0, starting transfers between devices: 21.3 us -> none  [shards(): lax.all_to_all(sent, 'fs', split_axis=0, concat_axis=1, tiled=True)]
    dynamic_update_slice x0 -> x25, local copies, waits for them, and re-layouts: none -> 10.5 us  [put(): return lax.dynamic_update_index_in_dim(array, value, index, axis)]
    unnamed x25 -> x12, local copies, waits for them, and re-layouts: 8.86 us -> 0.03 us
    dot_general x6 -> x8, matrix products: 17.5 us -> 11.2 us  [product(): total = total + jnp.dot(value, rows, preferred_element_type=f32)]
  transfers between devices with their start and end apart: 23 -> 50, of which waited for: 14 -> 17; matrix products, arithmetic and copies ran while one was open for 7% -> 15% of each run, Pallas kernels for 0% -> 0%
where the time goes in v2:
time: 316 us; the launch traced here: 313 us
  waiting for transfers between devices  183 us (58%)
  starting transfers between devices  77.1 us (24%)
  local copies, waits for them, and re-layouts  19.4 us (6%)
  other arithmetic  17.7 us (6%)
  matrix products  13.8 us (4%)
    ppermute x12, waiting for transfers between devices, line(): return lax.ppermute(value, 'fs', [(s, s ^ q * inner) for s in range(count)])  98.8 us
    ppermute x18, waiting for transfers between devices, plane(): return lax.ppermute(value, 'fs', [(s, s ^ r) for s in range(count)])  79.4 us
    ppermute x18, starting transfers between devices, plane(): return lax.ppermute(value, 'fs', [(s, s ^ r) for s in range(count)])  23.3 us
    ppermute x6, starting transfers between devices, shards(): upward = lax.ppermute((partial[reach] + upward).astype(bf16), 'fs', lift)  20 us
    ppermute x6, starting transfers between devices, shift(): return lax.ppermute(value, 'fs', pairs)  13.7 us
    ppermute x12, starting transfers between devices, line(): return lax.ppermute(value, 'fs', [(s, s ^ q * inner) for s in range(count)])  12.3 us
    dot_general x8, matrix products, product(): total = total + jnp.dot(value, rows, preferred_element_type=f32)  11.2 us
    dynamic_update_slice x25, local copies, waits for them, and re-layouts, put(): return lax.dynamic_update_index_in_dim(array, value, index, axis)  10.5 us
  transfers between devices with their start and end apart: 50, of which 17 were waited for; matrix products, arithmetic and copies ran while one was open for 15% of the time, Pallas kernels for 0%

profile of v2, /device:TPU:12, one launch (start us, length us, event | category | flops | bytes accessed | tf_op | source)
XLA Modules:
  0.0 312.8 jit_solution(6535936915109461710)
XLA Ops:
  2.0 1.7 fusion.107
  3.8 2.3 collective-permute-start
  6.1 3.5 %collective-permute-start.1 = (bf16[136,1024]{1,0:T(8,128)(2,1)}, bf16[136,1024]{1,0:T(8,128)(2,1)}, u32[]{:S(2)}, u32[]{:S(2)}) collective-permute-start(bf16[136,1024]{1,0:T(8,128)(2,1)} %get-tuple-element.53), channel_id=1, source_target_pairs={{0,8},{2,10},{4,12},{6,14},{8,16},{10,18},{12,20},{14,22},{16,24},... | collective-permute-start | bytes 835592 | tf_op jit(solution)/shard_map/ppermute | solution.py:95
  9.7 4.9 %fusion.22 = (bf16[4,128,512]{2,1,0:T(8,128)(2,1)S(1)}, bf16[4,128,512]{2,1,0:T(8,128)(2,1)}, bf16[4,128,512]{2,1,0:T(8,128)(2,1)}, bf16[4,128,512]{2,1,0:T(8,12...) fusion(f32[4,4,128,512]{3,2,1,0:T(8,128)} %bitcast.257, s32[]{:T(128)S(6)} %select_n.157, ...), kind=kLoop, calls=%fused_computation.37 | loop fusion | flops 3145728 | bytes 9437720 | tf_op jit(solution)/shard_map/convert_element_type | solution.py:111
  14.6 1.1 collective-permute-start.16
  15.7 1.4 collective-permute-start.17
  17.1 1.8 collective-permute-start.18
  18.9 1.5 broadcast.44.clone
  20.5 2.1 fusion.42
  22.8 1.4 fusion.43
  24.5 1.8 fusion.45
  26.3 3.1 fusion.48
  29.4 21.4 %collective-permute-done.16 = bf16[4,128,512]{2,1,0:T(8,128)(2,1)} collective-permute-done((bf16[4,128,512]{2,1,0:T(8,128)(2,1)}, bf16[4,128,512]{2,1,0:T(8,128)(2,1)}, u32[]{:S(2)}, u32[]{:S(2)}) %collective-permute-start.16) | collective-permute-done | bytes 524320 | tf_op jit(solution)/shard_map/ppermute | solution.py:82
  50.8 1.5 collective-permute-start.10
  52.3 1.9 bitcast_dynamic-update-slice_fusion.8
  54.2 8.1 %collective-permute-done.17 = bf16[4,128,512]{2,1,0:T(8,128)(2,1)} collective-permute-done((bf16[4,128,512]{2,1,0:T(8,128)(2,1)}, bf16[4,128,512]{2,1,0:T(8,128)(2,1)}, u32[]{:S(2)}, u32[]{:S(2)}) %collective-permute-start.17) | collective-permute-done | bytes 524320 | tf_op jit(solution)/shard_map/ppermute | solution.py:82
  62.8 1.9 bitcast_dynamic-update-slice_fusion.7
  64.7 2.5 collective-permute-start.12
  67.1 1.9 bitcast_dynamic-update-slice_fusion.6
  69.6 17.7 %collective-permute-done.11 = bf16[4,128,512]{2,1,0:T(8,128)(2,1)S(1)} collective-permute-done((bf16[4,128,512]{2,1,0:T(8,128)(2,1)}, bf16[4,128,512]{2,1,0:T(8,128)(2,1)S(1)}, u32[]{:S(2)}, u32[]{:S(2)}) %collective-permute-start.11) | collective-permute-done | bytes 524320 | tf_op jit(solution)/shard_map/ppermute | solution.py:79
  87.8 2.6 collective-permute-start.24
  90.3 1.9 collective-permute-start.4
  92.3 3.9 %collective-permute-start.2 = (bf16[136,1024]{1,0:T(8,128)(2,1)}, bf16[136,1024]{1,0:T(8,128)(2,1)S(1)}, u32[]{:S(2)}, u32[]{:S(2)}) collective-permute-start(bf16[136,1024]{1,0:T(8,128)(2,1)} %collective-permute-done.1), channel_id=1, source_target_pairs={{8,16},{10,18},{12,20},{14,22},{16,24},{18,26},{20,28},{22,30},{9,... | collective-permute-start | bytes 835592 | tf_op jit(solution)/shard_map/ppermute | solution.py:95
  96.3 14.8 %collective-permute-done.23 = bf16[4,64,1024]{2,1,0:T(8,128)(2,1)S(1)} collective-permute-done((bf16[4,64,1024]{2,1,0:T(8,128)(2,1)S(1)}, bf16[4,64,1024]{2,1,0:T(8,128)(2,1)S(1)}, u32[]{:S(2)}, u32[]{:S(2)}) %collective-permute-start.23) | collective-permute-done | bytes 524320 | tf_op jit(solution)/shard_map/ppermute | solution.py:79
  111.2 1.3 collective-permute-start.5
  112.5 2.5 dynamic-slice_bitcast_fusion
  115.3 1.6 collective-permute-start.19
  121.4 1.6 collective-permute-start.8
  123.8 1.1 collective-permute-start.6
  125.5 15.9 %collective-permute-done.8 = bf16[256,1024]{1,0:T(8,128)(2,1)S(1)} collective-permute-done((bf16[256,1024]{1,0:T(8,128)(2,1)S(1)}, bf16[256,1024]{1,0:T(8,128)(2,1)S(1)}, u32[]{:S(2)}, u32[]{:S(2)}) %collective-permute-start.8) | collective-permute-done | bytes 524320 | tf_op jit(solution)/shard_map/ppermute | solution.py:79
  141.4 2.5 collective-permute-start.21
  143.9 18.9 %collective-permute-done.7 = bf16[256,1024]{1,0:T(8,128)(2,1)S(1)} collective-permute-done((bf16[256,1024]{1,0:T(8,128)(2,1)S(1)}, bf16[256,1024]{1,0:T(8,128)(2,1)S(1)}, u32[]{:S(2)}, u32[]{:S(2)}) %collective-permute-start.7) | collective-permute-done | bytes 524320 | tf_op jit(solution)/shard_map/ppermute | solution.py:79
  164.0 5.3 %collective-permute-done.38 = bf16[4,64,256]{2,1,0:T(8,128)(2,1)S(1)} collective-permute-done((bf16[4,64,256]{2,1,0:T(8,128)(2,1)S(1)}, bf16[4,64,256]{2,1,0:T(8,128)(2,1)S(1)}, u32[]{:S(2)}, u32[]{:S(2)}) %collective-permute-start.38) | collective-permute-done | bytes 131104 | tf_op jit(solution)/shard_map/ppermute | solution.py:82
  169.3 5.7 %collective-permute-done.39 = bf16[4,64,256]{2,1,0:T(8,128)(2,1)S(1)} collective-permute-done((bf16[4,64,256]{2,1,0:T(8,128)(2,1)S(1)}, bf16[4,64,256]{2,1,0:T(8,128)(2,1)S(1)}, u32[]{:S(2)}, u32[]{:S(2)}) %collective-permute-start.39) | collective-permute-done | bytes 131104 | tf_op jit(solution)/shard_map/ppermute | solution.py:82
  176.8 3.5 %collective-permute-start.15 = (bf16[4,128,512]{2,1,0:T(8,128)(2,1)S(1)}, bf16[4,128,512]{2,1,0:T(8,128)(2,1)S(1)}, u32[]{:S(2)}, u32[]{:S(2)}) collective-permute-start(bf16[4,128,512]{2,1,0:T(8,128)(2,1)S(1)} %get-tuple-element.15), channel_id=1, source_target_pairs={{0,8},{2,10},{4,12},{6,14},{8,0},{10,2},{12,4},{14,6},{16,24},{18,... | collective-permute-start | bytes 1572872 | tf_op jit(solution)/shard_map/ppermute | solution.py:82
  182.0 25.3 %collective-permute-done.13 = bf16[4,128,512]{2,1,0:T(8,128)(2,1)S(1)} collective-permute-done((bf16[4,128,512]{2,1,0:T(8,128)(2,1)S(1)}, bf16[4,128,512]{2,1,0:T(8,128)(2,1)S(1)}, u32[]{:S(2)}, u32[]{:S(2)}) %collective-permute-start.13) | collective-permute-done | bytes 524320 | tf_op jit(solution)/shard_map/ppermute | solution.py:82
  207.3 3.4 %collective-permute-start.25 = (bf16[4,64,768]{2,1,0:T(8,128)(2,1)S(1)}, bf16[4,64,768]{2,1,0:T(8,128)(2,1)S(1)}, u32[]{:S(2)}, u32[]{:S(2)}) collective-permute-start(bf16[4,64,768]{2,1,0:T(8,128)(2,1)S(1)} %get-tuple-element.38), channel_id=1, source_target_pairs={{0,16},{2,18},{4,20},{6,22},{8,24},{10,26},{12,28},{14,30},{16,0},... | collective-permute-start | bytes 1179656 | tf_op jit(solution)/shard_map/ppermute | solution.py:82
  210.7 27.3 %collective-permute-done.14 = bf16[4,128,512]{2,1,0:T(8,128)(2,1)S(1)} collective-permute-done((bf16[4,128,512]{2,1,0:T(8,128)(2,1)S(1)}, bf16[4,128,512]{2,1,0:T(8,128)(2,1)S(1)}, u32[]{:S(2)}, u32[]{:S(2)}) %collective-permute-start.14) | collective-permute-done | bytes 524320 | tf_op jit(solution)/shard_map/ppermute | solution.py:82
  238.7 1.3 fusion.31
  240.0 1.3 fusion.29
  241.3 2.5 fusion.26
  243.9 3.2 %multiply_convert_fusion = bf16[1024,512]{1,0:T(8,128)(2,1)S(1)} fusion(f32[1024,512]{1,0:T(8,128)S(1)} %fusion.26, f32[1024,512]{1,0:T(8,128)S(1)} %fusion.31, f32[1024,512]{1,0:T(8,128)S(1)} %fusion.29, bf16[2048,512]{1,0:T(8,128)(2,1)} %bitcast.43, s32[]{:T(128)S(6)} %select_n.162, bf16[1024,1024]{1,0:T(8,128)(2,1)S(1)} %get-tuple-element.5, ...), kind=kOutput, calls=%fused_computation.11 | convolution fusion | flops 1083179008 | bytes 10489860 | tf_op jit(solution)/shard_map/dot_general | solution.py:55
  247.3 5.7 %collective-permute-done.26 = bf16[4,64,768]{2,1,0:T(8,128)(2,1)S(1)} collective-permute-done((bf16[4,64,768]{2,1,0:T(8,128)(2,1)S(1)}, bf16[4,64,768]{2,1,0:T(8,128)(2,1)S(1)}, u32[]{:S(2)}, u32[]{:S(2)}) %collective-permute-start.26) | collective-permute-done | bytes 393248 | tf_op jit(solution)/shard_map/ppermute | solution.py:82
  253.1 1.6 maximum_bitcast_fusion
  255.7 1.9 collective-permute-start.42
  257.6 1.6 collective-permute-start.41
  261.4 1.8 collective-permute-start.30
  263.2 1.6 collective-permute-start.29
  264.8 3.7 %collective-permute-done.42 = bf16[256,256]{1,0:T(8,128)(2,1)S(1)} collective-permute-done((bf16[256,256]{1,0:T(8,128)(2,1)S(1)}, bf16[256,256]{1,0:T(8,128)(2,1)S(1)}, u32[]{:S(2)}, u32[]{:S(2)}) %collective-permute-start.42) | collective-permute-done | bytes 131104 | tf_op jit(solution)/shard_map/ppermute | solution.py:79
  269.3 1.3 collective-permute-start.44
  271.3 3.0 collective-permute-done.31
  274.2 5.5 %collective-permute-done.30 = bf16[256,768]{1,0:T(8,128)(2,1)S(1)} collective-permute-done((bf16[256,768]{1,0:T(8,128)(2,1)S(1)}, bf16[256,768]{1,0:T(8,128)(2,1)S(1)}, u32[]{:S(2)}, u32[]{:S(2)}) %collective-permute-start.30) | collective-permute-done | bytes 393248 | tf_op jit(solution)/shard_map/ppermute | solution.py:79
  280.9 1.3 collective-permute-start.32
  282.9 4.2 %collective-permute-start.45 = (bf16[128,256]{1,0:T(8,128)(2,1)S(1)}, bf16[128,256]{1,0:T(8,128)(2,1)S(1)}, u32[]{:S(2)}, u32[]{:S(2)}) collective-permute-start(bf16[128,256]{1,0:T(8,128)(2,1)S(1)} %get-tuple-element.41), channel_id=1, source_target_pairs={{0,8},{2,10},{4,12},{6,14},{8,16},{10,18},{12,20},{14,22},{1,9},{3... | collective-permute-start | bytes 196616 | tf_op jit(solution)/shard_map/ppermute | solution.py:202
  287.1 1.3 collective-permute-start.48
  288.4 1.3 collective-permute-done.32
  289.8 4.7 %collective-permute-start.33 = (bf16[128,768]{1,0:T(8,128)(2,1)S(1)}, bf16[128,768]{1,0:T(8,128)(2,1)S(1)}, u32[]{:S(2)}, u32[]{:S(2)}) collective-permute-start(bf16[128,768]{1,0:T(8,128)(2,1)S(1)} %get-tuple-element.28), channel_id=1, source_target_pairs={{0,8},{2,10},{4,12},{6,14},{8,16},{10,18},{12,20},{14,22},{1,9},{3... | collective-permute-start | bytes 589832 | tf_op jit(solution)/shard_map/ppermute | solution.py:202
  294.5 1.3 collective-permute-start.36
  295.9 1.9 collective-permute-start.49
  297.8 4.6 %collective-permute-start.46 = (bf16[128,256]{1,0:T(8,128)(2,1)S(1)}, bf16[128,256]{1,0:T(8,128)(2,1)S(1)}, u32[]{:S(2)}, u32[]{:S(2)}) collective-permute-start(bf16[128,256]{1,0:T(8,128)(2,1)S(1)} %get-tuple-element.39), channel_id=1, source_target_pairs={{0,8},{2,10},{4,12},{6,14},{8,16},{10,18},{12,20},{14,22},{16,24},... | collective-permute-start | bytes 196616 | tf_op jit(solution)/shard_map/ppermute | solution.py:202
  302.5 1.9 collective-permute-start.37
  304.4 3.9 %collective-permute-start.34 = (bf16[128,768]{1,0:T(8,128)(2,1)S(1)}, bf16[128,768]{1,0:T(8,128)(2,1)S(1)}, u32[]{:S(2)}, u32[]{:S(2)}) collective-permute-start(bf16[128,768]{1,0:T(8,128)(2,1)S(1)} %get-tuple-element.26), channel_id=1, source_target_pairs={{0,8},{2,10},{4,12},{6,14},{8,16},{10,18},{12,20},{14,22},{16,24},... | collective-permute-start | bytes 589832 | tf_op jit(solution)/shard_map/ppermute | solution.py:202
  308.4 1.7 collective-permute-done.37
  310.0 1.9 collective-permute-done.34
  (130 shorter events, 22.7 us)
Async XLA Ops:
  3.8 84.0 %collective-permute-start = (bf16[136,1024]{1,0:T(8,128)(2,1)}, bf16[136,1024]{1,0:T(8,128)(2,1)}, u32[]{:S(2)}, u32[]{:S(2)}) collective-permute-start(bf16[136,1024]{1,0:T(8,128)(2,1)} %get-tuple-element.53), channel_id=1, source_target_pairs={{8,0},{10,2},{12,4},{14,6},{16,8},{18,10},{20,12},{22,14},{24,16},... | collective-permute-start | bytes 835592 | tf_op jit(solution)/shard_map/ppermute | solution.py:95
  6.1 84.2 %collective-permute-start.1 = (bf16[136,1024]{1,0:T(8,128)(2,1)}, bf16[136,1024]{1,0:T(8,128)(2,1)}, u32[]{:S(2)}, u32[]{:S(2)}) collective-permute-start(bf16[136,1024]{1,0:T(8,128)(2,1)} %get-tuple-element.53), channel_id=1, source_target_pairs={{0,8},{2,10},{4,12},{6,14},{8,16},{10,18},{12,20},{14,22},{16,24},... | collective-permute-start | bytes 835592 | tf_op jit(solution)/shard_map/ppermute | solution.py:95
  14.6 5.9 %copy-start.5 = (f32[128]{0:T(128)S(1)}, f32[128]{0:T(128)}, u32[]{:S(2)}) copy-start(f32[128]{0:T(128)} %param.8) | copy-start | bytes 1540
  14.6 36.3 %collective-permute-start.16 = (bf16[4,128,512]{2,1,0:T(8,128)(2,1)}, bf16[4,128,512]{2,1,0:T(8,128)(2,1)}, u32[]{:S(2)}, u32[]{:S(2)}) collective-permute-start(bf16[4,128,512]{2,1,0:T(8,128)(2,1)} %get-tuple-element.59), channel_id=1, source_target_pairs={{0,16},{2,18},{4,20},{6,22},{8,24},{10,26},{12,28},{14,30},{16,0},... | collective-permute-start | bytes 1572872 | tf_op jit(solution)/shard_map/ppermute | solution.py:82
  15.7 46.6 %collective-permute-start.17 = (bf16[4,128,512]{2,1,0:T(8,128)(2,1)}, bf16[4,128,512]{2,1,0:T(8,128)(2,1)}, u32[]{:S(2)}, u32[]{:S(2)}) collective-permute-start(bf16[4,128,512]{2,1,0:T(8,128)(2,1)} %get-tuple-element.60), channel_id=1, source_target_pairs={{0,24},{2,26},{4,28},{6,30},{8,16},{10,18},{12,20},{14,22},{16,8},... | collective-permute-start | bytes 1572872 | tf_op jit(solution)/shard_map/ppermute | solution.py:82
  17.1 47.5 %collective-permute-start.18 = (bf16[4,128,512]{2,1,0:T(8,128)(2,1)}, bf16[4,128,512]{2,1,0:T(8,128)(2,1)}, u32[]{:S(2)}, u32[]{:S(2)}) collective-permute-start(bf16[4,128,512]{2,1,0:T(8,128)(2,1)} %get-tuple-element.61), channel_id=1, source_target_pairs={{0,8},{2,10},{4,12},{6,14},{8,0},{10,2},{12,4},{14,6},{16,24},{18,... | collective-permute-start | bytes 1572872 | tf_op jit(solution)/shard_map/ppermute | solution.py:82
  24.2 2.1 copy-start
  29.4 39.6 %copy-start.4 = (bf16[4,64,1024]{2,1,0:T(8,128)(2,1)S(1)}, bf16[4,64,1024]{2,1,0:T(8,128)(2,1)}, u32[]{:S(2)}) copy-start(bf16[4,64,1024]{2,1,0:T(8,128)(2,1)} %get-tuple-element.14) | copy-start | bytes 1572868
  29.4 40.1 %copy-start.1 = (bf16[4,4,128,512]{3,2,1,0:T(8,128)(2,1)S(1)}, bf16[4,4,128,512]{3,2,1,0:T(8,128)(2,1)}, u32[]{:S(2)}) copy-start(bf16[4,4,128,512]{3,2,1,0:T(8,128)(2,1)} %copy-done) | copy-start | bytes 6291460
  50.8 36.4 %copy-start.3 = (bf16[4,64,1024]{2,1,0:T(8,128)(2,1)S(1)}, bf16[4,64,1024]{2,1,0:T(8,128)(2,1)}, u32[]{:S(2)}) copy-start(bf16[4,64,1024]{2,1,0:T(8,128)(2,1)} %get-tuple-element.13) | copy-start | bytes 1572868
  50.8 18.2 %collective-permute-start.10 = (bf16[4,128,512]{2,1,0:T(8,128)(2,1)}, bf16[4,128,512]{2,1,0:T(8,128)(2,1)S(1)}, u32[]{:S(2)}, u32[]{:S(2)}) collective-permute-start(bf16[4,128,512]{2,1,0:T(8,128)(2,1)} %get-tuple-element.8), channel_id=1, source_target_pairs={{0,2},{2,0},{4,6},{6,4},{8,10},{10,8},{12,14},{14,12},{16,18},{18,... | collective-permute-start | bytes 1572872 | tf_op jit(solution)/shard_map/ppermute | solution.py:79
  62.3 24.9 %collective-permute-start.11 = (bf16[4,128,512]{2,1,0:T(8,128)(2,1)}, bf16[4,128,512]{2,1,0:T(8,128)(2,1)S(1)}, u32[]{:S(2)}, u32[]{:S(2)}) collective-permute-start(bf16[4,128,512]{2,1,0:T(8,128)(2,1)} %get-tuple-element.7), channel_id=1, source_target_pairs={{0,4},{2,6},{4,0},{6,2},{8,12},{10,14},{12,8},{14,10},{16,20},{18,... | collective-permute-start | bytes 1572872 | tf_op jit(solution)/shard_map/ppermute | solution.py:79
  64.7 27.6 %collective-permute-start.12 = (bf16[4,128,512]{2,1,0:T(8,128)(2,1)S(1)}, bf16[4,128,512]{2,1,0:T(8,128)(2,1)S(1)}, u32[]{:S(2)}, u32[]{:S(2)}) collective-permute-start(bf16[4,128,512]{2,1,0:T(8,128)(2,1)S(1)} %get-tuple-element.6), channel_id=1, source_target_pairs={{0,6},{2,4},{4,2},{6,0},{8,14},{10,12},{12,10},{14,8},{16,22},{18,... | collective-permute-start | bytes 1572872 | tf_op jit(solution)/shard_map/ppermute | solution.py:79
  69.0 27.3 %collective-permute-start.22 = (bf16[4,64,1024]{2,1,0:T(8,128)(2,1)S(1)}, bf16[4,64,1024]{2,1,0:T(8,128)(2,1)S(1)}, u32[]{:S(2)}, u32[]{:S(2)}) collective-permute-start(bf16[4,64,1024]{2,1,0:T(8,128)(2,1)S(1)} %copy-done.4), channel_id=1, source_target_pairs={{0,2},{2,0},{4,6},{6,4},{8,10},{10,8},{12,14},{14,12},{16,18},{18,... | collective-permute-start | bytes 1572872 | tf_op jit(solution)/shard_map/ppermute | solution.py:79
  87.2 23.9 %collective-permute-start.23 = (bf16[4,64,1024]{2,1,0:T(8,128)(2,1)S(1)}, bf16[4,64,1024]{2,1,0:T(8,128)(2,1)S(1)}, u32[]{:S(2)}, u32[]{:S(2)}) collective-permute-start(bf16[4,64,1024]{2,1,0:T(8,128)(2,1)S(1)} %copy-done.3), channel_id=1, source_target_pairs={{0,4},{2,6},{4,0},{6,2},{8,12},{10,14},{12,8},{14,10},{16,20},{18,... | collective-permute-start | bytes 1572872 | tf_op jit(solution)/shard_map/ppermute | solution.py:79
  87.8 23.4 %collective-permute-start.24 = (bf16[4,64,1024]{2,1,0:T(8,128)(2,1)S(1)}, bf16[4,64,1024]{2,1,0:T(8,128)(2,1)S(1)}, u32[]{:S(2)}, u32[]{:S(2)}) collective-permute-start(bf16[4,64,1024]{2,1,0:T(8,128)(2,1)S(1)} %get-tuple-element.12), channel_id=1, source_target_pairs={{0,6},{2,4},{4,2},{6,0},{8,14},{10,12},{12,10},{14,8},{16,22},{18,... | collective-permute-start | bytes 1572872 | tf_op jit(solution)/shard_map/ppermute | solution.py:79
  90.3 20.9 %collective-permute-start.4 = (bf16[136,1024]{1,0:T(8,128)(2,1)}, bf16[136,1024]{1,0:T(8,128)(2,1)S(1)}, u32[]{:S(2)}, u32[]{:S(2)}) collective-permute-start(bf16[136,1024]{1,0:T(8,128)(2,1)} %collective-permute-done), channel_id=1, source_target_pairs={{8,0},{10,2},{12,4},{14,6},{16,8},{18,10},{20,12},{22,14},{9,1},{1... | collective-permute-start | bytes 835592 | tf_op jit(solution)/shard_map/ppermute | solution.py:95
  92.3 25.1 %collective-permute-start.2 = (bf16[136,1024]{1,0:T(8,128)(2,1)}, bf16[136,1024]{1,0:T(8,128)(2,1)S(1)}, u32[]{:S(2)}, u32[]{:S(2)}) collective-permute-start(bf16[136,1024]{1,0:T(8,128)(2,1)} %collective-permute-done.1), channel_id=1, source_target_pairs={{8,16},{10,18},{12,20},{14,22},{16,24},{18,26},{20,28},{22,30},{9,... | collective-permute-start | bytes 835592 | tf_op jit(solution)/shard_map/ppermute | solution.py:95
  111.2 6.9 %collective-permute-start.5 = (bf16[136,1024]{1,0:T(8,128)(2,1)S(1)}, bf16[136,1024]{1,0:T(8,128)(2,1)S(1)}, u32[]{:S(2)}, u32[]{:S(2)}) collective-permute-start(bf16[136,1024]{1,0:T(8,128)(2,1)S(1)} %collective-permute-done.4), channel_id=1, source_target_pairs={{8,0},{10,2},{12,4},{14,6},{9,1},{11,3},{13,5},{15,7}} | collective-permute-start | bytes 835592 | tf_op jit(solution)/shard_map/ppermute | solution.py:95
  115.3 60.6 %collective-permute-start.19 = (bf16[4,128,512]{2,1,0:T(8,128)(2,1)S(1)}, bf16[4,128,512]{2,1,0:T(8,128)(2,1)S(1)}, u32[]{:S(2)}, u32[]{:S(2)}) collective-permute-start(bf16[4,128,512]{2,1,0:T(8,128)(2,1)S(1)} %get-tuple-element.24), channel_id=1, source_target_pairs={{0,2},{2,0},{4,6},{6,4},{8,10},{10,8},{12,14},{14,12},{16,18},{18,... | collective-permute-start | bytes 1572872 | tf_op jit(solution)/shard_map/ppermute | solution.py:79
  116.9 59.9 %collective-permute-start.20 = (bf16[4,128,512]{2,1,0:T(8,128)(2,1)S(1)}, bf16[4,128,512]{2,1,0:T(8,128)(2,1)S(1)}, u32[]{:S(2)}, u32[]{:S(2)}) collective-permute-start(bf16[4,128,512]{2,1,0:T(8,128)(2,1)S(1)} %get-tuple-element.23), channel_id=1, source_target_pairs={{0,4},{2,6},{4,0},{6,2},{8,12},{10,14},{12,8},{14,10},{16,20},{18,... | collective-permute-start | bytes 1572872 | tf_op jit(solution)/shard_map/ppermute | solution.py:79
  117.4 1.7 collective-permute-start.3
  121.4 20.0 %collective-permute-start.8 = (bf16[256,1024]{1,0:T(8,128)(2,1)S(1)}, bf16[256,1024]{1,0:T(8,128)(2,1)S(1)}, u32[]{:S(2)}, u32[]{:S(2)}) collective-permute-start(bf16[256,1024]{1,0:T(8,128)(2,1)S(1)} %bitcast.267), channel_id=1, source_target_pairs={{0,6},{2,4},{4,2},{6,0},{8,14},{10,12},{12,10},{14,8},{16,22},{18,... | collective-permute-start | bytes 1572872 | tf_op jit(solution)/shard_map/ppermute | solution.py:79
  122.9 39.9 %collective-permute-start.7 = (bf16[256,1024]{1,0:T(8,128)(2,1)S(1)}, bf16[256,1024]{1,0:T(8,128)(2,1)S(1)}, u32[]{:S(2)}, u32[]{:S(2)}) collective-permute-start(bf16[256,1024]{1,0:T(8,128)(2,1)S(1)} %bitcast.266), channel_id=1, source_target_pairs={{0,4},{2,6},{4,0},{6,2},{8,12},{10,14},{12,8},{14,10},{16,20},{18,... | collective-permute-start | bytes 1572872 | tf_op jit(solution)/shard_map/ppermute | solution.py:79
  123.8 39.0 %collective-permute-start.6 = (bf16[256,1024]{1,0:T(8,128)(2,1)S(1)}, bf16[256,1024]{1,0:T(8,128)(2,1)S(1)}, u32[]{:S(2)}, u32[]{:S(2)}) collective-permute-start(bf16[256,1024]{1,0:T(8,128)(2,1)S(1)} %bitcast.265), channel_id=1, source_target_pairs={{0,2},{2,0},{4,6},{6,4},{8,10},{10,8},{12,14},{14,12},{16,18},{18,... | collective-permute-start | bytes 1572872 | tf_op jit(solution)/shard_map/ppermute | solution.py:79
  141.4 39.8 %collective-permute-start.21 = (bf16[4,128,512]{2,1,0:T(8,128)(2,1)S(1)}, bf16[4,128,512]{2,1,0:T(8,128)(2,1)S(1)}, u32[]{:S(2)}, u32[]{:S(2)}) collective-permute-start(bf16[4,128,512]{2,1,0:T(8,128)(2,1)S(1)} %get-tuple-element.22), channel_id=1, source_target_pairs={{0,6},{2,4},{4,2},{6,0},{8,14},{10,12},{12,10},{14,8},{16,22},{18,... | collective-permute-start | bytes 1572872 | tf_op jit(solution)/shard_map/ppermute | solution.py:79
  162.8 6.5 %collective-permute-start.38 = (bf16[4,64,256]{2,1,0:T(8,128)(2,1)S(1)}, bf16[4,64,256]{2,1,0:T(8,128)(2,1)S(1)}, u32[]{:S(2)}, u32[]{:S(2)}) collective-permute-start(bf16[4,64,256]{2,1,0:T(8,128)(2,1)S(1)} %get-tuple-element.51), channel_id=1, source_target_pairs={{0,16},{2,18},{4,20},{6,22},{8,24},{10,26},{12,28},{14,30},{16,0},... | collective-permute-start | bytes 393224 | tf_op jit(solution)/shard_map/ppermute | solution.py:82
  163.6 74.6 %collective-permute-start.9 = (bf16[1024,1024]{1,0:T(8,128)(2,1)S(1)}, bf16[1024,1024]{1,0:T(8,128)(2,1)S(1)}, u32[]{:S(2)}, u32[]{:S(2)}) collective-permute-start(bf16[1024,1024]{1,0:T(8,128)(2,1)S(1)} %get-tuple-element.5), channel_id=1, source_target_pairs={{0,1},{1,0},{2,3},{3,2},{4,5},{5,4},{6,7},{7,6},{8,9},{9,8},{10,11... | collective-permute-start | bytes 6291464 | tf_op jit(solution)/shard_map/ppermute | solution.py:46
  169.3 5.7 %collective-permute-start.39 = (bf16[4,64,256]{2,1,0:T(8,128)(2,1)S(1)}, bf16[4,64,256]{2,1,0:T(8,128)(2,1)S(1)}, u32[]{:S(2)}, u32[]{:S(2)}) collective-permute-start(bf16[4,64,256]{2,1,0:T(8,128)(2,1)S(1)} %get-tuple-element.50), channel_id=1, source_target_pairs={{0,24},{2,26},{4,28},{6,30},{8,16},{10,18},{12,20},{14,22},{16,8},... | collective-permute-start | bytes 393224 | tf_op jit(solution)/shard_map/ppermute | solution.py:82
  175.0 32.2 %collective-permute-start.13 = (bf16[4,128,512]{2,1,0:T(8,128)(2,1)S(1)}, bf16[4,128,512]{2,1,0:T(8,128)(2,1)S(1)}, u32[]{:S(2)}, u32[]{:S(2)}) collective-permute-start(bf16[4,128,512]{2,1,0:T(8,128)(2,1)S(1)} %get-tuple-element.17), channel_id=1, source_target_pairs={{0,16},{2,18},{4,20},{6,22},{8,24},{10,26},{12,28},{14,30},{16,0},... | collective-permute-start | bytes 1572872 | tf_op jit(solution)/shard_map/ppermute | solution.py:82
  175.9 62.1 %collective-permute-start.14 = (bf16[4,128,512]{2,1,0:T(8,128)(2,1)S(1)}, bf16[4,128,512]{2,1,0:T(8,128)(2,1)S(1)}, u32[]{:S(2)}, u32[]{:S(2)}) collective-permute-start(bf16[4,128,512]{2,1,0:T(8,128)(2,1)S(1)} %get-tuple-element.16), channel_id=1, source_target_pairs={{0,24},{2,26},{4,28},{6,30},{8,16},{10,18},{12,20},{14,22},{16,8},... | collective-permute-start | bytes 1572872 | tf_op jit(solution)/shard_map/ppermute | solution.py:82
  176.8 61.2 %collective-permute-start.15 = (bf16[4,128,512]{2,1,0:T(8,128)(2,1)S(1)}, bf16[4,128,512]{2,1,0:T(8,128)(2,1)S(1)}, u32[]{:S(2)}, u32[]{:S(2)}) collective-permute-start(bf16[4,128,512]{2,1,0:T(8,128)(2,1)S(1)} %get-tuple-element.15), channel_id=1, source_target_pairs={{0,8},{2,10},{4,12},{6,14},{8,0},{10,2},{12,4},{14,6},{16,24},{18,... | collective-permute-start | bytes 1572872 | tf_op jit(solution)/shard_map/ppermute | solution.py:82
  181.2 66.0 %collective-permute-start.40 = (bf16[4,64,256]{2,1,0:T(8,128)(2,1)S(1)}, bf16[4,64,256]{2,1,0:T(8,128)(2,1)S(1)}, u32[]{:S(2)}, u32[]{:S(2)}) collective-permute-start(bf16[4,64,256]{2,1,0:T(8,128)(2,1)S(1)} %get-tuple-element.49), channel_id=1, source_target_pairs={{0,8},{2,10},{4,12},{6,14},{8,0},{10,2},{12,4},{14,6},{16,24},{18,... | collective-permute-start | bytes 393224 | tf_op jit(solution)/shard_map/ppermute | solution.py:82
  207.3 40.0 %collective-permute-start.25 = (bf16[4,64,768]{2,1,0:T(8,128)(2,1)S(1)}, bf16[4,64,768]{2,1,0:T(8,128)(2,1)S(1)}, u32[]{:S(2)}, u32[]{:S(2)}) collective-permute-start(bf16[4,64,768]{2,1,0:T(8,128)(2,1)S(1)} %get-tuple-element.38), channel_id=1, source_target_pairs={{0,16},{2,18},{4,20},{6,22},{8,24},{10,26},{12,28},{14,30},{16,0},... | collective-permute-start | bytes 1179656 | tf_op jit(solution)/shard_map/ppermute | solution.py:82
  238.0 15.0 %collective-permute-start.26 = (bf16[4,64,768]{2,1,0:T(8,128)(2,1)S(1)}, bf16[4,64,768]{2,1,0:T(8,128)(2,1)S(1)}, u32[]{:S(2)}, u32[]{:S(2)}) collective-permute-start(bf16[4,64,768]{2,1,0:T(8,128)(2,1)S(1)} %get-tuple-element.37), channel_id=1, source_target_pairs={{0,24},{2,26},{4,28},{6,30},{8,16},{10,18},{12,20},{14,22},{16,8},... | collective-permute-start | bytes 1179656 | tf_op jit(solution)/shard_map/ppermute | solution.py:82
  238.1 15.0 %collective-permute-start.27 = (bf16[4,64,768]{2,1,0:T(8,128)(2,1)S(1)}, bf16[4,64,768]{2,1,0:T(8,128)(2,1)S(1)}, u32[]{:S(2)}, u32[]{:S(2)}) collective-permute-start(bf16[4,64,768]{2,1,0:T(8,128)(2,1)S(1)} %get-tuple-element.36), channel_id=1, source_target_pairs={{0,8},{2,10},{4,12},{6,14},{8,0},{10,2},{12,4},{14,6},{16,24},{18,... | collective-permute-start | bytes 1179656 | tf_op jit(solution)/shard_map/ppermute | solution.py:82
  238.2 1.8 copy-start.2
  247.1 7.6 %collective-permute-start.28 = (bf16[1024,512]{1,0:T(8,128)(2,1)S(1)}, bf16[1024,512]{1,0:T(8,128)(2,1)S(1)}, u32[]{:S(2)}, u32[]{:S(2)}) collective-permute-start(bf16[1024,512]{1,0:T(8,128)(2,1)S(1)} %multiply_convert_fusion), channel_id=1, source_target_pairs={{0,1},{1,0},{2,3},{3,2},{4,5},{5,4},{6,7},{7,6},{8,9},{9,8},{10,11... | collective-permute-start | bytes 3145736 | tf_op jit(solution)/shard_map/ppermute | solution.py:46
  255.6 7.6 %collective-permute-start.43 = (bf16[256,256]{1,0:T(8,128)(2,1)S(1)}, bf16[256,256]{1,0:T(8,128)(2,1)S(1)}, u32[]{:S(2)}, u32[]{:S(2)}) collective-permute-start(bf16[256,256]{1,0:T(8,128)(2,1)S(1)} %get-tuple-element.46), channel_id=1, source_target_pairs={{0,6},{2,4},{4,2},{6,0},{8,14},{10,12},{12,10},{14,8},{16,22},{18,... | collective-permute-start | bytes 393224 | tf_op jit(solution)/shard_map/ppermute | solution.py:79
  255.7 12.8 %collective-permute-start.42 = (bf16[256,256]{1,0:T(8,128)(2,1)S(1)}, bf16[256,256]{1,0:T(8,128)(2,1)S(1)}, u32[]{:S(2)}, u32[]{:S(2)}) collective-permute-start(bf16[256,256]{1,0:T(8,128)(2,1)S(1)} %get-tuple-element.47), channel_id=1, source_target_pairs={{0,4},{2,6},{4,0},{6,2},{8,12},{10,14},{12,8},{14,10},{16,20},{18,... | collective-permute-start | bytes 393224 | tf_op jit(solution)/shard_map/ppermute | solution.py:79
  257.6 10.9 %collective-permute-start.41 = (bf16[256,256]{1,0:T(8,128)(2,1)S(1)}, bf16[256,256]{1,0:T(8,128)(2,1)S(1)}, u32[]{:S(2)}, u32[]{:S(2)}) collective-permute-start(bf16[256,256]{1,0:T(8,128)(2,1)S(1)} %get-tuple-element.48), channel_id=1, source_target_pairs={{0,2},{2,0},{4,6},{6,4},{8,10},{10,8},{12,14},{14,12},{16,18},{18,... | collective-permute-start | bytes 393224 | tf_op jit(solution)/shard_map/ppermute | solution.py:79
  261.3 13.0 %collective-permute-start.31 = (bf16[256,768]{1,0:T(8,128)(2,1)S(1)}, bf16[256,768]{1,0:T(8,128)(2,1)S(1)}, u32[]{:S(2)}, u32[]{:S(2)}) collective-permute-start(bf16[256,768]{1,0:T(8,128)(2,1)S(1)} %get-tuple-element.33), channel_id=1, source_target_pairs={{0,6},{2,4},{4,2},{6,0},{8,14},{10,12},{12,10},{14,8},{16,22},{18,... | collective-permute-start | bytes 1179656 | tf_op jit(solution)/shard_map/ppermute | solution.py:79
  261.4 18.3 %collective-permute-start.30 = (bf16[256,768]{1,0:T(8,128)(2,1)S(1)}, bf16[256,768]{1,0:T(8,128)(2,1)S(1)}, u32[]{:S(2)}, u32[]{:S(2)}) collective-permute-start(bf16[256,768]{1,0:T(8,128)(2,1)S(1)} %get-tuple-element.34), channel_id=1, source_target_pairs={{0,4},{2,6},{4,0},{6,2},{8,12},{10,14},{12,8},{14,10},{16,20},{18,... | collective-permute-start | bytes 1179656 | tf_op jit(solution)/shard_map/ppermute | solution.py:79
  263.2 16.5 %collective-permute-start.29 = (bf16[256,768]{1,0:T(8,128)(2,1)S(1)}, bf16[256,768]{1,0:T(8,128)(2,1)S(1)}, u32[]{:S(2)}, u32[]{:S(2)}) collective-permute-start(bf16[256,768]{1,0:T(8,128)(2,1)S(1)} %get-tuple-element.35), channel_id=1, source_target_pairs={{0,2},{2,0},{4,6},{6,4},{8,10},{10,8},{12,14},{14,12},{16,18},{18,... | collective-permute-start | bytes 1179656 | tf_op jit(solution)/shard_map/ppermute | solution.py:79
  269.3 13.5 %collective-permute-start.44 = (bf16[128,256]{1,0:T(8,128)(2,1)S(1)}, bf16[128,256]{1,0:T(8,128)(2,1)S(1)}, u32[]{:S(2)}, u32[]{:S(2)}) collective-permute-start(bf16[128,256]{1,0:T(8,128)(2,1)S(1)} %get-tuple-element.43), channel_id=1, source_target_pairs={{0,8},{2,10},{4,12},{6,14},{1,9},{3,11},{5,13},{7,15}} | collective-permute-start | bytes 196616 | tf_op jit(solution)/shard_map/ppermute | solution.py:202
  270.6 12.3 %collective-permute-start.47 = (bf16[128,256]{1,0:T(8,128)(2,1)S(1)}, bf16[128,256]{1,0:T(8,128)(2,1)S(1)}, u32[]{:S(2)}, u32[]{:S(2)}) collective-permute-start(bf16[128,256]{1,0:T(8,128)(2,1)S(1)} %get-tuple-element.44), channel_id=1, source_target_pairs={{24,16},{26,18},{28,20},{30,22},{25,17},{27,19},{29,21},{31,23}} | collective-permute-start | bytes 196616 | tf_op jit(solution)/shard_map/ppermute | solution.py:203
  280.9 8.8 %collective-permute-start.32 = (bf16[128,768]{1,0:T(8,128)(2,1)S(1)}, bf16[128,768]{1,0:T(8,128)(2,1)S(1)}, u32[]{:S(2)}, u32[]{:S(2)}) collective-permute-start(bf16[128,768]{1,0:T(8,128)(2,1)S(1)} %get-tuple-element.30), channel_id=1, source_target_pairs={{0,8},{2,10},{4,12},{6,14},{1,9},{3,11},{5,13},{7,15}} | collective-permute-start | bytes 589832 | tf_op jit(solution)/shard_map/ppermute | solution.py:202
  282.2 7.5 %collective-permute-start.35 = (bf16[128,768]{1,0:T(8,128)(2,1)S(1)}, bf16[128,768]{1,0:T(8,128)(2,1)S(1)}, u32[]{:S(2)}, u32[]{:S(2)}) collective-permute-start(bf16[128,768]{1,0:T(8,128)(2,1)S(1)} %get-tuple-element.31), channel_id=1, source_target_pairs={{24,16},{26,18},{28,20},{30,22},{25,17},{27,19},{29,21},{31,23}} | collective-permute-start | bytes 589832 | tf_op jit(solution)/shard_map/ppermute | solution.py:203
  282.9 12.9 %collective-permute-start.45 = (bf16[128,256]{1,0:T(8,128)(2,1)S(1)}, bf16[128,256]{1,0:T(8,128)(2,1)S(1)}, u32[]{:S(2)}, u32[]{:S(2)}) collective-permute-start(bf16[128,256]{1,0:T(8,128)(2,1)S(1)} %get-tuple-element.41), channel_id=1, source_target_pairs={{0,8},{2,10},{4,12},{6,14},{8,16},{10,18},{12,20},{14,22},{1,9},{3... | collective-permute-start | bytes 196616 | tf_op jit(solution)/shard_map/ppermute | solution.py:202
  287.1 8.7 %collective-permute-start.48 = (bf16[128,256]{1,0:T(8,128)(2,1)S(1)}, bf16[128,256]{1,0:T(8,128)(2,1)S(1)}, u32[]{:S(2)}, u32[]{:S(2)}) collective-permute-start(bf16[128,256]{1,0:T(8,128)(2,1)S(1)} %get-tuple-element.42), channel_id=1, source_target_pairs={{16,8},{18,10},{20,12},{22,14},{24,16},{26,18},{28,20},{30,22},{17... | collective-permute-start | bytes 196616 | tf_op jit(solution)/shard_map/ppermute | solution.py:203
  289.8 12.6 %collective-permute-start.33 = (bf16[128,768]{1,0:T(8,128)(2,1)S(1)}, bf16[128,768]{1,0:T(8,128)(2,1)S(1)}, u32[]{:S(2)}, u32[]{:S(2)}) collective-permute-start(bf16[128,768]{1,0:T(8,128)(2,1)S(1)} %get-tuple-element.28), channel_id=1, source_target_pairs={{0,8},{2,10},{4,12},{6,14},{8,16},{10,18},{12,20},{14,22},{1,9},{3... | collective-permute-start | bytes 589832 | tf_op jit(solution)/shard_map/ppermute | solution.py:202
  294.5 7.9 %collective-permute-start.36 = (bf16[128,768]{1,0:T(8,128)(2,1)S(1)}, bf16[128,768]{1,0:T(8,128)(2,1)S(1)}, u32[]{:S(2)}, u32[]{:S(2)}) collective-permute-start(bf16[128,768]{1,0:T(8,128)(2,1)S(1)} %get-tuple-element.29), channel_id=1, source_target_pairs={{16,8},{18,10},{20,12},{22,14},{24,16},{26,18},{28,20},{30,22},{17... | collective-permute-start | bytes 589832 | tf_op jit(solution)/shard_map/ppermute | solution.py:203
  295.9 12.5 %collective-permute-start.49 = (bf16[128,256]{1,0:T(8,128)(2,1)S(1)}, bf16[128,256]{1,0:T(8,128)(2,1)S(1)}, u32[]{:S(2)}, u32[]{:S(2)}) collective-permute-start(bf16[128,256]{1,0:T(8,128)(2,1)S(1)} %get-tuple-element.40), channel_id=1, source_target_pairs={{8,0},{10,2},{12,4},{14,6},{16,8},{18,10},{20,12},{22,14},{24,16},... | collective-permute-start | bytes 196616 | tf_op jit(solution)/shard_map/ppermute | solution.py:203
  297.8 10.5 %collective-permute-start.46 = (bf16[128,256]{1,0:T(8,128)(2,1)S(1)}, bf16[128,256]{1,0:T(8,128)(2,1)S(1)}, u32[]{:S(2)}, u32[]{:S(2)}) collective-permute-start(bf16[128,256]{1,0:T(8,128)(2,1)S(1)} %get-tuple-element.39), channel_id=1, source_target_pairs={{0,8},{2,10},{4,12},{6,14},{8,16},{10,18},{12,20},{14,22},{16,24},... | collective-permute-start | bytes 196616 | tf_op jit(solution)/shard_map/ppermute | solution.py:202
  302.5 7.6 %collective-permute-start.37 = (bf16[128,768]{1,0:T(8,128)(2,1)S(1)}, bf16[128,768]{1,0:T(8,128)(2,1)S(1)}, u32[]{:S(2)}, u32[]{:S(2)}) collective-permute-start(bf16[128,768]{1,0:T(8,128)(2,1)S(1)} %get-tuple-element.27), channel_id=1, source_target_pairs={{8,0},{10,2},{12,4},{14,6},{16,8},{18,10},{20,12},{22,14},{24,16},... | collective-permute-start | bytes 589832 | tf_op jit(solution)/shard_map/ppermute | solution.py:203
  304.4 7.6 %collective-permute-start.34 = (bf16[128,768]{1,0:T(8,128)(2,1)S(1)}, bf16[128,768]{1,0:T(8,128)(2,1)S(1)}, u32[]{:S(2)}, u32[]{:S(2)}) collective-permute-start(bf16[128,768]{1,0:T(8,128)(2,1)S(1)} %get-tuple-element.26), channel_id=1, source_target_pairs={{0,8},{2,10},{4,12},{6,14},{8,16},{10,18},{12,20},{14,22},{16,24},... | collective-permute-start | bytes 589832 | tf_op jit(solution)/shard_map/ppermute | solution.py:202

commit v3 on v2

--- a/solution.py
+++ b/solution.py
@@ -30,12 +30,16 @@
 
 
 def chunks_of(width):
-    last = width // 4 if width % 512 == 0 else width // 2
-    return [(0, width - last), (width - last, last)]
+    unit = width // 4
+    return [(0, 2 * unit), (2 * unit, unit), (3 * unit, width - 3 * unit)]
 
 
 def far_first(depth):
     return [q for q in range(1, depth) if q != 1] + [1] * (depth > 1)
+
+
+def after(value, *others):
+    return lax.optimization_barrier((value,) + others)[0]
 
 
 def over_tp(value):
@@ -100,7 +104,11 @@
         downs.append(shift(downs[-1], -1, n - 1))
     column = [payload]
     for q in range(1, depth):
-        column.append(jnp.where(level + q < depth, downs[q], ups[depth - q]))
+        block = payload
+        for offset in sorted({(at ^ q) - at for at in range(depth)}):
+            held = downs[offset] if offset > 0 else ups[-offset]
+            block = jnp.where((level ^ q) - level == offset, held, block)
+        column.append(block)
     column = jnp.stack(column)
 
     def blocks_of(weight, gain):
@@ -112,42 +120,53 @@
 
         return block
 
+    def chained(block, axis, indices, held):
+        made = []
+        for index in indices:
+            made.append(block(after(index, held), axis))
+            held = made[-1]
+        return made
+
+    line_order, plane_order = far_first(depth), list(range(1, inner))
+
     def line_then_plane(block):
-        stage = jnp.zeros((depth, inner) + block(0, 0).shape[1:], bf16)
-        stage = put(stage, block(level, 0), level, 0)
-        for q in far_first(depth):
-            stage = put(stage, line(block(level ^ q, 0), q), level ^ q, 0)
+        made = [block(level ^ line_order[0], 0)] if depth > 1 else []
+        rest = [level ^ q for q in line_order[1:]] + [level]
+        made += chained(block, 0, rest, ups[min(1, depth - 1)])
+        stage = jnp.zeros((depth, inner) + made[0].shape[1:], bf16)
+        stage = put(stage, made[-1], level, 0)
+        for q, piece in zip(line_order, made):
+            stage = put(stage, line(piece, q), level ^ q, 0)
         out = put(stage, take(stage, place, 1), place, 1)
         for r in range(1, inner):
             got = plane(take(stage, place ^ r, 1), r)
             out = put(out, got, place ^ r, 1)
-        return out
-
-    def plane_stage(block):
-        stage = jnp.zeros((inner, depth) + block(0, 0).shape[1:], bf16)
-        stage = put(stage, block(place, 1), place, 0)
-        for r in range(1, inner):
-            stage = put(stage, plane(block(place ^ r, 1), r), place ^ r, 0)
+        return out, made[0]
+
+    def plane_stage(block, held):
+        made = chained(block, 1, [place ^ r for r in plane_order] + [place], held)
+        stage = jnp.zeros((inner, depth) + made[0].shape[1:], bf16)
+        stage = put(stage, made[-1], place, 0)
+        for r, piece in zip(plane_order, made):
+            stage = put(stage, plane(piece, r), place ^ r, 0)
         return stage
 
-    def line_stage(stage):
-        out = jnp.zeros((depth, inner) + stage.shape[2:], bf16)
-        out = put(out, take(stage, level, 1), level, 0)
-        for q in far_first(depth):
-            got = line(take(stage, level ^ q, 1), q)
-            out = put(out, got, level ^ q, 0)
-        return out
-
-    gate_out = line_then_plane(blocks_of(gate_weight, norm_gain))
+    def line_parts(stage):
+        return [take(stage, level, 1)] + [line(take(stage, level ^ q, 1), q) for q in line_order]
+
+    def joined(parts, held=None):
+        out = jnp.zeros((depth,) + parts[0].shape, bf16)
+        for q, part in zip([0] + line_order, parts):
+            index = level ^ q if held is None else after(level ^ q, held)
+            out = put(out, part, index, 0)
+        return out.reshape(-1, parts[0].shape[-1])
+
+    gate_out, first_sent = line_then_plane(blocks_of(gate_weight, norm_gain))
     gate_ready = gate_out.reshape(-1, gate_weight.shape[2])
-    up_out = line_stage(plane_stage(blocks_of(up_weight, norm_gain)))
-    up_ready = up_out.reshape(-1, up_weight.shape[2])
-    down_stage = plane_stage(blocks_of(down_weight, None))
-    down_parts = []
-    for start, size in chunks:
-        part = line_stage(down_stage[..., start : start + size])
-        down_parts.append(part.reshape(-1, size))
-    down_ready = jnp.concatenate(down_parts, axis=1)
+    up_stage = plane_stage(blocks_of(up_weight, norm_gain), first_sent)
+    up_ready = joined(line_parts(up_stage))
+    down_stage = plane_stage(blocks_of(down_weight, None), up_stage)
+    down_parts = [line_parts(down_stage[..., start : start + size]) for start, size in chunks]
 
     column_tokens = column[:, :rows]
     column_notes = column[:, rows:, : 2 * rows].astype(f32)
@@ -177,9 +196,11 @@
     hidden = over_tp(hidden)
 
     scale = jnp.where(chosen, share[:, :, None, :], 0.0)
-    partials = []
+    partials, down_ready, held = [], [], hidden[-1][1]
     for c, (start, size) in enumerate(chunks):
-        results = product(hidden, down_parts[c]).astype(bf16)
+        down_ready.append(joined(down_parts[c], held))
+        results = product(hidden, down_ready[c]).astype(bf16)
+        held = results
         results = results.reshape(inner, depth * capacity, size)
         back = [results[0]] + [plane(results[r], r) for r in range(1, inner)]
         back = jnp.stack(back).reshape(inner, depth, capacity, size)
@@ -194,16 +215,12 @@
         )
     mixed = []
     for partial in partials:
-        upward, downward = 0.0, 0.0
-        for n in range(1, depth):
-            reach = depth - n
-            lift = [(s, s + inner) for s in range(count) if s // inner + reach < depth]
-            drop = [(s, s - inner) for s in range(count) if s // inner >= reach]
-            upward = lax.ppermute((partial[reach] + upward).astype(bf16), "fs", lift)
-            downward = lax.ppermute((partial[n] + downward).astype(bf16), "fs", drop)
-            upward, downward = upward.astype(f32), downward.astype(f32)
-        mixed.append((partial[0] + upward + downward).astype(bf16))
+        total = partial[0]
+        for q in line_order:
+            total = total + line(partial[q].astype(bf16), q).astype(f32)
+        mixed.append(total.astype(bf16))
     mixed = jnp.concatenate(mixed, axis=1)
+    down_ready = jnp.concatenate(down_ready, axis=1)
     return (mixed, gate_ready[None], up_ready[None], down_ready[None])
 
 

time: 316 us -> 283 us (0.90)
  the two profiles are of different devices: /device:TPU:12 before, /device:TPU:0 now
where the time goes in v3:
time: 283 us; the launch traced here: 282 us
  waiting for transfers between devices  122 us (43%)
  starting transfers between devices  77.2 us (27%)
  local copies, waits for them, and re-layouts  41.3 us (15%)
  other arithmetic  24.6 us (9%)
  matrix products  14.8 us (5%)
    ppermute x24, waiting for transfers between devices, line(): return lax.ppermute(value, 'fs', [(s, s ^ q * inner) for s in range(count)])  55.8 us
    ppermute x21, waiting for transfers between devices, plane(): return lax.ppermute(value, 'fs', [(s, s ^ r) for s in range(count)])  45.6 us
    ppermute x24, starting transfers between devices, line(): return lax.ppermute(value, 'fs', [(s, s ^ q * inner) for s in range(count)])  38.5 us
    ppermute x21, starting transfers between devices, plane(): return lax.ppermute(value, 'fs', [(s, s ^ r) for s in range(count)])  27 us
    dynamic_update_slice x29, local copies, waits for them, and re-layouts, put(): return lax.dynamic_update_index_in_dim(array, value, index, axis)  23.6 us
    ppermute x6, waiting for transfers between devices, shift(): return lax.ppermute(value, 'fs', pairs)  21 us
    ppermute x6, starting transfers between devices, shift(): return lax.ppermute(value, 'fs', pairs)  11.6 us
    dot_general x10, matrix products, product(): total = total + jnp.dot(value, rows, preferred_element_type=f32)  11.5 us
  transfers between devices with their start and end apart: 53, of which 23 were waited for; matrix products, arithmetic and copies ran while one was open for 27% of the time, Pallas kernels for 0%

profile of v3, /device:TPU:0, one launch (start us, length us, event | category | flops | bytes accessed | tf_op | source)
XLA Modules:
  0.0 281.8 jit_solution(17877559860594654035)
XLA Ops:
  3.0 5.0 %collective-permute-start.1 = (bf16[136,1024]{1,0:T(8,128)(2,1)S(1)}, bf16[136,1024]{1,0:T(8,128)(2,1)S(1)}, u32[]{:S(2)}, u32[]{:S(2)}) collective-permute-start(bf16[136,1024]{1,0:T(8,128)(2,1)S(1)} %pad_maximum_fusion.6), channel_id=1, source_target_pairs={{0,8},{2,10},{4,12},{6,14},{8,16},{10,18},{12,20},{14,22},{16,24},... | collective-permute-start | bytes 835592 | tf_op jit(solution)/shard_map/ppermute | solution.py:99
  9.4 4.4 %collective-permute-done.1 = bf16[136,1024]{1,0:T(8,128)(2,1)S(1)} collective-permute-done((bf16[136,1024]{1,0:T(8,128)(2,1)S(1)}, bf16[136,1024]{1,0:T(8,128)(2,1)S(1)}, u32[]{:S(2)}, u32[]{:S(2)}) %collective-permute-start.1) | collective-permute-done | bytes 278560 | tf_op jit(solution)/shard_map/ppermute | solution.py:99
  13.9 2.1 fusion.17
  16.0 2.7 fusion.22
  18.7 3.5 %collective-permute-start.16 = (bf16[4,128,512]{2,1,0:T(8,128)(2,1)}, bf16[4,128,512]{2,1,0:T(8,128)(2,1)}, u32[]{:S(2)}, u32[]{:S(2)}) collective-permute-start(bf16[4,128,512]{2,1,0:T(8,128)(2,1)} %get-tuple-element.52), channel_id=1, source_target_pairs={{0,16},{2,18},{4,20},{6,22},{8,24},{10,26},{12,28},{14,30},{16,0},... | collective-permute-start | bytes 1572872 | tf_op jit(solution)/shard_map/ppermute | solution.py:86
  22.2 2.1 fusion.21
  24.3 2.2 fusion.20
  26.5 1.5 collective-permute-start.10
  28.0 1.5 collective-permute-start.11
  30.9 2.1 fusion.19
  34.3 1.5 broadcast.47.clone
  35.8 2.1 fusion.37
  39.5 11.2 %collective-permute-done.2 = bf16[136,1024]{1,0:T(8,128)(2,1)} collective-permute-done((bf16[136,1024]{1,0:T(8,128)(2,1)S(1)}, bf16[136,1024]{1,0:T(8,128)(2,1)}, u32[]{:S(2)}, u32[]{:S(2)}) %collective-permute-start.2) | collective-permute-done | bytes 278560 | tf_op jit(solution)/shard_map/ppermute | solution.py:99
  50.8 1.9 collective-permute-start.12
  58.6 7.1 %collective-permute-done.12 = bf16[4,128,512]{2,1,0:T(8,128)(2,1)S(1)} collective-permute-done((bf16[4,128,512]{2,1,0:T(8,128)(2,1)}, bf16[4,128,512]{2,1,0:T(8,128)(2,1)S(1)}, u32[]{:S(2)}, u32[]{:S(2)}) %collective-permute-start.12) | collective-permute-done | bytes 524320 | tf_op jit(solution)/shard_map/ppermute | solution.py:83
  67.1 2.1 fusion.38
  69.2 2.1 fusion.39
  71.3 2.1 fusion.40
  73.4 1.5 collective-permute-start.22
  74.9 1.9 bitcast_dynamic-update-slice_fusion.8
  76.8 1.9 bitcast_dynamic-update-slice_fusion.7
  78.7 5.4 %collective-permute-done.4 = bf16[136,1024]{1,0:T(8,128)(2,1)} collective-permute-done((bf16[136,1024]{1,0:T(8,128)(2,1)}, bf16[136,1024]{1,0:T(8,128)(2,1)}, u32[]{:S(2)}, u32[]{:S(2)}) %collective-permute-start.4) | collective-permute-done | bytes 278560 | tf_op jit(solution)/shard_map/ppermute | solution.py:99
  87.5 1.4 collective-permute-start.8
  89.0 1.5 collective-permute-start.7
  91.0 1.9 bitcast_dynamic-update-slice_fusion.6
  92.9 2.9 %dynamic-slice_bitcast_fusion = (bf16[4,128,512]{2,1,0:T(8,128)(2,1)}, bf16[4,128,512]{2,1,0:T(8,128)(2,1)}, bf16[4,128,512]{2,1,0:T(8,128)(2,1)}, bf16[4,4,128,512]{3,2,1,0:T(8,128)(2,1)}) fusion(bf16[4,4,128,512]{3,2,1,0:T(8,128)(2,1)} %bitcast_dynamic-update-slice_fusion.6, s32[]{:T(128)S(6)} %select_n.258, s32[]{:T(128)S(6)} %select_n.257, ...), kind=kLoop, calls=%fused_computation.102 | loop fusion | bytes 4194320 | tf_op jit(solution)/shard_map/jit(dynamic_index_in_dim)/squeeze | solution.py:64
  95.7 1.5 collective-permute-start.19
  97.5 6.1 %collective-permute-done.8 = bf16[256,1024]{1,0:T(8,128)(2,1)} collective-permute-done((bf16[256,1024]{1,0:T(8,128)(2,1)}, bf16[256,1024]{1,0:T(8,128)(2,1)}, u32[]{:S(2)}, u32[]{:S(2)}) %collective-permute-start.8) | collective-permute-done | bytes 524320 | tf_op jit(solution)/shard_map/ppermute | solution.py:83
  103.6 1.5 collective-permute-start.20
  105.1 8.8 %collective-permute-done.7 = bf16[256,1024]{1,0:T(8,128)(2,1)} collective-permute-done((bf16[256,1024]{1,0:T(8,128)(2,1)}, bf16[256,1024]{1,0:T(8,128)(2,1)}, u32[]{:S(2)}, u32[]{:S(2)}) %collective-permute-start.7) | collective-permute-done | bytes 524320 | tf_op jit(solution)/shard_map/ppermute | solution.py:83
  115.4 1.9 fusion
  119.2 6.8 %collective-permute-done.19 = bf16[4,128,512]{2,1,0:T(8,128)(2,1)S(1)} collective-permute-done((bf16[4,128,512]{2,1,0:T(8,128)(2,1)}, bf16[4,128,512]{2,1,0:T(8,128)(2,1)S(1)}, u32[]{:S(2)}, u32[]{:S(2)}) %collective-permute-start.19) | collective-permute-done | bytes 524320 | tf_op jit(solution)/shard_map/ppermute | solution.py:83
  126.0 1.5 collective-permute-start.13
  129.2 7.0 %collective-permute-done.21 = bf16[4,128,512]{2,1,0:T(8,128)(2,1)S(1)} collective-permute-done((bf16[4,128,512]{2,1,0:T(8,128)(2,1)S(1)}, bf16[4,128,512]{2,1,0:T(8,128)(2,1)S(1)}, u32[]{:S(2)}, u32[]{:S(2)}) %collective-permute-start.21) | collective-permute-done | bytes 524320 | tf_op jit(solution)/shard_map/ppermute | solution.py:83
  137.1 22.5 %collective-permute-done.13 = bf16[4,128,512]{2,1,0:T(8,128)(2,1)S(1)} collective-permute-done((bf16[4,128,512]{2,1,0:T(8,128)(2,1)S(1)}, bf16[4,128,512]{2,1,0:T(8,128)(2,1)S(1)}, u32[]{:S(2)}, u32[]{:S(2)}) %collective-permute-start.13) | collective-permute-done | bytes 524320 | tf_op jit(solution)/shard_map/ppermute | solution.py:86
  160.1 1.5 collective-permute-start.24
  161.7 8.0 %collective-permute-done.15 = bf16[4,128,512]{2,1,0:T(8,128)(2,1)S(1)} collective-permute-done((bf16[4,128,512]{2,1,0:T(8,128)(2,1)S(1)}, bf16[4,128,512]{2,1,0:T(8,128)(2,1)S(1)}, u32[]{:S(2)}, u32[]{:S(2)}) %collective-permute-start.15) | collective-permute-done | bytes 524320 | tf_op jit(solution)/shard_map/ppermute | solution.py:86
  169.8 1.5 bitcast_dynamic-update-slice_fusion.2
  174.4 2.5 fusion.23
  177.0 3.2 %multiply_convert_fusion = bf16[1024,512]{1,0:T(8,128)(2,1)S(1)} fusion(f32[1024,512]{1,0:T(8,128)S(1)} %fusion.23, f32[1024,512]{1,0:T(8,128)S(1)} %fusion.28, f32[1024,512]{1,0:T(8,128)S(1)} %fusion.26, bf16[2048,512]{1,0:T(8,128)(2,1)} %bitcast.43, s32[]{:T(128)S(6)} %select_n.262, bf16[1024,1024]{1,0:T(8,128)(2,1)S(1)} %get-tuple-element.51, ...), kind=kOutput, calls=%fused_computation.11 | convolution fusion | flops 1083179008 | bytes 10489860 | tf_op jit(solution)/shard_map/dot_general | solution.py:59
  180.2 4.4 %collective-permute-done.23 = bf16[4,64,1024]{2,1,0:T(8,128)(2,1)S(1)} collective-permute-done((bf16[4,64,1024]{2,1,0:T(8,128)(2,1)S(1)}, bf16[4,64,1024]{2,1,0:T(8,128)(2,1)S(1)}, u32[]{:S(2)}, u32[]{:S(2)}) %collective-permute-start.23) | collective-permute-done | bytes 524320 | tf_op jit(solution)/shard_map/ppermute | solution.py:83
  187.1 2.5 collective-permute-start.27
  190.6 1.9 collective-permute-start.35
  193.2 2.5 collective-permute-start.36
  196.9 11.5 %collective-permute-done.26 = bf16[4,64,512]{2,1,0:T(8,128)(2,1)} collective-permute-done((bf16[4,64,512]{2,1,0:T(8,128)(2,1)}, bf16[4,64,512]{2,1,0:T(8,128)(2,1)}, u32[]{:S(2)}, u32[]{:S(2)}) %collective-permute-start.26) | collective-permute-done | bytes 262176 | tf_op jit(solution)/shard_map/ppermute | solution.py:86
  209.4 8.4 %collective-permute-start.44 = (bf16[4,64,256]{2,1,0:T(8,128)(2,1)}, bf16[4,64,256]{2,1,0:T(8,128)(2,1)S(1)}, u32[]{:S(2)}, u32[]{:S(2)}) collective-permute-start(bf16[4,64,256]{2,1,0:T(8,128)(2,1)} %get-tuple-element.89), channel_id=1, source_target_pairs={{0,16},{2,18},{4,20},{6,22},{8,24},{10,26},{12,28},{14,30},{16,0},... | collective-permute-start | bytes 393224 | tf_op jit(solution)/shard_map/ppermute | solution.py:86
  218.8 3.0 %collective-permute-start.45 = (bf16[4,64,256]{2,1,0:T(8,128)(2,1)}, bf16[4,64,256]{2,1,0:T(8,128)(2,1)}, u32[]{:S(2)}, u32[]{:S(2)}) collective-permute-start(bf16[4,64,256]{2,1,0:T(8,128)(2,1)} %get-tuple-element.88), channel_id=1, source_target_pairs={{0,24},{2,26},{4,28},{6,30},{8,16},{10,18},{12,20},{14,22},{16,8},... | collective-permute-start | bytes 393224 | tf_op jit(solution)/shard_map/ppermute | solution.py:86
  234.7 1.5 collective-permute-start.49
  236.7 1.5 collective-permute-start.47
  240.3 1.6 maximum_bitcast_fusion
  242.0 1.5 collective-permute-start.38
  243.5 1.4 collective-permute-done.48
  244.9 1.5 collective-permute-start.31
  248.0 1.6 collective-permute-start.29
  249.5 3.8 %collective-permute-done.39 = bf16[256,256]{1,0:T(8,128)(2,1)S(1)} collective-permute-done((bf16[256,256]{1,0:T(8,128)(2,1)S(1)}, bf16[256,256]{1,0:T(8,128)(2,1)S(1)}, u32[]{:S(2)}, u32[]{:S(2)}) %collective-permute-start.39) | collective-permute-done | bytes 131104 | tf_op jit(solution)/shard_map/ppermute | solution.py:83
  253.3 3.0 %collective-permute-start.52 = (bf16[128,256]{1,0:T(8,128)(2,1)S(1)}, bf16[128,256]{1,0:T(8,128)(2,1)S(1)}, u32[]{:S(2)}, u32[]{:S(2)}) collective-permute-start(bf16[128,256]{1,0:T(8,128)(2,1)S(1)} %get-tuple-element.98), channel_id=1, source_target_pairs={{0,8},{2,10},{4,12},{6,14},{8,0},{10,2},{12,4},{14,6},{16,24},{18,... | collective-permute-start | bytes 196616 | tf_op jit(solution)/shard_map/ppermute | solution.py:86
  258.7 1.9 collective-permute-start.50
  260.6 2.4 collective-permute-done.51
  263.0 3.0 %collective-permute-done.50 = bf16[128,256]{1,0:T(8,128)(2,1)S(1)} collective-permute-done((bf16[128,256]{1,0:T(8,128)(2,1)S(1)}, bf16[128,256]{1,0:T(8,128)(2,1)S(1)}, u32[]{:S(2)}, u32[]{:S(2)}) %collective-permute-start.50) | collective-permute-done | bytes 65568 | tf_op jit(solution)/shard_map/ppermute | solution.py:86
  266.0 1.6 collective-permute-start.42
  268.6 2.8 collective-permute-start.34
  271.4 1.6 collective-permute-start.33
  275.7 2.6 collective-permute-done.33
  278.3 2.7 collective-permute-done.32
  (183 shorter events, 59.9 us)
Async XLA Ops:
  0.6 15.4 %copy-start.20 = (f32[128]{0:T(128)S(1)}, f32[128]{0:T(128)}, u32[]{:S(2)}) copy-start(f32[128]{0:T(128)} %param.8) | copy-start | bytes 1540
  3.0 10.9 %collective-permute-start.1 = (bf16[136,1024]{1,0:T(8,128)(2,1)S(1)}, bf16[136,1024]{1,0:T(8,128)(2,1)S(1)}, u32[]{:S(2)}, u32[]{:S(2)}) collective-permute-start(bf16[136,1024]{1,0:T(8,128)(2,1)S(1)} %pad_maximum_fusion.6), channel_id=1, source_target_pairs={{0,8},{2,10},{4,12},{6,14},{8,16},{10,18},{12,20},{14,22},{16,24},... | collective-permute-start | bytes 835592 | tf_op jit(solution)/shard_map/ppermute | solution.py:99
  8.0 25.0 %collective-permute-start = (bf16[136,1024]{1,0:T(8,128)(2,1)S(1)}, bf16[136,1024]{1,0:T(8,128)(2,1)S(1)}, u32[]{:S(2)}, u32[]{:S(2)}) collective-permute-start(bf16[136,1024]{1,0:T(8,128)(2,1)S(1)} %pad_maximum_fusion.6), channel_id=1, source_target_pairs={{8,0},{10,2},{12,4},{14,6},{16,8},{18,10},{20,12},{22,14},{24,16},... | collective-permute-start | bytes 835592 | tf_op jit(solution)/shard_map/ppermute | solution.py:99
  18.7 54.8 %collective-permute-start.16 = (bf16[4,128,512]{2,1,0:T(8,128)(2,1)}, bf16[4,128,512]{2,1,0:T(8,128)(2,1)}, u32[]{:S(2)}, u32[]{:S(2)}) collective-permute-start(bf16[4,128,512]{2,1,0:T(8,128)(2,1)} %get-tuple-element.52), channel_id=1, source_target_pairs={{0,16},{2,18},{4,20},{6,22},{8,24},{10,26},{12,28},{14,30},{16,0},... | collective-permute-start | bytes 1572872 | tf_op jit(solution)/shard_map/ppermute | solution.py:86
  26.5 27.3 %collective-permute-start.10 = (bf16[4,128,512]{2,1,0:T(8,128)(2,1)}, bf16[4,128,512]{2,1,0:T(8,128)(2,1)}, u32[]{:S(2)}, u32[]{:S(2)}) collective-permute-start(bf16[4,128,512]{2,1,0:T(8,128)(2,1)} %fusion.21), channel_id=1, source_target_pairs={{0,2},{2,0},{4,6},{6,4},{8,10},{10,8},{12,14},{14,12},{16,18},{18,... | collective-permute-start | bytes 1572872 | tf_op jit(solution)/shard_map/ppermute | solution.py:83
  28.0 28.3 %collective-permute-start.11 = (bf16[4,128,512]{2,1,0:T(8,128)(2,1)}, bf16[4,128,512]{2,1,0:T(8,128)(2,1)}, u32[]{:S(2)}, u32[]{:S(2)}) collective-permute-start(bf16[4,128,512]{2,1,0:T(8,128)(2,1)} %fusion.20), channel_id=1, source_target_pairs={{0,4},{2,6},{4,0},{6,2},{8,12},{10,14},{12,8},{14,10},{16,20},{18,... | collective-permute-start | bytes 1572872 | tf_op jit(solution)/shard_map/ppermute | solution.py:83
  29.5 21.3 %collective-permute-start.3 = (bf16[136,1024]{1,0:T(8,128)(2,1)S(1)}, bf16[136,1024]{1,0:T(8,128)(2,1)}, u32[]{:S(2)}, u32[]{:S(2)}) collective-permute-start(bf16[136,1024]{1,0:T(8,128)(2,1)S(1)} %collective-permute-done.1), channel_id=1, source_target_pairs={{8,16},{10,18},{12,20},{14,22},{16,24},{18,26},{20,28},{22,30},{9,... | collective-permute-start | bytes 835592 | tf_op jit(solution)/shard_map/ppermute | solution.py:99
  33.0 17.8 %collective-permute-start.2 = (bf16[136,1024]{1,0:T(8,128)(2,1)S(1)}, bf16[136,1024]{1,0:T(8,128)(2,1)}, u32[]{:S(2)}, u32[]{:S(2)}) collective-permute-start(bf16[136,1024]{1,0:T(8,128)(2,1)S(1)} %collective-permute-done), channel_id=1, source_target_pairs={{8,0},{10,2},{12,4},{14,6},{16,8},{18,10},{20,12},{22,14},{9,1},{1... | collective-permute-start | bytes 835592 | tf_op jit(solution)/shard_map/ppermute | solution.py:99
  38.0 14.8 %copy-start.3 = (bf16[128,1024]{1,0:T(8,128)(2,1)S(1)}, bf16[128,1024]{1,0:T(8,128)(2,1)}, u32[]{:S(2)}) copy-start(bf16[128,1024]{1,0:T(8,128)(2,1)} %param.7) | copy-start | bytes 786436
  50.8 26.0 %collective-permute-start.17 = (bf16[4,128,512]{2,1,0:T(8,128)(2,1)}, bf16[4,128,512]{2,1,0:T(8,128)(2,1)}, u32[]{:S(2)}, u32[]{:S(2)}) collective-permute-start(bf16[4,128,512]{2,1,0:T(8,128)(2,1)} %fusion.17), channel_id=1, source_target_pairs={{0,24},{2,26},{4,28},{6,30},{8,16},{10,18},{12,20},{14,22},{16,8},... | collective-permute-start | bytes 1572872 | tf_op jit(solution)/shard_map/ppermute | solution.py:86
  50.8 15.0 %collective-permute-start.12 = (bf16[4,128,512]{2,1,0:T(8,128)(2,1)}, bf16[4,128,512]{2,1,0:T(8,128)(2,1)S(1)}, u32[]{:S(2)}, u32[]{:S(2)}) collective-permute-start(bf16[4,128,512]{2,1,0:T(8,128)(2,1)} %fusion.19), channel_id=1, source_target_pairs={{0,6},{2,4},{4,2},{6,0},{8,14},{10,12},{12,10},{14,8},{16,22},{18,... | collective-permute-start | bytes 1572872 | tf_op jit(solution)/shard_map/ppermute | solution.py:83
  53.8 37.2 %collective-permute-start.18 = (bf16[4,128,512]{2,1,0:T(8,128)(2,1)S(1)}, bf16[4,128,512]{2,1,0:T(8,128)(2,1)}, u32[]{:S(2)}, u32[]{:S(2)}) collective-permute-start(bf16[4,128,512]{2,1,0:T(8,128)(2,1)S(1)} %get-tuple-element.53), channel_id=1, source_target_pairs={{0,8},{2,10},{4,12},{6,14},{8,0},{10,2},{12,4},{14,6},{16,24},{18,... | collective-permute-start | bytes 1572872 | tf_op jit(solution)/shard_map/ppermute | solution.py:86
  56.2 27.8 %collective-permute-start.4 = (bf16[136,1024]{1,0:T(8,128)(2,1)}, bf16[136,1024]{1,0:T(8,128)(2,1)}, u32[]{:S(2)}, u32[]{:S(2)}) collective-permute-start(bf16[136,1024]{1,0:T(8,128)(2,1)} %collective-permute-done.2), channel_id=1, source_target_pairs={{8,0},{10,2},{12,4},{14,6},{9,1},{11,3},{13,5},{15,7}} | collective-permute-start | bytes 835592 | tf_op jit(solution)/shard_map/ppermute | solution.py:99
  65.7 18.3 %collective-permute-start.5 = (bf16[136,1024]{1,0:T(8,128)(2,1)}, bf16[136,1024]{1,0:T(8,128)(2,1)}, u32[]{:S(2)}, u32[]{:S(2)}) collective-permute-start(bf16[136,1024]{1,0:T(8,128)(2,1)} %collective-permute-done.3), channel_id=1, source_target_pairs={{16,24},{18,26},{20,28},{22,30},{17,25},{19,27},{21,29},{23,31}} | collective-permute-start | bytes 835592 | tf_op jit(solution)/shard_map/ppermute | solution.py:99
  73.4 10.6 %copy-start.12 = (bf16[136,1024]{1,0:T(8,128)(2,1)S(1)}, bf16[136,1024]{1,0:T(8,128)(2,1)}, u32[]{:S(2)}) copy-start(bf16[136,1024]{1,0:T(8,128)(2,1)} %copy-done.11) | copy-start | bytes 835588
  73.4 96.4 %collective-permute-start.22 = (bf16[4,64,1024]{2,1,0:T(8,128)(2,1)}, bf16[4,64,1024]{2,1,0:T(8,128)(2,1)}, u32[]{:S(2)}, u32[]{:S(2)}) collective-permute-start(bf16[4,64,1024]{2,1,0:T(8,128)(2,1)} %fusion.38), channel_id=1, source_target_pairs={{0,2},{2,0},{4,6},{6,4},{8,10},{10,8},{12,14},{14,12},{16,18},{18,... | collective-permute-start | bytes 1572872 | tf_op jit(solution)/shard_map/ppermute | solution.py:83
  87.5 16.1 %collective-permute-start.8 = (bf16[256,1024]{1,0:T(8,128)(2,1)}, bf16[256,1024]{1,0:T(8,128)(2,1)}, u32[]{:S(2)}, u32[]{:S(2)}) collective-permute-start(bf16[256,1024]{1,0:T(8,128)(2,1)} %bitcast.13), channel_id=1, source_target_pairs={{0,6},{2,4},{4,2},{6,0},{8,14},{10,12},{12,10},{14,8},{16,22},{18,... | collective-permute-start | bytes 1572872 | tf_op jit(solution)/shard_map/ppermute | solution.py:83
  89.0 24.9 %collective-permute-start.7 = (bf16[256,1024]{1,0:T(8,128)(2,1)}, bf16[256,1024]{1,0:T(8,128)(2,1)}, u32[]{:S(2)}, u32[]{:S(2)}) collective-permute-start(bf16[256,1024]{1,0:T(8,128)(2,1)} %bitcast.12), channel_id=1, source_target_pairs={{0,4},{2,6},{4,0},{6,2},{8,12},{10,14},{12,8},{14,10},{16,20},{18,... | collective-permute-start | bytes 1572872 | tf_op jit(solution)/shard_map/ppermute | solution.py:83
  90.5 24.9 %collective-permute-start.6 = (bf16[256,1024]{1,0:T(8,128)(2,1)}, bf16[256,1024]{1,0:T(8,128)(2,1)}, u32[]{:S(2)}, u32[]{:S(2)}) collective-permute-start(bf16[256,1024]{1,0:T(8,128)(2,1)} %bitcast.11), channel_id=1, source_target_pairs={{0,2},{2,0},{4,6},{6,4},{8,10},{10,8},{12,14},{14,12},{16,18},{18,... | collective-permute-start | bytes 1572872 | tf_op jit(solution)/shard_map/ppermute | solution.py:83
  95.7 30.3 %collective-permute-start.19 = (bf16[4,128,512]{2,1,0:T(8,128)(2,1)}, bf16[4,128,512]{2,1,0:T(8,128)(2,1)S(1)}, u32[]{:S(2)}, u32[]{:S(2)}) collective-permute-start(bf16[4,128,512]{2,1,0:T(8,128)(2,1)} %get-tuple-element.65), channel_id=1, source_target_pairs={{0,2},{2,0},{4,6},{6,4},{8,10},{10,8},{12,14},{14,12},{16,18},{18,... | collective-permute-start | bytes 1572872 | tf_op jit(solution)/shard_map/ppermute | solution.py:83
  97.2 6.3 %copy-start.10 = (bf16[4,128,512]{2,1,0:T(8,128)(2,1)S(1)}, bf16[4,128,512]{2,1,0:T(8,128)(2,1)}, u32[]{:S(2)}) copy-start(bf16[4,128,512]{2,1,0:T(8,128)(2,1)} %get-tuple-element.64) | copy-start | bytes 1572868
  97.2 16.7 %copy-start.9 = (bf16[4,128,512]{2,1,0:T(8,128)(2,1)S(1)}, bf16[4,128,512]{2,1,0:T(8,128)(2,1)}, u32[]{:S(2)}) copy-start(bf16[4,128,512]{2,1,0:T(8,128)(2,1)} %get-tuple-element.63) | copy-start | bytes 1572868
  103.6 24.8 %collective-permute-start.20 = (bf16[4,128,512]{2,1,0:T(8,128)(2,1)S(1)}, bf16[4,128,512]{2,1,0:T(8,128)(2,1)S(1)}, u32[]{:S(2)}, u32[]{:S(2)}) collective-permute-start(bf16[4,128,512]{2,1,0:T(8,128)(2,1)S(1)} %copy-done.10), channel_id=1, source_target_pairs={{0,4},{2,6},{4,0},{6,2},{8,12},{10,14},{12,8},{14,10},{16,20},{18,... | collective-permute-start | bytes 1572872 | tf_op jit(solution)/shard_map/ppermute | solution.py:83
  113.9 22.3 %collective-permute-start.21 = (bf16[4,128,512]{2,1,0:T(8,128)(2,1)S(1)}, bf16[4,128,512]{2,1,0:T(8,128)(2,1)S(1)}, u32[]{:S(2)}, u32[]{:S(2)}) collective-permute-start(bf16[4,128,512]{2,1,0:T(8,128)(2,1)S(1)} %copy-done.9), channel_id=1, source_target_pairs={{0,6},{2,4},{4,2},{6,0},{8,14},{10,12},{12,10},{14,8},{16,22},{18,... | collective-permute-start | bytes 1572872 | tf_op jit(solution)/shard_map/ppermute | solution.py:83
  117.3 54.0 %collective-permute-start.9 = (bf16[1024,1024]{1,0:T(8,128)(2,1)S(1)}, bf16[1024,1024]{1,0:T(8,128)(2,1)S(1)}, u32[]{:S(2)}, u32[]{:S(2)}) collective-permute-start(bf16[1024,1024]{1,0:T(8,128)(2,1)S(1)} %get-tuple-element.51), channel_id=1, source_target_pairs={{0,1},{1,0},{2,3},{3,2},{4,5},{5,4},{6,7},{7,6},{8,9},{9,8},{10,11... | collective-permute-start | bytes 6291464 | tf_op jit(solution)/shard_map/ppermute | solution.py:50
  119.1 40.4 %copy-start.7 = (bf16[4,64,1024]{2,1,0:T(8,128)(2,1)S(1)}, bf16[4,64,1024]{2,1,0:T(8,128)(2,1)}, u32[]{:S(2)}) copy-start(bf16[4,64,1024]{2,1,0:T(8,128)(2,1)} %fusion.39) | copy-start | bytes 1572868
  126.0 33.6 %collective-permute-start.13 = (bf16[4,128,512]{2,1,0:T(8,128)(2,1)S(1)}, bf16[4,128,512]{2,1,0:T(8,128)(2,1)S(1)}, u32[]{:S(2)}, u32[]{:S(2)}) collective-permute-start(bf16[4,128,512]{2,1,0:T(8,128)(2,1)S(1)} %get-tuple-element.58), channel_id=1, source_target_pairs={{0,16},{2,18},{4,20},{6,22},{8,24},{10,26},{12,28},{14,30},{16,0},... | collective-permute-start | bytes 1572872 | tf_op jit(solution)/shard_map/ppermute | solution.py:86
  127.5 32.6 %copy-start.8 = (bf16[4,64,1024]{2,1,0:T(8,128)(2,1)S(1)}, bf16[4,64,1024]{2,1,0:T(8,128)(2,1)}, u32[]{:S(2)}) copy-start(bf16[4,64,1024]{2,1,0:T(8,128)(2,1)} %fusion.40) | copy-start | bytes 1572868
  128.4 31.8 %collective-permute-start.14 = (bf16[4,128,512]{2,1,0:T(8,128)(2,1)S(1)}, bf16[4,128,512]{2,1,0:T(8,128)(2,1)S(1)}, u32[]{:S(2)}, u32[]{:S(2)}) collective-permute-start(bf16[4,128,512]{2,1,0:T(8,128)(2,1)S(1)} %get-tuple-element.57), channel_id=1, source_target_pairs={{0,24},{2,26},{4,28},{6,30},{8,16},{10,18},{12,20},{14,22},{16,8},... | collective-permute-start | bytes 1572872 | tf_op jit(solution)/shard_map/ppermute | solution.py:86
  136.2 33.5 %collective-permute-start.15 = (bf16[4,128,512]{2,1,0:T(8,128)(2,1)S(1)}, bf16[4,128,512]{2,1,0:T(8,128)(2,1)S(1)}, u32[]{:S(2)}, u32[]{:S(2)}) collective-permute-start(bf16[4,128,512]{2,1,0:T(8,128)(2,1)S(1)} %get-tuple-element.56), channel_id=1, source_target_pairs={{0,8},{2,10},{4,12},{6,14},{8,0},{10,2},{12,4},{14,6},{16,24},{18,... | collective-permute-start | bytes 1572872 | tf_op jit(solution)/shard_map/ppermute | solution.py:86
  159.6 25.0 %collective-permute-start.23 = (bf16[4,64,1024]{2,1,0:T(8,128)(2,1)S(1)}, bf16[4,64,1024]{2,1,0:T(8,128)(2,1)S(1)}, u32[]{:S(2)}, u32[]{:S(2)}) collective-permute-start(bf16[4,64,1024]{2,1,0:T(8,128)(2,1)S(1)} %copy-done.7), channel_id=1, source_target_pairs={{0,4},{2,6},{4,0},{6,2},{8,12},{10,14},{12,8},{14,10},{16,20},{18,... | collective-permute-start | bytes 1572872 | tf_op jit(solution)/shard_map/ppermute | solution.py:83
  160.1 24.5 %collective-permute-start.24 = (bf16[4,64,1024]{2,1,0:T(8,128)(2,1)S(1)}, bf16[4,64,1024]{2,1,0:T(8,128)(2,1)S(1)}, u32[]{:S(2)}, u32[]{:S(2)}) collective-permute-start(bf16[4,64,1024]{2,1,0:T(8,128)(2,1)S(1)} %copy-done.8), channel_id=1, source_target_pairs={{0,6},{2,4},{4,2},{6,0},{8,14},{10,12},{12,10},{14,8},{16,22},{18,... | collective-permute-start | bytes 1572872 | tf_op jit(solution)/shard_map/ppermute | solution.py:83
  180.1 13.1 %collective-permute-start.25 = (bf16[1024,512]{1,0:T(8,128)(2,1)S(1)}, bf16[1024,512]{1,0:T(8,128)(2,1)S(1)}, u32[]{:S(2)}, u32[]{:S(2)}) collective-permute-start(bf16[1024,512]{1,0:T(8,128)(2,1)S(1)} %multiply_convert_fusion), channel_id=1, source_target_pairs={{0,1},{1,0},{2,3},{3,2},{4,5},{5,4},{6,7},{7,6},{8,9},{9,8},{10,11... | collective-permute-start | bytes 3145736 | tf_op jit(solution)/shard_map/ppermute | solution.py:50
  185.8 22.6 %collective-permute-start.26 = (bf16[4,64,512]{2,1,0:T(8,128)(2,1)}, bf16[4,64,512]{2,1,0:T(8,128)(2,1)}, u32[]{:S(2)}, u32[]{:S(2)}) collective-permute-start(bf16[4,64,512]{2,1,0:T(8,128)(2,1)} %get-tuple-element.73), channel_id=1, source_target_pairs={{0,16},{2,18},{4,20},{6,22},{8,24},{10,26},{12,28},{14,30},{16,0},... | collective-permute-start | bytes 786440 | tf_op jit(solution)/shard_map/ppermute | solution.py:86
  187.1 22.3 %collective-permute-start.27 = (bf16[4,64,512]{2,1,0:T(8,128)(2,1)}, bf16[4,64,512]{2,1,0:T(8,128)(2,1)}, u32[]{:S(2)}, u32[]{:S(2)}) collective-permute-start(bf16[4,64,512]{2,1,0:T(8,128)(2,1)} %get-tuple-element.72), channel_id=1, source_target_pairs={{0,24},{2,26},{4,28},{6,30},{8,16},{10,18},{12,20},{14,22},{16,8},... | collective-permute-start | bytes 786440 | tf_op jit(solution)/shard_map/ppermute | solution.py:86
  189.6 29.2 %collective-permute-start.28 = (bf16[4,64,512]{2,1,0:T(8,128)(2,1)S(1)}, bf16[4,64,512]{2,1,0:T(8,128)(2,1)}, u32[]{:S(2)}, u32[]{:S(2)}) collective-permute-start(bf16[4,64,512]{2,1,0:T(8,128)(2,1)S(1)} %get-tuple-element.71), channel_id=1, source_target_pairs={{0,8},{2,10},{4,12},{6,14},{8,0},{10,2},{12,4},{14,6},{16,24},{18,... | collective-permute-start | bytes 786440 | tf_op jit(solution)/shard_map/ppermute | solution.py:86
  190.6 35.5 %collective-permute-start.35 = (bf16[4,64,256]{2,1,0:T(8,128)(2,1)}, bf16[4,64,256]{2,1,0:T(8,128)(2,1)}, u32[]{:S(2)}, u32[]{:S(2)}) collective-permute-start(bf16[4,64,256]{2,1,0:T(8,128)(2,1)} %get-tuple-element.92), channel_id=1, source_target_pairs={{0,16},{2,18},{4,20},{6,22},{8,24},{10,26},{12,28},{14,30},{16,0},... | collective-permute-start | bytes 393224 | tf_op jit(solution)/shard_map/ppermute | solution.py:86
  193.2 33.9 %collective-permute-start.36 = (bf16[4,64,256]{2,1,0:T(8,128)(2,1)}, bf16[4,64,256]{2,1,0:T(8,128)(2,1)}, u32[]{:S(2)}, u32[]{:S(2)}) collective-permute-start(bf16[4,64,256]{2,1,0:T(8,128)(2,1)} %get-tuple-element.91), channel_id=1, source_target_pairs={{0,24},{2,26},{4,28},{6,30},{8,16},{10,18},{12,20},{14,22},{16,8},... | collective-permute-start | bytes 393224 | tf_op jit(solution)/shard_map/ppermute | solution.py:86
  208.4 19.7 %collective-permute-start.37 = (bf16[4,64,256]{2,1,0:T(8,128)(2,1)}, bf16[4,64,256]{2,1,0:T(8,128)(2,1)}, u32[]{:S(2)}, u32[]{:S(2)}) collective-permute-start(bf16[4,64,256]{2,1,0:T(8,128)(2,1)} %get-tuple-element.90), channel_id=1, source_target_pairs={{0,8},{2,10},{4,12},{6,14},{8,0},{10,2},{12,4},{14,6},{16,24},{18,... | collective-permute-start | bytes 393224 | tf_op jit(solution)/shard_map/ppermute | solution.py:86
  209.4 22.4 %collective-permute-start.44 = (bf16[4,64,256]{2,1,0:T(8,128)(2,1)}, bf16[4,64,256]{2,1,0:T(8,128)(2,1)S(1)}, u32[]{:S(2)}, u32[]{:S(2)}) collective-permute-start(bf16[4,64,256]{2,1,0:T(8,128)(2,1)} %get-tuple-element.89), channel_id=1, source_target_pairs={{0,16},{2,18},{4,20},{6,22},{8,24},{10,26},{12,28},{14,30},{16,0},... | collective-permute-start | bytes 393224 | tf_op jit(solution)/shard_map/ppermute | solution.py:86
  218.8 13.0 %collective-permute-start.45 = (bf16[4,64,256]{2,1,0:T(8,128)(2,1)}, bf16[4,64,256]{2,1,0:T(8,128)(2,1)}, u32[]{:S(2)}, u32[]{:S(2)}) collective-permute-start(bf16[4,64,256]{2,1,0:T(8,128)(2,1)} %get-tuple-element.88), channel_id=1, source_target_pairs={{0,24},{2,26},{4,28},{6,30},{8,16},{10,18},{12,20},{14,22},{16,8},... | collective-permute-start | bytes 393224 | tf_op jit(solution)/shard_map/ppermute | solution.py:86
  226.1 6.6 %collective-permute-start.46 = (bf16[4,64,256]{2,1,0:T(8,128)(2,1)}, bf16[4,64,256]{2,1,0:T(8,128)(2,1)}, u32[]{:S(2)}, u32[]{:S(2)}) collective-permute-start(bf16[4,64,256]{2,1,0:T(8,128)(2,1)} %get-tuple-element.87), channel_id=1, source_target_pairs={{0,8},{2,10},{4,12},{6,14},{8,0},{10,2},{12,4},{14,6},{16,24},{18,... | collective-permute-start | bytes 393224 | tf_op jit(solution)/shard_map/ppermute | solution.py:86
  234.2 6.1 %copy-start.1 = (bf16[4,4,64,256]{3,2,1,0:T(8,128)(2,1)S(1)}, bf16[4,4,64,256]{3,2,1,0:T(8,128)(2,1)}, u32[]{:S(2)}) copy-start(bf16[4,4,64,256]{3,2,1,0:T(8,128)(2,1)} %copy-done) | copy-start | bytes 1572868
  234.7 7.4 %collective-permute-start.49 = (bf16[256,256]{1,0:T(8,128)(2,1)S(1)}, bf16[256,256]{1,0:T(8,128)(2,1)S(1)}, u32[]{:S(2)}, u32[]{:S(2)}) collective-permute-start(bf16[256,256]{1,0:T(8,128)(2,1)S(1)} %get-tuple-element.84), channel_id=1, source_target_pairs={{0,6},{2,4},{4,2},{6,0},{8,14},{10,12},{12,10},{14,8},{16,22},{18,... | collective-permute-start | bytes 393224 | tf_op jit(solution)/shard_map/ppermute | solution.py:83
  236.2 8.8 %collective-permute-start.48 = (bf16[256,256]{1,0:T(8,128)(2,1)S(1)}, bf16[256,256]{1,0:T(8,128)(2,1)S(1)}, u32[]{:S(2)}, u32[]{:S(2)}) collective-permute-start(bf16[256,256]{1,0:T(8,128)(2,1)S(1)} %get-tuple-element.85), channel_id=1, source_target_pairs={{0,4},{2,6},{4,0},{6,2},{8,12},{10,14},{12,8},{14,10},{16,20},{18,... | collective-permute-start | bytes 393224 | tf_op jit(solution)/shard_map/ppermute | solution.py:83
  236.7 9.8 %collective-permute-start.47 = (bf16[256,256]{1,0:T(8,128)(2,1)S(1)}, bf16[256,256]{1,0:T(8,128)(2,1)S(1)}, u32[]{:S(2)}, u32[]{:S(2)}) collective-permute-start(bf16[256,256]{1,0:T(8,128)(2,1)S(1)} %get-tuple-element.86), channel_id=1, source_target_pairs={{0,2},{2,0},{4,6},{6,4},{8,10},{10,8},{12,14},{14,12},{16,18},{18,... | collective-permute-start | bytes 393224 | tf_op jit(solution)/shard_map/ppermute | solution.py:83
  238.2 9.7 %collective-permute-start.40 = (bf16[256,256]{1,0:T(8,128)(2,1)S(1)}, bf16[256,256]{1,0:T(8,128)(2,1)S(1)}, u32[]{:S(2)}, u32[]{:S(2)}) collective-permute-start(bf16[256,256]{1,0:T(8,128)(2,1)S(1)} %copy-done.19), channel_id=1, source_target_pairs={{0,6},{2,4},{4,2},{6,0},{8,14},{10,12},{12,10},{14,8},{16,22},{18,... | collective-permute-start | bytes 393224 | tf_op jit(solution)/shard_map/ppermute | solution.py:83
  239.7 6.8 %copy-start.14 = (bf16[256,512]{1,0:T(8,128)(2,1)S(1)}, bf16[256,512]{1,0:T(8,128)(2,1)}, u32[]{:S(2)}) copy-start(bf16[256,512]{1,0:T(8,128)(2,1)} %get-tuple-element.69) | copy-start | bytes 786436
  239.7 7.3 %copy-start.22 = (f32[4,4,128]{2,1,0:T(4,128)S(1)}, f32[4,4,128]{2,1,0:T(4,128)}, u32[]{:S(2)}) copy-start(f32[4,4,128]{2,1,0:T(4,128)} %copy-done.21) | copy-start | bytes 24580
  239.7 13.7 %collective-permute-start.39 = (bf16[256,256]{1,0:T(8,128)(2,1)S(1)}, bf16[256,256]{1,0:T(8,128)(2,1)S(1)}, u32[]{:S(2)}, u32[]{:S(2)}) collective-permute-start(bf16[256,256]{1,0:T(8,128)(2,1)S(1)} %copy-done.18), channel_id=1, source_target_pairs={{0,4},{2,6},{4,0},{6,2},{8,12},{10,14},{12,8},{14,10},{16,20},{18,... | collective-permute-start | bytes 393224 | tf_op jit(solution)/shard_map/ppermute | solution.py:83
  241.9 15.8 %copy-start.16 = (bf16[256,256]{1,0:T(8,128)(2,1)S(1)}, bf16[256,256]{1,0:T(8,128)(2,1)}, u32[]{:S(2)}) copy-start(bf16[256,256]{1,0:T(8,128)(2,1)} %get-tuple-element.79) | copy-start | bytes 393220
  242.0 14.3 %collective-permute-start.38 = (bf16[256,256]{1,0:T(8,128)(2,1)S(1)}, bf16[256,256]{1,0:T(8,128)(2,1)S(1)}, u32[]{:S(2)}, u32[]{:S(2)}) collective-permute-start(bf16[256,256]{1,0:T(8,128)(2,1)S(1)} %copy-done.17), channel_id=1, source_target_pairs={{0,2},{2,0},{4,6},{6,4},{8,10},{10,8},{12,14},{14,12},{16,18},{18,... | collective-permute-start | bytes 393224 | tf_op jit(solution)/shard_map/ppermute | solution.py:83
  244.9 22.7 %collective-permute-start.31 = (bf16[256,512]{1,0:T(8,128)(2,1)S(1)}, bf16[256,512]{1,0:T(8,128)(2,1)S(1)}, u32[]{:S(2)}, u32[]{:S(2)}) collective-permute-start(bf16[256,512]{1,0:T(8,128)(2,1)S(1)} %copy-done.15), channel_id=1, source_target_pairs={{0,6},{2,4},{4,2},{6,0},{8,14},{10,12},{12,10},{14,8},{16,22},{18,... | collective-permute-start | bytes 786440 | tf_op jit(solution)/shard_map/ppermute | solution.py:83
  246.4 21.3 %collective-permute-start.30 = (bf16[256,512]{1,0:T(8,128)(2,1)S(1)}, bf16[256,512]{1,0:T(8,128)(2,1)S(1)}, u32[]{:S(2)}, u32[]{:S(2)}) collective-permute-start(bf16[256,512]{1,0:T(8,128)(2,1)S(1)} %copy-done.14), channel_id=1, source_target_pairs={{0,4},{2,6},{4,0},{6,2},{8,12},{10,14},{12,8},{14,10},{16,20},{18,... | collective-permute-start | bytes 786440 | tf_op jit(solution)/shard_map/ppermute | solution.py:83
  248.0 19.8 %collective-permute-start.29 = (bf16[256,512]{1,0:T(8,128)(2,1)S(1)}, bf16[256,512]{1,0:T(8,128)(2,1)S(1)}, u32[]{:S(2)}, u32[]{:S(2)}) collective-permute-start(bf16[256,512]{1,0:T(8,128)(2,1)S(1)} %copy-done.13), channel_id=1, source_target_pairs={{0,2},{2,0},{4,6},{6,4},{8,10},{10,8},{12,14},{14,12},{16,18},{18,... | collective-permute-start | bytes 786440 | tf_op jit(solution)/shard_map/ppermute | solution.py:83
  253.3 5.3 %collective-permute-start.52 = (bf16[128,256]{1,0:T(8,128)(2,1)S(1)}, bf16[128,256]{1,0:T(8,128)(2,1)S(1)}, u32[]{:S(2)}, u32[]{:S(2)}) collective-permute-start(bf16[128,256]{1,0:T(8,128)(2,1)S(1)} %get-tuple-element.98), channel_id=1, source_target_pairs={{0,8},{2,10},{4,12},{6,14},{8,0},{10,2},{12,4},{14,6},{16,24},{18,... | collective-permute-start | bytes 196616 | tf_op jit(solution)/shard_map/ppermute | solution.py:86
  256.3 6.7 %collective-permute-start.51 = (bf16[128,256]{1,0:T(8,128)(2,1)S(1)}, bf16[128,256]{1,0:T(8,128)(2,1)S(1)}, u32[]{:S(2)}, u32[]{:S(2)}) collective-permute-start(bf16[128,256]{1,0:T(8,128)(2,1)S(1)} %get-tuple-element.99), channel_id=1, source_target_pairs={{0,24},{2,26},{4,28},{6,30},{8,16},{10,18},{12,20},{14,22},{16,8},... | collective-permute-start | bytes 196616 | tf_op jit(solution)/shard_map/ppermute | solution.py:86
  258.7 7.3 %collective-permute-start.50 = (bf16[128,256]{1,0:T(8,128)(2,1)S(1)}, bf16[128,256]{1,0:T(8,128)(2,1)S(1)}, u32[]{:S(2)}, u32[]{:S(2)}) collective-permute-start(bf16[128,256]{1,0:T(8,128)(2,1)S(1)} %get-tuple-element.97), channel_id=1, source_target_pairs={{0,16},{2,18},{4,20},{6,22},{8,24},{10,26},{12,28},{14,30},{16,0},... | collective-permute-start | bytes 196616 | tf_op jit(solution)/shard_map/ppermute | solution.py:86
  263.0 10.1 %collective-permute-start.43 = (bf16[128,256]{1,0:T(8,128)(2,1)S(1)}, bf16[128,256]{1,0:T(8,128)(2,1)S(1)}, u32[]{:S(2)}, u32[]{:S(2)}) collective-permute-start(bf16[128,256]{1,0:T(8,128)(2,1)S(1)} %get-tuple-element.95), channel_id=1, source_target_pairs={{0,8},{2,10},{4,12},{6,14},{8,0},{10,2},{12,4},{14,6},{16,24},{18,... | collective-permute-start | bytes 196616 | tf_op jit(solution)/shard_map/ppermute | solution.py:86
  266.0 7.1 %collective-permute-start.42 = (bf16[128,256]{1,0:T(8,128)(2,1)S(1)}, bf16[128,256]{1,0:T(8,128)(2,1)S(1)}, u32[]{:S(2)}, u32[]{:S(2)}) collective-permute-start(bf16[128,256]{1,0:T(8,128)(2,1)S(1)} %get-tuple-element.96), channel_id=1, source_target_pairs={{0,24},{2,26},{4,28},{6,30},{8,16},{10,18},{12,20},{14,22},{16,8},... | collective-permute-start | bytes 196616 | tf_op jit(solution)/shard_map/ppermute | solution.py:86
  267.7 6.8 %collective-permute-start.41 = (bf16[128,256]{1,0:T(8,128)(2,1)S(1)}, bf16[128,256]{1,0:T(8,128)(2,1)S(1)}, u32[]{:S(2)}, u32[]{:S(2)}) collective-permute-start(bf16[128,256]{1,0:T(8,128)(2,1)S(1)} %get-tuple-element.94), channel_id=1, source_target_pairs={{0,16},{2,18},{4,20},{6,22},{8,24},{10,26},{12,28},{14,30},{16,0},... | collective-permute-start | bytes 196616 | tf_op jit(solution)/shard_map/ppermute | solution.py:86
  268.6 7.1 %collective-permute-start.34 = (bf16[128,512]{1,0:T(8,128)(2,1)S(1)}, bf16[128,512]{1,0:T(8,128)(2,1)S(1)}, u32[]{:S(2)}, u32[]{:S(2)}) collective-permute-start(bf16[128,512]{1,0:T(8,128)(2,1)S(1)} %get-tuple-element.77), channel_id=1, source_target_pairs={{0,8},{2,10},{4,12},{6,14},{8,0},{10,2},{12,4},{14,6},{16,24},{18,... | collective-permute-start | bytes 393224 | tf_op jit(solution)/shard_map/ppermute | solution.py:86
  271.4 6.8 %collective-permute-start.33 = (bf16[128,512]{1,0:T(8,128)(2,1)S(1)}, bf16[128,512]{1,0:T(8,128)(2,1)S(1)}, u32[]{:S(2)}, u32[]{:S(2)}) collective-permute-start(bf16[128,512]{1,0:T(8,128)(2,1)S(1)} %get-tuple-element.78), channel_id=1, source_target_pairs={{0,24},{2,26},{4,28},{6,30},{8,16},{10,18},{12,20},{14,22},{16,8},... | collective-permute-start | bytes 393224 | tf_op jit(solution)/shard_map/ppermute | solution.py:86
  273.1 7.9 %collective-permute-start.32 = (bf16[128,512]{1,0:T(8,128)(2,1)S(1)}, bf16[128,512]{1,0:T(8,128)(2,1)S(1)}, u32[]{:S(2)}, u32[]{:S(2)}) collective-permute-start(bf16[128,512]{1,0:T(8,128)(2,1)S(1)} %get-tuple-element.76), channel_id=1, source_target_pairs={{0,16},{2,18},{4,20},{6,22},{8,24},{10,26},{12,28},{14,30},{16,0},... | collective-permute-start | bytes 393224 | tf_op jit(solution)/shard_map/ppermute | solution.py:86
  (12 other events, 46.3 us)

commit v4 on v2

v4 whole, which is shorter than its diff:
```python
import math

import jax
import jax.numpy as jnp
from jax import lax
from jax.sharding import PartitionSpec as P


epsilon = 1e-05
bf16 = jnp.bfloat16
f32 = jnp.float32


def activate(gate_pre, up_pre):
    gated = jnp.minimum(gate_pre, 7.0)
    upper = jnp.clip(up_pre, -7.0, 7.0)
    return (upper + 1.0) * gated * jax.nn.sigmoid(1.702 * gated)


def parts_of(weights):
    first = lax.reduce_precision(weights, 8, 7)
    rest = weights - first
    second = lax.reduce_precision(rest, 8, 7)
    return [p.astype(bf16) for p in (first, second, rest - second)]


def layout_of(count):
    inner = math.gcd(count, 4)
    return inner, count // inner


def chunks_of(width):
    unit = width // 4
    return [(0, 2 * unit), (2 * unit, unit), (3 * unit, width - 3 * unit)]


def far_first(depth):
    return [q for q in range(1, depth) if q != 1] + [1] * (depth > 1)


def after(value, *others):
    return lax.optimization_barrier((value,) + others)[0]


def over_tp(value):
    size, mine = lax.axis_size("tp"), lax.axis_index("tp")
    blocks = [(mine, value)]
    for j in range(1, size):
        pairs = [(s, (s + j) % size) for s in range(size)]
        blocks.append(((mine - j) % size, lax.ppermute(value, "tp", pairs)))
    return blocks


def product(blocks, matrix):
    total = 0.0
    for owner, value in blocks:
        depth = value.shape[1]
        rows = lax.dynamic_slice_in_dim(matrix, owner * depth, depth, 0)
        total = total + jnp.dot(value, rows, preferred_element_type=f32)
    return total


def take(array, index, axis):
    return lax.dynamic_index_in_dim(array, index, axis, keepdims=False)


def put(array, value, index, axis):
    return lax.dynamic_update_index_in_dim(array, value, index, axis)


def shards(tokens, norm_gain, gate_weight, up_weight, down_weight, routes, route_weights):
    count, tp = lax.axis_size("fs"), lax.axis_size("tp")
    inner, depth = layout_of(count)
    me = lax.axis_index("fs")
    level, place = me // inner, me % inner
    rows, width = tokens.shape
    top = routes.shape[1]
    experts = gate_weight.shape[0]
    capacity = 2 * rows * top // experts
    chunks = chunks_of(width)

    def plane(value, r):
        return lax.ppermute(value, "fs", [(s, s ^ r) for s in range(count)])

    def line(value, q):
        return lax.ppermute(value, "fs", [(s, s ^ (q * inner)) for s in range(count)])

    notes = jnp.concatenate([routes.T.astype(bf16)] + parts_of(route_weights.T), axis=0)
    notes = jnp.concatenate([notes[: 2 * top], notes[2 * top :]], axis=1)
    notes = jnp.pad(notes, ((0, 0), (0, width - 2 * rows)))
    payload = jnp.concatenate([tokens, notes], axis=0)

    def shift(value, step, first):
        pairs = []
        for s in range(count):
            at = s // inner
            if 0 <= at + step < depth and (at >= first if step > 0 else at < depth - first):
                pairs.append((s, s + step * inner))
        return lax.ppermute(value, "fs", pairs)

    ups, downs = [payload], [payload]
    for n in range(1, depth):
        ups.append(shift(ups[-1], 1, n - 1))
        downs.append(shift(downs[-1], -1, n - 1))

    line_order, plane_order = far_first(depth), list(range(1, inner))

    def shaped(weight):
        return weight.reshape((depth, inner) + weight.shape[1:])

    def block(weight, gain, index, axis, held):
        if held is not None:
            index = after(index, held)
        part = take(shaped(weight), index, axis)
        return (part * gain[None, :, None] if gain is not None else part).astype(bf16)

    held, gate_sent, up_sent, down_sent = None, {}, {}, {}
    for q in line_order[:1]:
        held = gate_sent[q] = block(gate_weight, norm_gain, level ^ q, 0, held)
    for r in plane_order:
        held = up_sent[r] = block(up_weight, norm_gain, place ^ r, 1, held)
    for q in line_order[1:]:
        held = gate_sent[q] = block(gate_weight, norm_gain, level ^ q, 0, held)
    for r in plane_order:
        held = down_sent[r] = block(down_weight, None, place ^ r, 1, held)
    held = gate_sent[0] = block(gate_weight, norm_gain, level, 0, held)
    held = up_sent[0] = block(up_weight, norm_gain, place, 1, held)
    held = down_sent[0] = block(down_weight, None, place, 1, held)

    gate_got = {q: line(gate_sent[q], q) for q in line_order}
    up_got = {r: plane(up_sent[r], r) for r in plane_order}
    down_got = {r: plane(down_sent[r], r) for r in plane_order}

    def gathered(own, got, at):
        stage = jnp.zeros((len(got) + 1,) + own.shape, bf16)
        stage = put(stage, own, at, 0)
        for step, piece in got.items():
            stage = put(stage, piece, at ^ step, 0)
        return stage

    up_stage = gathered(up_sent[0], up_got, place)
    up_parts = {q: take(up_stage, level ^ q, 1) for q in [0] + line_order}
    for q in line_order:
        up_parts[q] = line(up_parts[q], q)
    down_stage = gathered(down_sent[0], down_got, place)
    down_parts = [
        {
            q: take(down_stage[..., start : start + size], level ^ q, 1)
            for q in [0] + line_order
        }
        for start, size in chunks
    ]
    for c in range(len(chunks)):
        for q in line_order:
            down_parts[c][q] = line(down_parts[c][q], q)

    column = [payload]
    for q in range(1, depth):
        chosen = payload
        for offset in sorted({(at ^ q) - at for at in range(depth)}):
            other = downs[offset] if offset > 0 else ups[-offset]
            chosen = jnp.where((level ^ q) - level == offset, other, chosen)
        column.append(chosen)
    column = jnp.stack(column)
    column_tokens = column[:, :rows]
    column_notes = column[:, rows:, : 2 * rows].astype(f32)
    column_routes = column_notes[:, :top, :rows]
    column_weights = (
        column_notes[:, top:, :rows]
        + column_notes[:, :top, rows:]
        + column_notes[:, top:, rows:]
    )
    targets = level * inner + jnp.bitwise_xor(place, jnp.arange(inner, dtype=jnp.int32))
    named = column_routes[:, None] == targets.astype(f32)[None, :, None, None]
    member = jnp.any(named, axis=2)
    share = jnp.sum(jnp.where(named, column_weights[:, None], 0.0), axis=2)
    before = (jnp.arange(rows)[:, None] < jnp.arange(rows)[None, :]).astype(bf16)
    position = jnp.einsum("qrs,st->qrt", member.astype(bf16), before, preferred_element_type=f32)
    slots = jnp.arange(capacity, dtype=jnp.int32).astype(f32)
    chosen = member[:, :, None, :] & (position[:, :, None, :] == slots[None, None, :, None])
    picked = jnp.einsum(
        "qrct,qtd->rqcd", chosen.astype(bf16), column_tokens, preferred_element_type=f32
    ).astype(bf16)
    picked = picked.reshape(inner, depth * capacity, width)
    scale = jnp.where(chosen, share[:, :, None, :], 0.0)
    arrived = [picked[0]] + [plane(picked[r], r) for r in plane_order]

    gate_stage = gathered(gate_sent[0], gate_got, level)
    gate_parts = {r: take(gate_stage, place ^ r, 1) for r in [0] + plane_order}
    for r in plane_order:
        gate_parts[r] = plane(gate_parts[r], r)

    arrived = jnp.concatenate(arrived, axis=0)
    arrived = over_tp(arrived)
    squared = sum(
        jnp.sum(jnp.square(x.astype(f32)), axis=1, keepdims=True) for _, x in arrived
    )
    factor = lax.rsqrt(squared / (width * tp) + epsilon)
    normed = [(owner, (x.astype(f32) * factor).astype(bf16)) for owner, x in arrived]
    own = up_parts.pop(0)
    up_ready = gathered(own, up_parts, level).reshape(-1, up_weight.shape[2])
    own = gate_parts.pop(0)
    gate_ready = jnp.zeros((depth, inner) + own.shape[1:], bf16)
    gate_ready = put(gate_ready, own, place, 1)
    for r in plane_order:
        gate_ready = put(gate_ready, gate_parts[r], place ^ r, 1)
    gate_ready = gate_ready.reshape(-1, gate_weight.shape[2])
    hidden = activate(product(normed, gate_ready), product(normed, up_ready)).astype(bf16)
    hidden = over_tp(hidden)
    whole = []
    for owner in range(tp):
        piece = hidden[0][1]
        for other, value in hidden[1:]:
            piece = jnp.where(other == owner, value, piece)
        whole.append(piece)
    whole = jnp.concatenate(whole, axis=1)
    unit = whole.shape[1] // depth
    hidden_order = [0] + line_order
    hidden = jnp.concatenate(
        [lax.dynamic_slice_in_dim(whole, (level ^ q) * unit, unit, 1) for q in hidden_order],
        axis=1,
    )

    backs, held = [], None
    for c, (start, size) in enumerate(chunks):
        matrix = jnp.concatenate(
            [down_parts[c][q].reshape(unit, size) for q in hidden_order], axis=0
        )
        results = jnp.dot(hidden, matrix, preferred_element_type=f32).astype(bf16)
        results = results.reshape(inner, depth * capacity, size)
        backs.append([results[0]] + [plane(results[r], r) for r in plane_order])
    sums = []
    for c, (start, size) in enumerate(chunks):
        if held is not None:
            backs[c][0] = after(backs[c][0], held)
        back = jnp.stack(backs[c]).reshape(inner, depth, capacity, size)
        partial = jnp.einsum(
            "qrct,rqcd->qtd",
            scale,
            back.astype(f32),
            preferred_element_type=f32,
            precision=lax.Precision.HIGHEST,
        )
        leaving = {q: partial[q].astype(bf16) for q in line_order}
        held = leaving
        sums.append([partial[0]] + [line(leaving[q], q).astype(f32) for q in line_order])
    down_ready = []
    for c, (start, size) in enumerate(chunks):
        own = down_parts[c].pop(0)
        down_ready.append(gathered(own, down_parts[c], level).reshape(-1, size))
    down_ready = jnp.concatenate(down_ready, axis=1)
    mixed = []
    for c in range(len(chunks)):
        mixed.append(sum(sums[c]).astype(bf16))
    mixed = jnp.concatenate(mixed, axis=1)
    return (mixed, gate_ready[None], up_ready[None], down_ready[None])


def solution(mesh):
    placed = (
        P("fs", "tp"),
        P("fs"),
        P(None, "fs", "tp"),
        P(None, "fs", "tp"),
        P(None, "fs", "tp"),
        P("fs", None),
        P("fs", None),
    )

    def program(*arrays):
        return jax.shard_map(
            shards,
            mesh=mesh,
            in_specs=placed,
            out_specs=(P("fs", "tp"), P("fs", None, "tp"), P("fs", None, "tp"), P("fs", None, "tp")),
            check_vma=False,
        )(*arrays)

    return program
```

time: 316 us -> 288 us (0.911)
  waiting for transfers between devices: 183 us -> 127 us
  starting transfers between devices: 77.1 us -> 88.6 us
  other arithmetic: 17.7 us -> 28.6 us
  local copies, waits for them, and re-layouts: 19.4 us -> 23.3 us
    ppermute x12 -> x24, starting transfers between devices: 12.3 us -> 49 us  [line(): return lax.ppermute(value, 'fs', [(s, s ^ q * inner) for s in range(count)])]
    ppermute x18 -> x21, waiting for transfers between devices: 79.4 us -> 42.8 us  [plane(): return lax.ppermute(value, 'fs', [(s, s ^ r) for s in range(count)])]
    ppermute x12 -> x0, starting transfers between devices: 27.7 us -> none  [the longest x6 20 us: shards(): upward = lax.ppermute((partial[reach] + upward).astype(bf16), 'fs', lift)]
    ppermute x12 -> x24, waiting for transfers between devices: 98.8 us -> 82.8 us  [line(): return lax.ppermute(value, 'fs', [(s, s ^ q * inner) for s in range(count)])]
    convert_element_type x1 -> x6, other arithmetic: 4.89 us -> 12.9 us  [block(): (part * gain[None, :, None] if gain is not None else part).astype(bf16)]
    ppermute x12 -> x0, waiting for transfers between devices: 4.9 us -> none  [the longest x6 3.24 us: shards(): upward = lax.ppermute((partial[reach] + upward).astype(bf16), 'fs', lift)]
    dot_general x8 -> x4, matrix products: 11.2 us -> 6.5 us  [product(): total = total + jnp.dot(value, rows, preferred_element_type=f32)]
    concatenate x0 -> x2, other arithmetic: none -> 4.52 us  [the longest x1 2.85 us: shards(): whole = jnp.concatenate(whole, axis=1)]
  transfers between devices with their start and end apart: 50 -> 53, of which waited for: 17 -> 20; matrix products, arithmetic and copies ran while one was open for 15% -> 20% of each run, Pallas kernels for 0% -> 0%
where the time goes in v4:
time: 288 us; the launch traced here: 282 us
  waiting for transfers between devices  127 us (44%)
  starting transfers between devices  88.6 us (31%)
  other arithmetic  28.6 us (10%)
  local copies, waits for them, and re-layouts  23.3 us (8%)
  matrix products  12.8 us (4%)
    ppermute x24, waiting for transfers between devices, line(): return lax.ppermute(value, 'fs', [(s, s ^ q * inner) for s in range(count)])  82.8 us
    ppermute x24, starting transfers between devices, line(): return lax.ppermute(value, 'fs', [(s, s ^ q * inner) for s in range(count)])  49 us
    ppermute x21, waiting for transfers between devices, plane(): return lax.ppermute(value, 'fs', [(s, s ^ r) for s in range(count)])  42.8 us
    ppermute x21, starting transfers between devices, plane(): return lax.ppermute(value, 'fs', [(s, s ^ r) for s in range(count)])  25.6 us
    ppermute x6, starting transfers between devices, shift(): return lax.ppermute(value, 'fs', pairs)  13.8 us
    convert_element_type x6, other arithmetic, block(): (part * gain[None, :, None] if gain is not None else part).astype(bf16)  12.9 us
    dynamic_update_slice x29, local copies, waits for them, and re-layouts, put(): return lax.dynamic_update_index_in_dim(array, value, index, axis)  8.98 us
    dot_general x4, matrix products, product(): total = total + jnp.dot(value, rows, preferred_element_type=f32)  6.5 us
  transfers between devices with their start and end apart: 53, of which 20 were waited for; matrix products, arithmetic and copies ran while one was open for 20% of the time, Pallas kernels for 0%

profile of v4, /device:TPU:12, one launch (start us, length us, event | category | flops | bytes accessed | tf_op | source)
XLA Modules:
  0.0 282.3 jit_solution(902543994234885498)
XLA Ops:
  2.0 1.7 pad_maximum_fusion.7
  3.7 2.3 collective-permute-start
  6.1 3.5 %collective-permute-start.1 = (bf16[136,1024]{1,0:T(8,128)(2,1)}, bf16[136,1024]{1,0:T(8,128)(2,1)}, u32[]{:S(2)}, u32[]{:S(2)}) collective-permute-start(bf16[136,1024]{1,0:T(8,128)(2,1)} %pad_maximum_fusion.7), channel_id=1, source_target_pairs={{0,8},{2,10},{4,12},{6,14},{8,16},{10,18},{12,20},{14,22},{16,24},... | collective-permute-start | bytes 835592 | tf_op jit(solution)/shard_map/ppermute | solution.py:99
  9.6 2.2 fusion.26
  12.1 2.2 fusion.25
  14.3 2.1 fusion.24
  16.5 2.2 fusion.23
  18.6 2.1 fusion.22
  20.8 2.2 collective-permute-start.17
  22.9 2.2 fusion.21
  25.1 2.1 fusion.42
  28.7 2.1 fusion.43
  30.8 2.1 fusion.44
  34.4 2.1 fusion.45
  36.5 1.5 broadcast.47.clone.3
  38.1 2.1 fusion.48
  41.9 8.6 %collective-permute-done.16 = bf16[4,128,512]{2,1,0:T(8,128)(2,1)S(1)} collective-permute-done((bf16[4,128,512]{2,1,0:T(8,128)(2,1)}, bf16[4,128,512]{2,1,0:T(8,128)(2,1)S(1)}, u32[]{:S(2)}, u32[]{:S(2)}) %collective-permute-start.16) | collective-permute-done | bytes 524320 | tf_op jit(solution)/shard_map/ppermute | solution.py:86
  51.9 8.5 %collective-permute-done.17 = bf16[4,128,512]{2,1,0:T(8,128)(2,1)S(1)} collective-permute-done((bf16[4,128,512]{2,1,0:T(8,128)(2,1)}, bf16[4,128,512]{2,1,0:T(8,128)(2,1)S(1)}, u32[]{:S(2)}, u32[]{:S(2)}) %collective-permute-start.17) | collective-permute-done | bytes 524320 | tf_op jit(solution)/shard_map/ppermute | solution.py:86
  63.8 1.6 collective-permute-start.12
  65.4 11.0 %collective-permute-done.25 = bf16[4,64,1024]{2,1,0:T(8,128)(2,1)S(1)} collective-permute-done((bf16[4,64,1024]{2,1,0:T(8,128)(2,1)}, bf16[4,64,1024]{2,1,0:T(8,128)(2,1)S(1)}, u32[]{:S(2)}, u32[]{:S(2)}) %collective-permute-start.25) | collective-permute-done | bytes 524320 | tf_op jit(solution)/shard_map/ppermute | solution.py:83
  77.1 1.6 collective-permute-start.10
  78.7 1.9 collective-permute-start.2
  80.6 3.9 %collective-permute-start.3 = (bf16[136,1024]{1,0:T(8,128)(2,1)}, bf16[136,1024]{1,0:T(8,128)(2,1)S(1)}, u32[]{:S(2)}, u32[]{:S(2)}) collective-permute-start(bf16[136,1024]{1,0:T(8,128)(2,1)} %collective-permute-done.1), channel_id=1, source_target_pairs={{8,16},{10,18},{12,20},{14,22},{16,24},{18,26},{20,28},{22,30},{9,... | collective-permute-start | bytes 835592 | tf_op jit(solution)/shard_map/ppermute | solution.py:99
  85.9 1.7 dynamic-slice_bitcast_fusion
  87.7 7.9 %collective-permute-done.10 = bf16[4,128,512]{2,1,0:T(8,128)(2,1)S(1)} collective-permute-done((bf16[4,128,512]{2,1,0:T(8,128)(2,1)S(1)}, bf16[4,128,512]{2,1,0:T(8,128)(2,1)S(1)}, u32[]{:S(2)}, u32[]{:S(2)}) %collective-permute-start.10) | collective-permute-done | bytes 524320 | tf_op jit(solution)/shard_map/ppermute | solution.py:83
  95.6 2.4 collective-permute-start.21
  98.9 5.3 %collective-permute-start.35 = (bf16[4,64,256]{2,1,0:T(8,128)(2,1)S(1)}, bf16[4,64,256]{2,1,0:T(8,128)(2,1)S(1)}, u32[]{:S(2)}, u32[]{:S(2)}) collective-permute-start(bf16[4,64,256]{2,1,0:T(8,128)(2,1)S(1)} %get-tuple-element.67), channel_id=1, source_target_pairs={{0,16},{2,18},{4,20},{6,22},{8,24},{10,26},{12,28},{14,30},{16,0},... | collective-permute-start | bytes 393224 | tf_op jit(solution)/shard_map/ppermute | solution.py:86
  106.0 1.5 dynamic-slice_bitcast_fusion.3
  111.2 1.9 collective-permute-done.4
  117.1 2.0 collective-permute-start.6
  119.2 1.9 collective-permute-start.36
  121.1 3.1 %collective-permute-done.36 = bf16[4,64,256]{2,1,0:T(8,128)(2,1)S(1)} collective-permute-done((bf16[4,64,256]{2,1,0:T(8,128)(2,1)S(1)}, bf16[4,64,256]{2,1,0:T(8,128)(2,1)S(1)}, u32[]{:S(2)}, u32[]{:S(2)}) %collective-permute-start.36) | collective-permute-done | bytes 131104 | tf_op jit(solution)/shard_map/ppermute | solution.py:86
  124.2 7.1 %collective-permute-done.8 = bf16[256,1024]{1,0:T(8,128)(2,1)S(1)} collective-permute-done((bf16[256,1024]{1,0:T(8,128)(2,1)S(1)}, bf16[256,1024]{1,0:T(8,128)(2,1)S(1)}, u32[]{:S(2)}, u32[]{:S(2)}) %collective-permute-start.8) | collective-permute-done | bytes 524320 | tf_op jit(solution)/shard_map/ppermute | solution.py:83
  131.3 6.0 %collective-permute-done.7 = bf16[256,1024]{1,0:T(8,128)(2,1)S(1)} collective-permute-done((bf16[256,1024]{1,0:T(8,128)(2,1)S(1)}, bf16[256,1024]{1,0:T(8,128)(2,1)S(1)}, u32[]{:S(2)}, u32[]{:S(2)}) %collective-permute-start.7) | collective-permute-done | bytes 524320 | tf_op jit(solution)/shard_map/ppermute | solution.py:83
  137.4 2.2 collective-permute-start.37
  140.7 3.0 %collective-permute-start.44 = (bf16[4,64,256]{2,1,0:T(8,128)(2,1)S(1)}, bf16[4,64,256]{2,1,0:T(8,128)(2,1)S(1)}, u32[]{:S(2)}, u32[]{:S(2)}) collective-permute-start(bf16[4,64,256]{2,1,0:T(8,128)(2,1)S(1)} %get-tuple-element.75), channel_id=1, source_target_pairs={{0,16},{2,18},{4,20},{6,22},{8,24},{10,26},{12,28},{14,30},{16,0},... | collective-permute-start | bytes 393224 | tf_op jit(solution)/shard_map/ppermute | solution.py:86
  144.7 2.2 collective-permute-done.44
  148.4 4.3 %collective-permute-done.45 = bf16[4,64,256]{2,1,0:T(8,128)(2,1)S(1)} collective-permute-done((bf16[4,64,256]{2,1,0:T(8,128)(2,1)S(1)}, bf16[4,64,256]{2,1,0:T(8,128)(2,1)S(1)}, u32[]{:S(2)}, u32[]{:S(2)}) %collective-permute-start.45) | collective-permute-done | bytes 131104 | tf_op jit(solution)/shard_map/ppermute | solution.py:86
  152.6 5.8 %collective-permute-start.46 = (bf16[4,64,256]{2,1,0:T(8,128)(2,1)S(1)}, bf16[4,64,256]{2,1,0:T(8,128)(2,1)S(1)}, u32[]{:S(2)}, u32[]{:S(2)}) collective-permute-start(bf16[4,64,256]{2,1,0:T(8,128)(2,1)S(1)} %get-tuple-element.73), channel_id=1, source_target_pairs={{0,8},{2,10},{4,12},{6,14},{8,0},{10,2},{12,4},{14,6},{16,24},{18,... | collective-permute-start | bytes 393224 | tf_op jit(solution)/shard_map/ppermute | solution.py:86
  160.2 3.0 %collective-permute-start.15 = (bf16[4,128,512]{2,1,0:T(8,128)(2,1)S(1)}, bf16[4,128,512]{2,1,0:T(8,128)(2,1)S(1)}, u32[]{:S(2)}, u32[]{:S(2)}) collective-permute-start(bf16[4,128,512]{2,1,0:T(8,128)(2,1)S(1)} %get-tuple-element.36), channel_id=1, source_target_pairs={{0,8},{2,10},{4,12},{6,14},{8,0},{10,2},{12,4},{14,6},{16,24},{18,... | collective-permute-start | bytes 1572872 | tf_op jit(solution)/shard_map/ppermute | solution.py:86
  163.2 26.0 %collective-permute-done.13 = bf16[4,128,512]{2,1,0:T(8,128)(2,1)S(1)} collective-permute-done((bf16[4,128,512]{2,1,0:T(8,128)(2,1)S(1)}, bf16[4,128,512]{2,1,0:T(8,128)(2,1)S(1)}, u32[]{:S(2)}, u32[]{:S(2)}) %collective-permute-start.13) | collective-permute-done | bytes 524320 | tf_op jit(solution)/shard_map/ppermute | solution.py:86
  189.2 3.4 %collective-permute-start.28 = (bf16[4,64,512]{2,1,0:T(8,128)(2,1)S(1)}, bf16[4,64,512]{2,1,0:T(8,128)(2,1)S(1)}, u32[]{:S(2)}, u32[]{:S(2)}) collective-permute-start(bf16[4,64,512]{2,1,0:T(8,128)(2,1)S(1)} %get-tuple-element.52), channel_id=1, source_target_pairs={{0,8},{2,10},{4,12},{6,14},{8,0},{10,2},{12,4},{14,6},{16,24},{18,... | collective-permute-start | bytes 786440 | tf_op jit(solution)/shard_map/ppermute | solution.py:86
  192.6 13.9 %collective-permute-done.14 = bf16[4,128,512]{2,1,0:T(8,128)(2,1)S(1)} collective-permute-done((bf16[4,128,512]{2,1,0:T(8,128)(2,1)S(1)}, bf16[4,128,512]{2,1,0:T(8,128)(2,1)S(1)}, u32[]{:S(2)}, u32[]{:S(2)}) %collective-permute-start.14) | collective-permute-done | bytes 524320 | tf_op jit(solution)/shard_map/ppermute | solution.py:86
  212.3 2.1 multiply_convert_fusion
  214.5 8.3 %collective-permute-done.26 = bf16[4,64,512]{2,1,0:T(8,128)(2,1)S(1)} collective-permute-done((bf16[4,64,512]{2,1,0:T(8,128)(2,1)S(1)}, bf16[4,64,512]{2,1,0:T(8,128)(2,1)S(1)}, u32[]{:S(2)}, u32[]{:S(2)}) %collective-permute-start.26) | collective-permute-done | bytes 262176 | tf_op jit(solution)/shard_map/ppermute | solution.py:86
  222.9 1.6 maximum_bitcast_fusion
  224.7 2.9 %fusion.50 = (bf16[1024,256]{0,1:T(8,128)(2,1)S(1)}, bf16[1024,256]{0,1:T(8,128)(2,1)S(1)}, bf16[1024,256]{0,1:T(8,128)(2,1)S(1)}, bf16[1024,256]{0,1:T(8,128)(2,1)S(1)}) fusion(s32[]{:T(128)S(6)} %select_n.265, bf16[1024,512]{0,1:T(8,128)(2,1)S(1)} %get-tuple-element.35, bf16[1024,512]{0,1:T(8,128)(2,1)S(1)} %get-tuple-element.34, s32[]{:T(128)S(6)} %select_n.266, ...), kind=kLoop, calls=%fused_computation.86 | loop fusion | flops 4194304 | bytes 4194320 | tf_op jit(solution)/shard_map/concatenate | solution.py:216
  227.6 1.5 convolution_convert_fusion
  230.0 2.1 collective-permute-start.40
  232.1 1.6 collective-permute-start.39
  233.7 2.8 %collective-permute-start.31 = (bf16[256,512]{1,0:T(8,128)(2,1)S(1)}, bf16[256,512]{1,0:T(8,128)(2,1)S(1)}, u32[]{:S(2)}, u32[]{:S(2)}) collective-permute-start(bf16[256,512]{1,0:T(8,128)(2,1)S(1)} %get-tuple-element.48), channel_id=1, source_target_pairs={{0,6},{2,4},{4,2},{6,0},{8,14},{10,12},{12,10},{14,8},{16,22},{18,... | collective-permute-start | bytes 786440 | tf_op jit(solution)/shard_map/ppermute | solution.py:83
  238.0 5.8 %collective-permute-done.31 = bf16[256,512]{1,0:T(8,128)(2,1)S(1)} collective-permute-done((bf16[256,512]{1,0:T(8,128)(2,1)S(1)}, bf16[256,512]{1,0:T(8,128)(2,1)S(1)}, u32[]{:S(2)}, u32[]{:S(2)}) %collective-permute-start.31) | collective-permute-done | bytes 262176 | tf_op jit(solution)/shard_map/ppermute | solution.py:83
  245.2 3.8 %collective-permute-done.30 = bf16[256,512]{1,0:T(8,128)(2,1)S(1)} collective-permute-done((bf16[256,512]{1,0:T(8,128)(2,1)S(1)}, bf16[256,512]{1,0:T(8,128)(2,1)S(1)}, u32[]{:S(2)}, u32[]{:S(2)}) %collective-permute-start.30) | collective-permute-done | bytes 262176 | tf_op jit(solution)/shard_map/ppermute | solution.py:83
  249.0 1.7 collective-permute-start.49
  250.6 2.0 collective-permute-start.48
  253.9 2.1 collective-permute-start.33
  256.0 2.7 collective-permute-start.34
  259.5 2.3 collective-permute-start.42
  264.0 2.0 collective-permute-done.42
  266.0 3.3 %collective-permute-start.50 = (bf16[128,256]{1,0:T(8,128)(2,1)S(1)}, bf16[128,256]{1,0:T(8,128)(2,1)S(1)}, u32[]{:S(2)}, u32[]{:S(2)}) collective-permute-start(bf16[128,256]{1,0:T(8,128)(2,1)S(1)} %get-tuple-element.77), channel_id=1, source_target_pairs={{0,16},{2,18},{4,20},{6,22},{8,24},{10,26},{12,28},{14,30},{16,0},... | collective-permute-start | bytes 196616 | tf_op jit(solution)/shard_map/ppermute | solution.py:86
  270.4 1.5 collective-permute-start.51
  272.0 2.5 collective-permute-done.50
  274.5 3.5 %collective-permute-start.32 = (bf16[128,512]{1,0:T(8,128)(2,1)S(1)}, bf16[128,512]{1,0:T(8,128)(2,1)S(1)}, u32[]{:S(2)}, u32[]{:S(2)}) collective-permute-start(bf16[128,512]{1,0:T(8,128)(2,1)S(1)} %get-tuple-element.59), channel_id=1, source_target_pairs={{0,16},{2,18},{4,20},{6,22},{8,24},{10,26},{12,28},{14,30},{16,0},... | collective-permute-start | bytes 393224 | tf_op jit(solution)/shard_map/ppermute | solution.py:86
  278.2 3.3 %collective-permute-done.32 = bf16[128,512]{1,0:T(8,128)(2,1)S(1)} collective-permute-done((bf16[128,512]{1,0:T(8,128)(2,1)S(1)}, bf16[128,512]{1,0:T(8,128)(2,1)S(1)}, u32[]{:S(2)}, u32[]{:S(2)}) %collective-permute-start.32) | collective-permute-done | bytes 131104 | tf_op jit(solution)/shard_map/ppermute | solution.py:86
  (154 shorter events, 44.9 us)
Async XLA Ops:
  0.6 11.5 %copy-start.7 = (f32[128]{0:T(128)S(1)}, f32[128]{0:T(128)}, u32[]{:S(2)}) copy-start(f32[128]{0:T(128)} %param.8) | copy-start | bytes 1540
  3.7 73.4 %collective-permute-start = (bf16[136,1024]{1,0:T(8,128)(2,1)}, bf16[136,1024]{1,0:T(8,128)(2,1)S(1)}, u32[]{:S(2)}, u32[]{:S(2)}) collective-permute-start(bf16[136,1024]{1,0:T(8,128)(2,1)} %pad_maximum_fusion.7), channel_id=1, source_target_pairs={{8,0},{10,2},{12,4},{14,6},{16,8},{18,10},{20,12},{22,14},{24,16},... | collective-permute-start | bytes 835592 | tf_op jit(solution)/shard_map/ppermute | solution.py:99
  6.1 72.6 %collective-permute-start.1 = (bf16[136,1024]{1,0:T(8,128)(2,1)}, bf16[136,1024]{1,0:T(8,128)(2,1)}, u32[]{:S(2)}, u32[]{:S(2)}) collective-permute-start(bf16[136,1024]{1,0:T(8,128)(2,1)} %pad_maximum_fusion.7), channel_id=1, source_target_pairs={{0,8},{2,10},{4,12},{6,14},{8,16},{10,18},{12,20},{14,22},{16,24},... | collective-permute-start | bytes 835592 | tf_op jit(solution)/shard_map/ppermute | solution.py:99
  11.7 38.9 %collective-permute-start.16 = (bf16[4,128,512]{2,1,0:T(8,128)(2,1)}, bf16[4,128,512]{2,1,0:T(8,128)(2,1)S(1)}, u32[]{:S(2)}, u32[]{:S(2)}) collective-permute-start(bf16[4,128,512]{2,1,0:T(8,128)(2,1)} %fusion.26), channel_id=1, source_target_pairs={{0,16},{2,18},{4,20},{6,22},{8,24},{10,26},{12,28},{14,30},{16,0},... | collective-permute-start | bytes 1572872 | tf_op jit(solution)/shard_map/ppermute | solution.py:86
  20.8 39.7 %collective-permute-start.17 = (bf16[4,128,512]{2,1,0:T(8,128)(2,1)}, bf16[4,128,512]{2,1,0:T(8,128)(2,1)S(1)}, u32[]{:S(2)}, u32[]{:S(2)}) collective-permute-start(bf16[4,128,512]{2,1,0:T(8,128)(2,1)} %fusion.22), channel_id=1, source_target_pairs={{0,24},{2,26},{4,28},{6,30},{8,16},{10,18},{12,20},{14,22},{16,8},... | collective-permute-start | bytes 1572872 | tf_op jit(solution)/shard_map/ppermute | solution.py:86
  27.2 35.5 %collective-permute-start.23 = (bf16[4,64,1024]{2,1,0:T(8,128)(2,1)}, bf16[4,64,1024]{2,1,0:T(8,128)(2,1)}, u32[]{:S(2)}, u32[]{:S(2)}) collective-permute-start(bf16[4,64,1024]{2,1,0:T(8,128)(2,1)} %fusion.42), channel_id=1, source_target_pairs={{0,2},{2,0},{4,6},{6,4},{8,10},{10,8},{12,14},{14,12},{16,18},{18,... | collective-permute-start | bytes 1572872 | tf_op jit(solution)/shard_map/ppermute | solution.py:83
  41.9 20.8 %copy-start.6 = (bf16[4,128,512]{2,1,0:T(8,128)(2,1)S(1)}, bf16[4,128,512]{2,1,0:T(8,128)(2,1)}, u32[]{:S(2)}) copy-start(bf16[4,128,512]{2,1,0:T(8,128)(2,1)} %fusion.21) | copy-start | bytes 1572868
  41.9 21.9 %copy-start.3 = (bf16[4,128,512]{2,1,0:T(8,128)(2,1)S(1)}, bf16[4,128,512]{2,1,0:T(8,128)(2,1)}, u32[]{:S(2)}) copy-start(bf16[4,128,512]{2,1,0:T(8,128)(2,1)} %fusion.23) | copy-start | bytes 1572868
  41.9 34.5 %copy-start.4 = (bf16[4,128,512]{2,1,0:T(8,128)(2,1)S(1)}, bf16[4,128,512]{2,1,0:T(8,128)(2,1)}, u32[]{:S(2)}) copy-start(bf16[4,128,512]{2,1,0:T(8,128)(2,1)} %fusion.24) | copy-start | bytes 1572868
  50.6 13.2 %collective-permute-start.24 = (bf16[4,64,1024]{2,1,0:T(8,128)(2,1)}, bf16[4,64,1024]{2,1,0:T(8,128)(2,1)S(1)}, u32[]{:S(2)}, u32[]{:S(2)}) collective-permute-start(bf16[4,64,1024]{2,1,0:T(8,128)(2,1)} %fusion.43), channel_id=1, source_target_pairs={{0,4},{2,6},{4,0},{6,2},{8,12},{10,14},{12,8},{14,10},{16,20},{18,... | collective-permute-start | bytes 1572872 | tf_op jit(solution)/shard_map/ppermute | solution.py:83
  60.4 16.0 %collective-permute-start.25 = (bf16[4,64,1024]{2,1,0:T(8,128)(2,1)}, bf16[4,64,1024]{2,1,0:T(8,128)(2,1)S(1)}, u32[]{:S(2)}, u32[]{:S(2)}) collective-permute-start(bf16[4,64,1024]{2,1,0:T(8,128)(2,1)} %fusion.44), channel_id=1, source_target_pairs={{0,6},{2,4},{4,2},{6,0},{8,14},{10,12},{12,10},{14,8},{16,22},{18,... | collective-permute-start | bytes 1572872 | tf_op jit(solution)/shard_map/ppermute | solution.py:83
  62.7 17.9 %collective-permute-start.18 = (bf16[4,128,512]{2,1,0:T(8,128)(2,1)S(1)}, bf16[4,128,512]{2,1,0:T(8,128)(2,1)S(1)}, u32[]{:S(2)}, u32[]{:S(2)}) collective-permute-start(bf16[4,128,512]{2,1,0:T(8,128)(2,1)S(1)} %copy-done.6), channel_id=1, source_target_pairs={{0,8},{2,10},{4,12},{6,14},{8,0},{10,2},{12,4},{14,6},{16,24},{18,... | collective-permute-start | bytes 1572872 | tf_op jit(solution)/shard_map/ppermute | solution.py:86
  63.8 13.3 %copy-start.5 = (bf16[4,128,512]{2,1,0:T(8,128)(2,1)S(1)}, bf16[4,128,512]{2,1,0:T(8,128)(2,1)}, u32[]{:S(2)}) copy-start(bf16[4,128,512]{2,1,0:T(8,128)(2,1)} %fusion.25) | copy-start | bytes 1572868
  63.8 41.2 %collective-permute-start.12 = (bf16[4,128,512]{2,1,0:T(8,128)(2,1)S(1)}, bf16[4,128,512]{2,1,0:T(8,128)(2,1)S(1)}, u32[]{:S(2)}, u32[]{:S(2)}) collective-permute-start(bf16[4,128,512]{2,1,0:T(8,128)(2,1)S(1)} %copy-done.3), channel_id=1, source_target_pairs={{0,6},{2,4},{4,2},{6,0},{8,14},{10,12},{12,10},{14,8},{16,22},{18,... | collective-permute-start | bytes 1572872 | tf_op jit(solution)/shard_map/ppermute | solution.py:83
  76.4 22.5 %collective-permute-start.11 = (bf16[4,128,512]{2,1,0:T(8,128)(2,1)S(1)}, bf16[4,128,512]{2,1,0:T(8,128)(2,1)S(1)}, u32[]{:S(2)}, u32[]{:S(2)}) collective-permute-start(bf16[4,128,512]{2,1,0:T(8,128)(2,1)S(1)} %copy-done.4), channel_id=1, source_target_pairs={{0,4},{2,6},{4,0},{6,2},{8,12},{10,14},{12,8},{14,10},{16,20},{18,... | collective-permute-start | bytes 1572872 | tf_op jit(solution)/shard_map/ppermute | solution.py:83
  77.1 18.5 %collective-permute-start.10 = (bf16[4,128,512]{2,1,0:T(8,128)(2,1)S(1)}, bf16[4,128,512]{2,1,0:T(8,128)(2,1)S(1)}, u32[]{:S(2)}, u32[]{:S(2)}) collective-permute-start(bf16[4,128,512]{2,1,0:T(8,128)(2,1)S(1)} %copy-done.5), channel_id=1, source_target_pairs={{0,2},{2,0},{4,6},{6,4},{8,10},{10,8},{12,14},{14,12},{16,18},{18,... | collective-permute-start | bytes 1572872 | tf_op jit(solution)/shard_map/ppermute | solution.py:83
  78.7 28.9 %collective-permute-start.2 = (bf16[136,1024]{1,0:T(8,128)(2,1)S(1)}, bf16[136,1024]{1,0:T(8,128)(2,1)S(1)}, u32[]{:S(2)}, u32[]{:S(2)}) collective-permute-start(bf16[136,1024]{1,0:T(8,128)(2,1)S(1)} %collective-permute-done), channel_id=1, source_target_pairs={{8,0},{10,2},{12,4},{14,6},{16,8},{18,10},{20,12},{22,14},{9,1},{1... | collective-permute-start | bytes 835592 | tf_op jit(solution)/shard_map/ppermute | solution.py:99
  80.6 28.4 %collective-permute-start.3 = (bf16[136,1024]{1,0:T(8,128)(2,1)}, bf16[136,1024]{1,0:T(8,128)(2,1)S(1)}, u32[]{:S(2)}, u32[]{:S(2)}) collective-permute-start(bf16[136,1024]{1,0:T(8,128)(2,1)} %collective-permute-done.1), channel_id=1, source_target_pairs={{8,16},{10,18},{12,20},{14,22},{16,24},{18,26},{20,28},{22,30},{9,... | collective-permute-start | bytes 835592 | tf_op jit(solution)/shard_map/ppermute | solution.py:99
  95.6 64.5 %collective-permute-start.21 = (bf16[4,128,512]{2,1,0:T(8,128)(2,1)S(1)}, bf16[4,128,512]{2,1,0:T(8,128)(2,1)S(1)}, u32[]{:S(2)}, u32[]{:S(2)}) collective-permute-start(bf16[4,128,512]{2,1,0:T(8,128)(2,1)S(1)} %get-tuple-element.43), channel_id=1, source_target_pairs={{0,6},{2,4},{4,2},{6,0},{8,14},{10,12},{12,10},{14,8},{16,22},{18,... | collective-permute-start | bytes 1572872 | tf_op jit(solution)/shard_map/ppermute | solution.py:83
  98.9 20.3 %collective-permute-start.35 = (bf16[4,64,256]{2,1,0:T(8,128)(2,1)S(1)}, bf16[4,64,256]{2,1,0:T(8,128)(2,1)S(1)}, u32[]{:S(2)}, u32[]{:S(2)}) collective-permute-start(bf16[4,64,256]{2,1,0:T(8,128)(2,1)S(1)} %get-tuple-element.67), channel_id=1, source_target_pairs={{0,16},{2,18},{4,20},{6,22},{8,24},{10,26},{12,28},{14,30},{16,0},... | collective-permute-start | bytes 393224 | tf_op jit(solution)/shard_map/ppermute | solution.py:86
  107.5 3.5 %copy-start = (bf16[128,1024]{1,0:T(8,128)(2,1)S(1)}, bf16[128,1024]{1,0:T(8,128)(2,1)}, u32[]{:S(2)}) copy-start(bf16[128,1024]{1,0:T(8,128)(2,1)} %param.7) | copy-start | bytes 786436
  107.6 5.5 %collective-permute-start.4 = (bf16[136,1024]{1,0:T(8,128)(2,1)S(1)}, bf16[136,1024]{1,0:T(8,128)(2,1)S(1)}, u32[]{:S(2)}, u32[]{:S(2)}) collective-permute-start(bf16[136,1024]{1,0:T(8,128)(2,1)S(1)} %collective-permute-done.2), channel_id=1, source_target_pairs={{8,0},{10,2},{12,4},{14,6},{9,1},{11,3},{13,5},{15,7}} | collective-permute-start | bytes 835592 | tf_op jit(solution)/shard_map/ppermute | solution.py:99
  109.0 4.0 %collective-permute-start.5 = (bf16[136,1024]{1,0:T(8,128)(2,1)S(1)}, bf16[136,1024]{1,0:T(8,128)(2,1)S(1)}, u32[]{:S(2)}, u32[]{:S(2)}) collective-permute-start(bf16[136,1024]{1,0:T(8,128)(2,1)S(1)} %collective-permute-done.3), channel_id=1, source_target_pairs={{16,24},{18,26},{20,28},{22,30},{17,25},{19,27},{21,29},{23,31}} | collective-permute-start | bytes 835592 | tf_op jit(solution)/shard_map/ppermute | solution.py:99
  115.6 15.8 %collective-permute-start.8 = (bf16[256,1024]{1,0:T(8,128)(2,1)S(1)}, bf16[256,1024]{1,0:T(8,128)(2,1)S(1)}, u32[]{:S(2)}, u32[]{:S(2)}) collective-permute-start(bf16[256,1024]{1,0:T(8,128)(2,1)S(1)} %bitcast.307), channel_id=1, source_target_pairs={{0,6},{2,4},{4,2},{6,0},{8,14},{10,12},{12,10},{14,8},{16,22},{18,... | collective-permute-start | bytes 1572872 | tf_op jit(solution)/shard_map/ppermute | solution.py:83
  115.6 21.7 %collective-permute-start.7 = (bf16[256,1024]{1,0:T(8,128)(2,1)S(1)}, bf16[256,1024]{1,0:T(8,128)(2,1)S(1)}, u32[]{:S(2)}, u32[]{:S(2)}) collective-permute-start(bf16[256,1024]{1,0:T(8,128)(2,1)S(1)} %bitcast.306), channel_id=1, source_target_pairs={{0,4},{2,6},{4,0},{6,2},{8,12},{10,14},{12,8},{14,10},{16,20},{18,... | collective-permute-start | bytes 1572872 | tf_op jit(solution)/shard_map/ppermute | solution.py:83
  117.1 23.6 %collective-permute-start.6 = (bf16[256,1024]{1,0:T(8,128)(2,1)S(1)}, bf16[256,1024]{1,0:T(8,128)(2,1)S(1)}, u32[]{:S(2)}, u32[]{:S(2)}) collective-permute-start(bf16[256,1024]{1,0:T(8,128)(2,1)S(1)} %bitcast.305), channel_id=1, source_target_pairs={{0,2},{2,0},{4,6},{6,4},{8,10},{10,8},{12,14},{14,12},{16,18},{18,... | collective-permute-start | bytes 1572872 | tf_op jit(solution)/shard_map/ppermute | solution.py:83
  119.2 5.0 %collective-permute-start.36 = (bf16[4,64,256]{2,1,0:T(8,128)(2,1)S(1)}, bf16[4,64,256]{2,1,0:T(8,128)(2,1)S(1)}, u32[]{:S(2)}, u32[]{:S(2)}) collective-permute-start(bf16[4,64,256]{2,1,0:T(8,128)(2,1)S(1)} %get-tuple-element.66), channel_id=1, source_target_pairs={{0,24},{2,26},{4,28},{6,30},{8,16},{10,18},{12,20},{14,22},{16,8},... | collective-permute-start | bytes 393224 | tf_op jit(solution)/shard_map/ppermute | solution.py:86
  124.2 34.4 %collective-permute-start.20 = (bf16[4,128,512]{2,1,0:T(8,128)(2,1)S(1)}, bf16[4,128,512]{2,1,0:T(8,128)(2,1)S(1)}, u32[]{:S(2)}, u32[]{:S(2)}) collective-permute-start(bf16[4,128,512]{2,1,0:T(8,128)(2,1)S(1)} %get-tuple-element.44), channel_id=1, source_target_pairs={{0,4},{2,6},{4,0},{6,2},{8,12},{10,14},{12,8},{14,10},{16,20},{18,... | collective-permute-start | bytes 1572872 | tf_op jit(solution)/shard_map/ppermute | solution.py:83
  131.3 27.1 %collective-permute-start.19 = (bf16[4,128,512]{2,1,0:T(8,128)(2,1)S(1)}, bf16[4,128,512]{2,1,0:T(8,128)(2,1)S(1)}, u32[]{:S(2)}, u32[]{:S(2)}) collective-permute-start(bf16[4,128,512]{2,1,0:T(8,128)(2,1)S(1)} %get-tuple-element.45), channel_id=1, source_target_pairs={{0,2},{2,0},{4,6},{6,4},{8,10},{10,8},{12,14},{14,12},{16,18},{18,... | collective-permute-start | bytes 1572872 | tf_op jit(solution)/shard_map/ppermute | solution.py:83
  137.4 7.2 %collective-permute-start.37 = (bf16[4,64,256]{2,1,0:T(8,128)(2,1)S(1)}, bf16[4,64,256]{2,1,0:T(8,128)(2,1)S(1)}, u32[]{:S(2)}, u32[]{:S(2)}) collective-permute-start(bf16[4,64,256]{2,1,0:T(8,128)(2,1)S(1)} %get-tuple-element.65), channel_id=1, source_target_pairs={{0,8},{2,10},{4,12},{6,14},{8,0},{10,2},{12,4},{14,6},{16,24},{18,... | collective-permute-start | bytes 393224 | tf_op jit(solution)/shard_map/ppermute | solution.py:86
  140.7 6.2 %collective-permute-start.44 = (bf16[4,64,256]{2,1,0:T(8,128)(2,1)S(1)}, bf16[4,64,256]{2,1,0:T(8,128)(2,1)S(1)}, u32[]{:S(2)}, u32[]{:S(2)}) collective-permute-start(bf16[4,64,256]{2,1,0:T(8,128)(2,1)S(1)} %get-tuple-element.75), channel_id=1, source_target_pairs={{0,16},{2,18},{4,20},{6,22},{8,24},{10,26},{12,28},{14,30},{16,0},... | collective-permute-start | bytes 393224 | tf_op jit(solution)/shard_map/ppermute | solution.py:86
  144.6 62.8 %collective-permute-start.9 = (bf16[1024,1024]{1,0:T(8,128)(2,1)S(1)}, bf16[1024,1024]{1,0:T(8,128)(2,1)S(1)}, u32[]{:S(2)}, u32[]{:S(2)}) collective-permute-start(bf16[1024,1024]{1,0:T(8,128)(2,1)S(1)} %get-tuple-element.27), channel_id=1, source_target_pairs={{0,1},{1,0},{2,3},{3,2},{4,5},{5,4},{6,7},{7,6},{8,9},{9,8},{10,11... | collective-permute-start | bytes 6291464 | tf_op jit(solution)/shard_map/ppermute | solution.py:50
  146.9 5.7 %collective-permute-start.45 = (bf16[4,64,256]{2,1,0:T(8,128)(2,1)S(1)}, bf16[4,64,256]{2,1,0:T(8,128)(2,1)S(1)}, u32[]{:S(2)}, u32[]{:S(2)}) collective-permute-start(bf16[4,64,256]{2,1,0:T(8,128)(2,1)S(1)} %get-tuple-element.74), channel_id=1, source_target_pairs={{0,24},{2,26},{4,28},{6,30},{8,16},{10,18},{12,20},{14,22},{16,8},... | collective-permute-start | bytes 393224 | tf_op jit(solution)/shard_map/ppermute | solution.py:86
  152.6 61.8 %collective-permute-start.46 = (bf16[4,64,256]{2,1,0:T(8,128)(2,1)S(1)}, bf16[4,64,256]{2,1,0:T(8,128)(2,1)S(1)}, u32[]{:S(2)}, u32[]{:S(2)}) collective-permute-start(bf16[4,64,256]{2,1,0:T(8,128)(2,1)S(1)} %get-tuple-element.73), channel_id=1, source_target_pairs={{0,8},{2,10},{4,12},{6,14},{8,0},{10,2},{12,4},{14,6},{16,24},{18,... | collective-permute-start | bytes 393224 | tf_op jit(solution)/shard_map/ppermute | solution.py:86
  158.5 30.8 %collective-permute-start.13 = (bf16[4,128,512]{2,1,0:T(8,128)(2,1)S(1)}, bf16[4,128,512]{2,1,0:T(8,128)(2,1)S(1)}, u32[]{:S(2)}, u32[]{:S(2)}) collective-permute-start(bf16[4,128,512]{2,1,0:T(8,128)(2,1)S(1)} %get-tuple-element.38), channel_id=1, source_target_pairs={{0,16},{2,18},{4,20},{6,22},{8,24},{10,26},{12,28},{14,30},{16,0},... | collective-permute-start | bytes 1572872 | tf_op jit(solution)/shard_map/ppermute | solution.py:86
  158.6 47.9 %collective-permute-start.14 = (bf16[4,128,512]{2,1,0:T(8,128)(2,1)S(1)}, bf16[4,128,512]{2,1,0:T(8,128)(2,1)S(1)}, u32[]{:S(2)}, u32[]{:S(2)}) collective-permute-start(bf16[4,128,512]{2,1,0:T(8,128)(2,1)S(1)} %get-tuple-element.37), channel_id=1, source_target_pairs={{0,24},{2,26},{4,28},{6,30},{8,16},{10,18},{12,20},{14,22},{16,8},... | collective-permute-start | bytes 1572872 | tf_op jit(solution)/shard_map/ppermute | solution.py:86
  160.2 47.0 %collective-permute-start.15 = (bf16[4,128,512]{2,1,0:T(8,128)(2,1)S(1)}, bf16[4,128,512]{2,1,0:T(8,128)(2,1)S(1)}, u32[]{:S(2)}, u32[]{:S(2)}) collective-permute-start(bf16[4,128,512]{2,1,0:T(8,128)(2,1)S(1)} %get-tuple-element.36), channel_id=1, source_target_pairs={{0,8},{2,10},{4,12},{6,14},{8,0},{10,2},{12,4},{14,6},{16,24},{18,... | collective-permute-start | bytes 1572872 | tf_op jit(solution)/shard_map/ppermute | solution.py:86
  163.2 49.1 %copy-start.1 = (bf16[4,4,128,512]{3,2,1,0:T(8,128)(2,1)}, bf16[4,4,128,512]{3,2,1,0:T(8,128)(2,1)S(1)}, u32[]{:S(2)}) copy-start(bf16[4,4,128,512]{3,2,1,0:T(8,128)(2,1)S(1)} %bitcast_dynamic-update-slice_fusion.3) | copy-start | bytes 6291460
  189.2 33.6 %collective-permute-start.28 = (bf16[4,64,512]{2,1,0:T(8,128)(2,1)S(1)}, bf16[4,64,512]{2,1,0:T(8,128)(2,1)S(1)}, u32[]{:S(2)}, u32[]{:S(2)}) collective-permute-start(bf16[4,64,512]{2,1,0:T(8,128)(2,1)S(1)} %get-tuple-element.52), channel_id=1, source_target_pairs={{0,8},{2,10},{4,12},{6,14},{8,0},{10,2},{12,4},{14,6},{16,24},{18,... | collective-permute-start | bytes 786440 | tf_op jit(solution)/shard_map/ppermute | solution.py:86
  206.5 16.3 %collective-permute-start.27 = (bf16[4,64,512]{2,1,0:T(8,128)(2,1)S(1)}, bf16[4,64,512]{2,1,0:T(8,128)(2,1)S(1)}, u32[]{:S(2)}, u32[]{:S(2)}) collective-permute-start(bf16[4,64,512]{2,1,0:T(8,128)(2,1)S(1)} %get-tuple-element.53), channel_id=1, source_target_pairs={{0,24},{2,26},{4,28},{6,30},{8,16},{10,18},{12,20},{14,22},{16,8},... | collective-permute-start | bytes 786440 | tf_op jit(solution)/shard_map/ppermute | solution.py:86
  207.2 15.6 %collective-permute-start.26 = (bf16[4,64,512]{2,1,0:T(8,128)(2,1)S(1)}, bf16[4,64,512]{2,1,0:T(8,128)(2,1)S(1)}, u32[]{:S(2)}, u32[]{:S(2)}) collective-permute-start(bf16[4,64,512]{2,1,0:T(8,128)(2,1)S(1)} %get-tuple-element.54), channel_id=1, source_target_pairs={{0,16},{2,18},{4,20},{6,22},{8,24},{10,26},{12,28},{14,30},{16,0},... | collective-permute-start | bytes 786440 | tf_op jit(solution)/shard_map/ppermute | solution.py:86
  207.3 2.0 copy-start.2
  214.4 10.2 %collective-permute-start.22 = (bf16[1024,512]{0,1:T(8,128)(2,1)S(1)}, bf16[1024,512]{0,1:T(8,128)(2,1)S(1)}, u32[]{:S(2)}, u32[]{:S(2)}) collective-permute-start(bf16[1024,512]{0,1:T(8,128)(2,1)S(1)} %multiply_convert_fusion), channel_id=1, source_target_pairs={{0,1},{1,0},{2,3},{3,2},{4,5},{5,4},{6,7},{7,6},{8,9},{9,8},{10,11... | collective-permute-start | bytes 3145736 | tf_op jit(solution)/shard_map/ppermute | solution.py:50
  230.0 23.4 %collective-permute-start.40 = (bf16[256,256]{1,0:T(8,128)(2,1)S(1)}, bf16[256,256]{1,0:T(8,128)(2,1)S(1)}, u32[]{:S(2)}, u32[]{:S(2)}) collective-permute-start(bf16[256,256]{1,0:T(8,128)(2,1)S(1)} %get-tuple-element.61), channel_id=1, source_target_pairs={{0,6},{2,4},{4,2},{6,0},{8,14},{10,12},{12,10},{14,8},{16,22},{18,... | collective-permute-start | bytes 393224 | tf_op jit(solution)/shard_map/ppermute | solution.py:83
  232.1 21.7 %collective-permute-start.39 = (bf16[256,256]{1,0:T(8,128)(2,1)S(1)}, bf16[256,256]{1,0:T(8,128)(2,1)S(1)}, u32[]{:S(2)}, u32[]{:S(2)}) collective-permute-start(bf16[256,256]{1,0:T(8,128)(2,1)S(1)} %get-tuple-element.62), channel_id=1, source_target_pairs={{0,4},{2,6},{4,0},{6,2},{8,12},{10,14},{12,8},{14,10},{16,20},{18,... | collective-permute-start | bytes 393224 | tf_op jit(solution)/shard_map/ppermute | solution.py:83
  233.7 10.1 %collective-permute-start.31 = (bf16[256,512]{1,0:T(8,128)(2,1)S(1)}, bf16[256,512]{1,0:T(8,128)(2,1)S(1)}, u32[]{:S(2)}, u32[]{:S(2)}) collective-permute-start(bf16[256,512]{1,0:T(8,128)(2,1)S(1)} %get-tuple-element.48), channel_id=1, source_target_pairs={{0,6},{2,4},{4,2},{6,0},{8,14},{10,12},{12,10},{14,8},{16,22},{18,... | collective-permute-start | bytes 786440 | tf_op jit(solution)/shard_map/ppermute | solution.py:83
  236.6 12.4 %collective-permute-start.30 = (bf16[256,512]{1,0:T(8,128)(2,1)S(1)}, bf16[256,512]{1,0:T(8,128)(2,1)S(1)}, u32[]{:S(2)}, u32[]{:S(2)}) collective-permute-start(bf16[256,512]{1,0:T(8,128)(2,1)S(1)} %get-tuple-element.49), channel_id=1, source_target_pairs={{0,4},{2,6},{4,0},{6,2},{8,12},{10,14},{12,8},{14,10},{16,20},{18,... | collective-permute-start | bytes 786440 | tf_op jit(solution)/shard_map/ppermute | solution.py:83
  236.6 14.1 %collective-permute-start.29 = (bf16[256,512]{1,0:T(8,128)(2,1)S(1)}, bf16[256,512]{1,0:T(8,128)(2,1)S(1)}, u32[]{:S(2)}, u32[]{:S(2)}) collective-permute-start(bf16[256,512]{1,0:T(8,128)(2,1)S(1)} %get-tuple-element.50), channel_id=1, source_target_pairs={{0,2},{2,0},{4,6},{6,4},{8,10},{10,8},{12,14},{14,12},{16,18},{18,... | collective-permute-start | bytes 786440 | tf_op jit(solution)/shard_map/ppermute | solution.py:83
  243.8 12.2 %collective-permute-start.38 = (bf16[256,256]{1,0:T(8,128)(2,1)S(1)}, bf16[256,256]{1,0:T(8,128)(2,1)S(1)}, u32[]{:S(2)}, u32[]{:S(2)}) collective-permute-start(bf16[256,256]{1,0:T(8,128)(2,1)S(1)} %get-tuple-element.63), channel_id=1, source_target_pairs={{0,2},{2,0},{4,6},{6,4},{8,10},{10,8},{12,14},{14,12},{16,18},{18,... | collective-permute-start | bytes 393224 | tf_op jit(solution)/shard_map/ppermute | solution.py:83
  249.0 10.5 %collective-permute-start.49 = (bf16[256,256]{1,0:T(8,128)(2,1)S(1)}, bf16[256,256]{1,0:T(8,128)(2,1)S(1)}, u32[]{:S(2)}, u32[]{:S(2)}) collective-permute-start(bf16[256,256]{1,0:T(8,128)(2,1)S(1)} %get-tuple-element.69), channel_id=1, source_target_pairs={{0,6},{2,4},{4,2},{6,0},{8,14},{10,12},{12,10},{14,8},{16,22},{18,... | collective-permute-start | bytes 393224 | tf_op jit(solution)/shard_map/ppermute | solution.py:83
  250.6 11.1 %collective-permute-start.48 = (bf16[256,256]{1,0:T(8,128)(2,1)S(1)}, bf16[256,256]{1,0:T(8,128)(2,1)S(1)}, u32[]{:S(2)}, u32[]{:S(2)}) collective-permute-start(bf16[256,256]{1,0:T(8,128)(2,1)S(1)} %get-tuple-element.70), channel_id=1, source_target_pairs={{0,4},{2,6},{4,0},{6,2},{8,12},{10,14},{12,8},{14,10},{16,20},{18,... | collective-permute-start | bytes 393224 | tf_op jit(solution)/shard_map/ppermute | solution.py:83
  253.5 9.1 %collective-permute-start.47 = (bf16[256,256]{1,0:T(8,128)(2,1)S(1)}, bf16[256,256]{1,0:T(8,128)(2,1)S(1)}, u32[]{:S(2)}, u32[]{:S(2)}) collective-permute-start(bf16[256,256]{1,0:T(8,128)(2,1)S(1)} %get-tuple-element.71), channel_id=1, source_target_pairs={{0,2},{2,0},{4,6},{6,4},{8,10},{10,8},{12,14},{14,12},{16,18},{18,... | collective-permute-start | bytes 393224 | tf_op jit(solution)/shard_map/ppermute | solution.py:83
  253.9 24.3 %collective-permute-start.33 = (bf16[128,512]{1,0:T(8,128)(2,1)S(1)}, bf16[128,512]{1,0:T(8,128)(2,1)S(1)}, u32[]{:S(2)}, u32[]{:S(2)}) collective-permute-start(bf16[128,512]{1,0:T(8,128)(2,1)S(1)} %get-tuple-element.57), channel_id=1, source_target_pairs={{0,24},{2,26},{4,28},{6,30},{8,16},{10,18},{12,20},{14,22},{16,8},... | collective-permute-start | bytes 393224 | tf_op jit(solution)/shard_map/ppermute | solution.py:86
  256.0 22.2 %collective-permute-start.34 = (bf16[128,512]{1,0:T(8,128)(2,1)S(1)}, bf16[128,512]{1,0:T(8,128)(2,1)S(1)}, u32[]{:S(2)}, u32[]{:S(2)}) collective-permute-start(bf16[128,512]{1,0:T(8,128)(2,1)S(1)} %get-tuple-element.58), channel_id=1, source_target_pairs={{0,8},{2,10},{4,12},{6,14},{8,0},{10,2},{12,4},{14,6},{16,24},{18,... | collective-permute-start | bytes 393224 | tf_op jit(solution)/shard_map/ppermute | solution.py:86
  259.5 6.6 %collective-permute-start.42 = (bf16[128,256]{1,0:T(8,128)(2,1)S(1)}, bf16[128,256]{1,0:T(8,128)(2,1)S(1)}, u32[]{:S(2)}, u32[]{:S(2)}) collective-permute-start(bf16[128,256]{1,0:T(8,128)(2,1)S(1)} %get-tuple-element.80), channel_id=1, source_target_pairs={{0,24},{2,26},{4,28},{6,30},{8,16},{10,18},{12,20},{14,22},{16,8},... | collective-permute-start | bytes 196616 | tf_op jit(solution)/shard_map/ppermute | solution.py:86
  261.7 7.6 %collective-permute-start.43 = (bf16[128,256]{1,0:T(8,128)(2,1)S(1)}, bf16[128,256]{1,0:T(8,128)(2,1)S(1)}, u32[]{:S(2)}, u32[]{:S(2)}) collective-permute-start(bf16[128,256]{1,0:T(8,128)(2,1)S(1)} %get-tuple-element.81), channel_id=1, source_target_pairs={{0,8},{2,10},{4,12},{6,14},{8,0},{10,2},{12,4},{14,6},{16,24},{18,... | collective-permute-start | bytes 196616 | tf_op jit(solution)/shard_map/ppermute | solution.py:86
  262.6 7.8 %collective-permute-start.41 = (bf16[128,256]{1,0:T(8,128)(2,1)S(1)}, bf16[128,256]{1,0:T(8,128)(2,1)S(1)}, u32[]{:S(2)}, u32[]{:S(2)}) collective-permute-start(bf16[128,256]{1,0:T(8,128)(2,1)S(1)} %get-tuple-element.82), channel_id=1, source_target_pairs={{0,16},{2,18},{4,20},{6,22},{8,24},{10,26},{12,28},{14,30},{16,0},... | collective-permute-start | bytes 196616 | tf_op jit(solution)/shard_map/ppermute | solution.py:86
  266.0 8.5 %collective-permute-start.50 = (bf16[128,256]{1,0:T(8,128)(2,1)S(1)}, bf16[128,256]{1,0:T(8,128)(2,1)S(1)}, u32[]{:S(2)}, u32[]{:S(2)}) collective-permute-start(bf16[128,256]{1,0:T(8,128)(2,1)S(1)} %get-tuple-element.77), channel_id=1, source_target_pairs={{0,16},{2,18},{4,20},{6,22},{8,24},{10,26},{12,28},{14,30},{16,0},... | collective-permute-start | bytes 196616 | tf_op jit(solution)/shard_map/ppermute | solution.py:86
  269.4 8.7 %collective-permute-start.52 = (bf16[128,256]{1,0:T(8,128)(2,1)S(1)}, bf16[128,256]{1,0:T(8,128)(2,1)S(1)}, u32[]{:S(2)}, u32[]{:S(2)}) collective-permute-start(bf16[128,256]{1,0:T(8,128)(2,1)S(1)} %get-tuple-element.78), channel_id=1, source_target_pairs={{0,8},{2,10},{4,12},{6,14},{8,0},{10,2},{12,4},{14,6},{16,24},{18,... | collective-permute-start | bytes 196616 | tf_op jit(solution)/shard_map/ppermute | solution.py:86
  270.4 7.7 %collective-permute-start.51 = (bf16[128,256]{1,0:T(8,128)(2,1)S(1)}, bf16[128,256]{1,0:T(8,128)(2,1)S(1)}, u32[]{:S(2)}, u32[]{:S(2)}) collective-permute-start(bf16[128,256]{1,0:T(8,128)(2,1)S(1)} %get-tuple-element.79), channel_id=1, source_target_pairs={{0,24},{2,26},{4,28},{6,30},{8,16},{10,18},{12,20},{14,22},{16,8},... | collective-permute-start | bytes 196616 | tf_op jit(solution)/shard_map/ppermute | solution.py:86
  274.5 7.0 %collective-permute-start.32 = (bf16[128,512]{1,0:T(8,128)(2,1)S(1)}, bf16[128,512]{1,0:T(8,128)(2,1)S(1)}, u32[]{:S(2)}, u32[]{:S(2)}) collective-permute-start(bf16[128,512]{1,0:T(8,128)(2,1)S(1)} %get-tuple-element.59), channel_id=1, source_target_pairs={{0,16},{2,18},{4,20},{6,22},{8,24},{10,26},{12,28},{14,30},{16,0},... | collective-permute-start | bytes 393224 | tf_op jit(solution)/shard_map/ppermute | solution.py:86

commit v5 on v4

--- a/solution.py
+++ b/solution.py
@@ -1,8 +1,11 @@
+import functools
 import math
 
 import jax
 import jax.numpy as jnp
 from jax import lax
+from jax.experimental import pallas as pl
+from jax.experimental.pallas import tpu as pltpu
 from jax.sharding import PartitionSpec as P
 
 
@@ -30,8 +33,9 @@
 
 
 def chunks_of(width):
-    unit = width // 4
-    return [(0, 2 * unit), (2 * unit, unit), (3 * unit, width - 3 * unit)]
+    unit = max(width // 4, math.gcd(width, 128))
+    first = max(width // 2, unit)
+    return [(0, first)] + [(at, unit) for at in range(first, width, unit)]
 
 
 def far_first(depth):
@@ -43,21 +47,130 @@
 
 
 def over_tp(value):
-    size, mine = lax.axis_size("tp"), lax.axis_index("tp")
-    blocks = [(mine, value)]
+    size = lax.axis_size("tp")
+    blocks = [value]
     for j in range(1, size):
         pairs = [(s, (s + j) % size) for s in range(size)]
-        blocks.append(((mine - j) % size, lax.ppermute(value, "tp", pairs)))
+        blocks.append(lax.ppermute(value, "tp", pairs))
     return blocks
 
 
-def product(blocks, matrix):
-    total = 0.0
-    for owner, value in blocks:
-        depth = value.shape[1]
-        rows = lax.dynamic_slice_in_dim(matrix, owner * depth, depth, 0)
-        total = total + jnp.dot(value, rows, preferred_element_type=f32)
-    return total
+def spot(index, size):
+    return pl.ds(pl.multiple_of(index * size, size), size)
+
+
+def hidden_kernel(inner, depth, tp, line_order, *refs):
+    at, refs = refs[0], list(refs[1:])
+    level, place, mine = at[0], at[1], at[2]
+    xs, refs = refs[:tp], refs[tp:]
+    gates, refs = refs[:inner], refs[inner:]
+    ups, refs = refs[:depth], refs[depth:]
+    hidden, gate_out, up_out, gate, up, sems = refs
+    block = gates[0].shape[1]
+    for r in range(inner):
+        for level_at in range(depth):
+            gate[spot(level_at * inner + (place ^ r), block), :] = gates[r][level_at]
+    for q, piece in zip([0] + line_order, ups):
+        rows = piece.shape[0] * piece.shape[1]
+        up[spot(level ^ q, rows), :] = piece[...].reshape(rows, piece.shape[2])
+    width = xs[0].shape[1]
+    tile = math.gcd(xs[0].shape[0], 256)
+
+    @pl.loop(0, xs[0].shape[0] // tile)
+    def _(step):
+        rows = spot(step, tile)
+        squared = 0.0
+        for x in xs:
+            value = x[rows, :].astype(f32)
+            squared = squared + jnp.sum(value * value, axis=1, keepdims=True)
+        factor = lax.rsqrt(squared / (width * tp) + epsilon)
+        gate_pre, up_pre = 0.0, 0.0
+        for j, x in enumerate(xs):
+            normed = (x[rows, :].astype(f32) * factor).astype(bf16)
+            held = spot(lax.rem(mine - j + tp, tp), width)
+            gate_pre = gate_pre + jnp.dot(normed, gate[held, :], preferred_element_type=f32)
+            up_pre = up_pre + jnp.dot(normed, up[held, :], preferred_element_type=f32)
+        hidden[rows, :] = activate(gate_pre, up_pre).astype(bf16)
+
+    copies = [
+        pltpu.make_async_copy(gate, gate_out, sems.at[0]),
+        pltpu.make_async_copy(up, up_out, sems.at[1]),
+    ]
+    for copy in copies:
+        copy.start()
+    for copy in copies:
+        copy.wait()
+
+
+def hidden_call(where, xs, gates, ups, line_order, depth_rows):
+    inner, depth, tp = len(gates), len(ups), len(xs)
+    columns = gates[0].shape[2]
+    rows = xs[0].shape[0]
+    vmem = pl.BlockSpec(memory_space=pltpu.VMEM)
+    matrix = jax.ShapeDtypeStruct((depth_rows, columns), bf16)
+    return pl.pallas_call(
+        functools.partial(hidden_kernel, inner, depth, tp, line_order),
+        out_shape=(jax.ShapeDtypeStruct((rows, columns), bf16), matrix, matrix),
+        in_specs=[pl.BlockSpec(memory_space=pltpu.SMEM)] + [vmem] * (tp + inner + depth),
+        out_specs=(vmem, pl.BlockSpec(memory_space=pl.ANY), pl.BlockSpec(memory_space=pl.ANY)),
+        scratch_shapes=[
+            pltpu.VMEM((depth_rows, columns), bf16),
+            pltpu.VMEM((depth_rows, columns), bf16),
+            pltpu.SemaphoreType.DMA((2,)),
+        ],
+        compiler_params=pltpu.CompilerParams(vmem_limit_bytes=28 << 20),
+        cost_estimate=pl.CostEstimate(
+            flops=4 * rows * depth_rows * columns,
+            bytes_accessed=4 * rows * depth_rows,
+            transcendentals=rows * columns,
+        ),
+        name="hidden",
+    )(where, *xs, *gates, *ups)
+
+
+def result_kernel(inner, depth, tp, line_order, start, again, *refs):
+    at, refs = refs[0], list(refs[1:])
+    level, mine = at[0], at[2]
+    hiddens, refs = refs[:tp], refs[tp:]
+    parts, refs = refs[:depth], refs[depth + again :]
+    results, (down_out, matrix, sem) = refs[:inner], refs[inner:]
+    for q, part in zip([0] + line_order, parts):
+        rows = part.shape[0] * part.shape[1]
+        matrix[spot(level ^ q, rows), :] = part[...].reshape(rows, part.shape[2])
+    width, rows = hiddens[0].shape[1], results[0].shape[0]
+    for r in range(inner):
+        total = 0.0
+        for j, hidden in enumerate(hiddens):
+            held = matrix[spot(lax.rem(mine - j + tp, tp), width), :]
+            total = total + jnp.dot(
+                hidden[pl.ds(r * rows, rows), :], held, preferred_element_type=f32
+            )
+        results[r][...] = total.astype(bf16)
+    copy = pltpu.make_async_copy(matrix, down_out.at[:, pl.ds(start, matrix.shape[1])], sem)
+    copy.start()
+    copy.wait()
+
+
+def result_call(where, hiddens, parts, before, start, full, inner, line_order):
+    depth, tp = len(parts), len(hiddens)
+    rows, columns = hiddens[0].shape[0], parts[0].shape[2]
+    vmem, anywhere = (pl.BlockSpec(memory_space=m) for m in (pltpu.VMEM, pl.ANY))
+    again = int(before is not None)
+    piece = jax.ShapeDtypeStruct((rows // inner, columns), bf16)
+    return pl.pallas_call(
+        functools.partial(result_kernel, inner, depth, tp, line_order, start, again),
+        out_shape=(piece,) * inner + (jax.ShapeDtypeStruct(full, bf16),),
+        in_specs=[pl.BlockSpec(memory_space=pltpu.SMEM)]
+        + [vmem] * (tp + depth)
+        + [anywhere] * again,
+        out_specs=(vmem,) * inner + (anywhere,),
+        scratch_shapes=[pltpu.VMEM((full[0], columns), bf16), pltpu.SemaphoreType.DMA],
+        input_output_aliases={1 + tp + depth: inner} if again else {},
+        compiler_params=pltpu.CompilerParams(vmem_limit_bytes=16 << 20),
+        cost_estimate=pl.CostEstimate(
+            flops=2 * rows * full[0] * columns, bytes_accessed=4 * rows * columns, transcendentals=0
+        ),
+    )(where, *hiddens, *parts, *([before] if again else []))
 
 
 def take(array, index, axis):
@@ -192,42 +305,29 @@
 
     arrived = jnp.concatenate(arrived, axis=0)
     arrived = over_tp(arrived)
-    squared = sum(
-        jnp.sum(jnp.square(x.astype(f32)), axis=1, keepdims=True) for _, x in arrived
+    spots = jnp.stack([level, place, lax.axis_index("tp")]).astype(jnp.int32)
+    hidden, gate_ready, up_ready = hidden_call(
+        spots,
+        arrived,
+        [gate_parts[r] for r in [0] + plane_order],
+        [up_parts[q] for q in [0] + line_order],
+        line_order,
+        width * tp,
     )
-    factor = lax.rsqrt(squared / (width * tp) + epsilon)
-    normed = [(owner, (x.astype(f32) * factor).astype(bf16)) for owner, x in arrived]
-    own = up_parts.pop(0)
-    up_ready = gathered(own, up_parts, level).reshape(-1, up_weight.shape[2])
-    own = gate_parts.pop(0)
-    gate_ready = jnp.zeros((depth, inner) + own.shape[1:], bf16)
-    gate_ready = put(gate_ready, own, place, 1)
-    for r in plane_order:
-        gate_ready = put(gate_ready, gate_parts[r], place ^ r, 1)
-    gate_ready = gate_ready.reshape(-1, gate_weight.shape[2])
-    hidden = activate(product(normed, gate_ready), product(normed, up_ready)).astype(bf16)
     hidden = over_tp(hidden)
-    whole = []
-    for owner in range(tp):
-        piece = hidden[0][1]
-        for other, value in hidden[1:]:
-            piece = jnp.where(other == owner, value, piece)
-        whole.append(piece)
-    whole = jnp.concatenate(whole, axis=1)
-    unit = whole.shape[1] // depth
-    hidden_order = [0] + line_order
-    hidden = jnp.concatenate(
-        [lax.dynamic_slice_in_dim(whole, (level ^ q) * unit, unit, 1) for q in hidden_order],
-        axis=1,
-    )
-
-    backs, held = [], None
+
+    backs, held, down_ready = [], None, None
     for c, (start, size) in enumerate(chunks):
-        matrix = jnp.concatenate(
-            [down_parts[c][q].reshape(unit, size) for q in hidden_order], axis=0
+        *results, down_ready = result_call(
+            spots,
+            hidden,
+            [down_parts[c][q] for q in [0] + line_order],
+            down_ready,
+            start,
+            (hidden[0].shape[1] * tp, width),
+            inner,
+            line_order,
         )
-        results = jnp.dot(hidden, matrix, preferred_element_type=f32).astype(bf16)
-        results = results.reshape(inner, depth * capacity, size)
         backs.append([results[0]] + [plane(results[r], r) for r in plane_order])
     sums = []
     for c, (start, size) in enumerate(chunks):
@@ -244,11 +344,6 @@
         leaving = {q: partial[q].astype(bf16) for q in line_order}
         held = leaving
         sums.append([partial[0]] + [line(leaving[q], q).astype(f32) for q in line_order])
-    down_ready = []
-    for c, (start, size) in enumerate(chunks):
-        own = down_parts[c].pop(0)
-        down_ready.append(gathered(own, down_parts[c], level).reshape(-1, size))
-    down_ready = jnp.concatenate(down_ready, axis=1)
     mixed = []
     for c in range(len(chunks)):
         mixed.append(sum(sums[c]).astype(bf16))
@@ -268,12 +363,13 @@
     )
 
     def program(*arrays):
-        return jax.shard_map(
+        step = jax.shard_map(
             shards,
             mesh=mesh,
             in_specs=placed,
             out_specs=(P("fs", "tp"), P("fs", None, "tp"), P("fs", None, "tp"), P("fs", None, "tp")),
             check_vma=False,
-        )(*arrays)
+        )
+        return step(*arrays)
 
     return program

time: 288 us -> 289 us (level)
  Pallas kernels: 0 us -> 15.6 us
  matrix products: 12.8 us -> 3.16 us
  waiting for transfers between devices: 127 us -> 135 us
  other arithmetic: 28.6 us -> 22.1 us
    ppermute x6, waiting for transfers between devices: 1.89 us -> 29.8 us  [shift(): return lax.ppermute(value, 'fs', pairs)]
    ppermute x24, waiting for transfers between devices: 82.8 us -> 61.1 us  [line(): return lax.ppermute(value, 'fs', [(s, s ^ q * inner) for s in range(count)])]
    pallas_call x0 -> x4, Pallas kernels: none -> 15.6 us  [the longest x1 9.36 us: hidden_call(): pl.pallas_call(functools.partial(hidden_kernel, inner, depth, tp, line_or...]
    dot_general x7 -> x0, matrix products: 9.58 us -> none  [the longest x4 6.5 us: product(): total = total + jnp.dot(value, rows, preferred_element_type=f32)]
    ppermute x24, starting transfers between devices: 49 us -> 43.2 us  [line(): return lax.ppermute(value, 'fs', [(s, s ^ q * inner) for s in range(count)])]
    dynamic_update_slice x29 -> x10, local copies, waits for them, and re-layouts: 8.98 us -> 5.24 us  [put(): return lax.dynamic_update_index_in_dim(array, value, index, axis)]
  transfers between devices with their start and end apart: 53 -> 53, of which waited for: 20 -> 23; matrix products, arithmetic and copies ran while one was open for 20% -> 14% of each run, Pallas kernels for 0% -> 5%
where the time goes in v5:
time: 289 us; the launch traced here: 284 us
  waiting for transfers between devices  135 us (47%)
  starting transfers between devices  86.2 us (30%)
  other arithmetic  22.1 us (8%)
  local copies, waits for them, and re-layouts  20.8 us (7%)
  Pallas kernels  15.6 us (5%)
  matrix products  3.16 us (1%)
    ppermute x24, waiting for transfers between devices, line(): return lax.ppermute(value, 'fs', [(s, s ^ q * inner) for s in range(count)])  61.1 us
    ppermute x21, waiting for transfers between devices, plane(): return lax.ppermute(value, 'fs', [(s, s ^ r) for s in range(count)])  44.2 us
    ppermute x24, starting transfers between devices, line(): return lax.ppermute(value, 'fs', [(s, s ^ q * inner) for s in range(count)])  43.2 us
    ppermute x6, waiting for transfers between devices, shift(): return lax.ppermute(value, 'fs', pairs)  29.8 us
    ppermute x21, starting transfers between devices, plane(): return lax.ppermute(value, 'fs', [(s, s ^ r) for s in range(count)])  26.3 us
    ppermute x6, starting transfers between devices, shift(): return lax.ppermute(value, 'fs', pairs)  16.6 us
    convert_element_type x6, other arithmetic, block(): (part * gain[None, :, None] if gain is not None else part).astype(bf16)  13 us
    pallas_call x1, Pallas kernels, hidden_call(): pl.pallas_call(functools.partial(hidden_kernel, inner, depth, tp, line_or...  9.36 us
  transfers between devices with their start and end apart: 53, of which 23 were waited for; matrix products, arithmetic and copies ran while one was open for 14% of the time, Pallas kernels for 5%

profile of v5, /device:TPU:12, one launch (start us, length us, event | category | flops | bytes accessed | tf_op | source)
XLA Modules:
  0.0 284.1 jit_solution(1939629548792209021)
XLA Ops:
  3.0 2.4 collective-permute-start
  5.4 3.5 %collective-permute-start.1 = (bf16[136,1024]{1,0:T(8,128)(2,1)S(1)}, bf16[136,1024]{1,0:T(8,128)(2,1)S(1)}, u32[]{:S(2)}, u32[]{:S(2)}) collective-permute-start(bf16[136,1024]{1,0:T(8,128)(2,1)S(1)} %pad_maximum_fusion.6), channel_id=1, source_target_pairs={{0,8},{2,10},{4,12},{6,14},{8,16},{10,18},{12,20},{14,22},{16,24},... | collective-permute-start | bytes 835592 | tf_op jit(solution)/shard_map/ppermute | solution.py:212
  8.9 2.2 fusion.17
  11.5 2.2 fusion.16
  13.6 2.2 fusion.15
  15.8 2.2 fusion.14
  18.0 2.2 fusion.13
  20.1 1.5 collective-permute-start.11
  21.6 2.2 fusion.12
  23.8 2.1 fusion.22
  25.9 4.4 %collective-permute-start.2 = (bf16[136,1024]{1,0:T(8,128)(2,1)S(1)}, bf16[136,1024]{1,0:T(8,128)(2,1)S(1)}, u32[]{:S(2)}, u32[]{:S(2)}) collective-permute-start(bf16[136,1024]{1,0:T(8,128)(2,1)S(1)} %collective-permute-done), channel_id=1, source_target_pairs={{8,0},{10,2},{12,4},{14,6},{16,8},{18,10},{20,12},{22,14},{9,1},{1... | collective-permute-start | bytes 835592 | tf_op jit(solution)/shard_map/ppermute | solution.py:212
  30.3 8.1 %collective-permute-done.1 = bf16[136,1024]{1,0:T(8,128)(2,1)S(1)} collective-permute-done((bf16[136,1024]{1,0:T(8,128)(2,1)S(1)}, bf16[136,1024]{1,0:T(8,128)(2,1)S(1)}, u32[]{:S(2)}, u32[]{:S(2)}) %collective-permute-start.1) | collective-permute-done | bytes 278560 | tf_op jit(solution)/shard_map/ppermute | solution.py:212
  38.4 4.4 %collective-permute-start.3 = (bf16[136,1024]{1,0:T(8,128)(2,1)S(1)}, bf16[136,1024]{1,0:T(8,128)(2,1)S(1)}, u32[]{:S(2)}, u32[]{:S(2)}) collective-permute-start(bf16[136,1024]{1,0:T(8,128)(2,1)S(1)} %collective-permute-done.1), channel_id=1, source_target_pairs={{8,16},{10,18},{12,20},{14,22},{16,24},{18,26},{20,28},{22,30},{9,... | collective-permute-start | bytes 835592 | tf_op jit(solution)/shard_map/ppermute | solution.py:212
  42.8 2.1 fusion.23
  44.9 2.1 fusion.24
  47.0 17.2 %collective-permute-done.2 = bf16[136,1024]{1,0:T(8,128)(2,1)S(1)} collective-permute-done((bf16[136,1024]{1,0:T(8,128)(2,1)S(1)}, bf16[136,1024]{1,0:T(8,128)(2,1)S(1)}, u32[]{:S(2)}, u32[]{:S(2)}) %collective-permute-start.2) | collective-permute-done | bytes 278560 | tf_op jit(solution)/shard_map/ppermute | solution.py:212
  64.3 1.3 collective-permute-start.4
  66.5 4.4 %collective-permute-done.4 = bf16[136,1024]{1,0:T(8,128)(2,1)S(1)} collective-permute-done((bf16[136,1024]{1,0:T(8,128)(2,1)S(1)}, bf16[136,1024]{1,0:T(8,128)(2,1)S(1)}, u32[]{:S(2)}, u32[]{:S(2)}) %collective-permute-start.4) | collective-permute-done | bytes 278560 | tf_op jit(solution)/shard_map/ppermute | solution.py:212
  73.4 1.4 collective-permute-start.8
  74.8 1.5 collective-permute-start.7
  77.1 1.4 fusion.25
  78.4 1.5 broadcast.29.clone.1
  80.0 2.1 fusion.21
  82.1 2.5 collective-permute-start.12
  84.7 4.7 %collective-permute-done.8 = bf16[256,1024]{1,0:T(8,128)(2,1)} collective-permute-done((bf16[256,1024]{1,0:T(8,128)(2,1)}, bf16[256,1024]{1,0:T(8,128)(2,1)}, u32[]{:S(2)}, u32[]{:S(2)}) %collective-permute-start.8) | collective-permute-done | bytes 524320 | tf_op jit(solution)/shard_map/ppermute | solution.py:196
  89.4 1.5 collective-permute-start.16
  90.9 7.2 %collective-permute-done.7 = bf16[256,1024]{1,0:T(8,128)(2,1)} collective-permute-done((bf16[256,1024]{1,0:T(8,128)(2,1)}, bf16[256,1024]{1,0:T(8,128)(2,1)}, u32[]{:S(2)}, u32[]{:S(2)}) %collective-permute-start.7) | collective-permute-done | bytes 524320 | tf_op jit(solution)/shard_map/ppermute | solution.py:196
  99.9 2.2 collective-permute-start.18
  102.1 1.7 pad_maximum_fusion.refs_1_
  106.9 4.2 %collective-permute-done.16 = bf16[4,128,512]{2,1,0:T(8,128)(2,1)S(1)} collective-permute-done((bf16[4,128,512]{2,1,0:T(8,128)(2,1)}, bf16[4,128,512]{2,1,0:T(8,128)(2,1)S(1)}, u32[]{:S(2)}, u32[]{:S(2)}) %collective-permute-start.16) | collective-permute-done | bytes 524320 | tf_op jit(solution)/shard_map/ppermute | solution.py:196
  113.1 10.3 %collective-permute-done.17 = bf16[4,128,512]{2,1,0:T(8,128)(2,1)S(1)} collective-permute-done((bf16[4,128,512]{2,1,0:T(8,128)(2,1)}, bf16[4,128,512]{2,1,0:T(8,128)(2,1)S(1)}, u32[]{:S(2)}, u32[]{:S(2)}) %collective-permute-start.17) | collective-permute-done | bytes 524320 | tf_op jit(solution)/shard_map/ppermute | solution.py:196
  127.2 2.7 dynamic-slice_bitcast_fusion
  129.9 3.7 %collective-permute-done.23 = bf16[4,64,1024]{2,1,0:T(8,128)(2,1)S(1)} collective-permute-done((bf16[4,64,1024]{2,1,0:T(8,128)(2,1)}, bf16[4,64,1024]{2,1,0:T(8,128)(2,1)S(1)}, u32[]{:S(2)}, u32[]{:S(2)}) %collective-permute-start.23) | collective-permute-done | bytes 524320 | tf_op jit(solution)/shard_map/ppermute | solution.py:196
  133.6 5.1 %collective-permute-start.19 = (bf16[4,128,512]{2,1,0:T(8,128)(2,1)}, bf16[4,128,512]{2,1,0:T(8,128)(2,1)}, u32[]{:S(2)}, u32[]{:S(2)}) collective-permute-start(bf16[4,128,512]{2,1,0:T(8,128)(2,1)} %get-tuple-element.66), channel_id=1, source_target_pairs={{0,16},{2,18},{4,20},{6,22},{8,24},{10,26},{12,28},{14,30},{16,0},... | collective-permute-start | bytes 1572872 | tf_op jit(solution)/shard_map/ppermute | solution.py:199
  138.6 6.2 %collective-permute-done.13.refs_4_ = bf16[4,128,512]{2,1,0:T(8,128)(2,1)S(1)} collective-permute-done((bf16[4,128,512]{2,1,0:T(8,128)(2,1)S(1)}, bf16[4,128,512]{2,1,0:T(8,128)(2,1)S(1)}, u32[]{:S(2)}, u32[]{:S(2)}) %collective-permute-start.13) | collective-permute-done | bytes 524320 | tf_op jit(solution)/shard_map/ppermute | solution.py:196
  145.6 3.1 %collective-permute-start.20 = (bf16[4,128,512]{2,1,0:T(8,128)(2,1)}, bf16[4,128,512]{2,1,0:T(8,128)(2,1)}, u32[]{:S(2)}, u32[]{:S(2)}) collective-permute-start(bf16[4,128,512]{2,1,0:T(8,128)(2,1)} %get-tuple-element.65), channel_id=1, source_target_pairs={{0,24},{2,26},{4,28},{6,30},{8,16},{10,18},{12,20},{14,22},{16,8},... | collective-permute-start | bytes 1572872 | tf_op jit(solution)/shard_map/ppermute | solution.py:199
  149.5 3.4 %collective-permute-start.21 = (bf16[4,128,512]{2,1,0:T(8,128)(2,1)}, bf16[4,128,512]{2,1,0:T(8,128)(2,1)}, u32[]{:S(2)}, u32[]{:S(2)}) collective-permute-start(bf16[4,128,512]{2,1,0:T(8,128)(2,1)} %get-tuple-element.64), channel_id=1, source_target_pairs={{0,8},{2,10},{4,12},{6,14},{8,0},{10,2},{12,4},{14,6},{16,24},{18,... | collective-permute-start | bytes 1572872 | tf_op jit(solution)/shard_map/ppermute | solution.py:199
  153.3 1.5 fusion.27
  154.8 1.5 collective-permute-start.24
  156.4 10.9 %collective-permute-done.19.refs_8_ = bf16[4,128,512]{2,1,0:T(8,128)(2,1)} collective-permute-done((bf16[4,128,512]{2,1,0:T(8,128)(2,1)}, bf16[4,128,512]{2,1,0:T(8,128)(2,1)}, u32[]{:S(2)}, u32[]{:S(2)}) %collective-permute-start.19) | collective-permute-done | bytes 524320 | tf_op jit(solution)/shard_map/ppermute | solution.py:199
  167.2 2.4 collective-permute-start.25
  169.6 9.2 %collective-permute-done.20.refs_9_ = bf16[4,128,512]{2,1,0:T(8,128)(2,1)} collective-permute-done((bf16[4,128,512]{2,1,0:T(8,128)(2,1)}, bf16[4,128,512]{2,1,0:T(8,128)(2,1)}, u32[]{:S(2)}, u32[]{:S(2)}) %collective-permute-start.20) | collective-permute-done | bytes 524320 | tf_op jit(solution)/shard_map/ppermute | solution.py:199
  178.8 9.4 %hidden.1 = (bf16[1024,512]{1,0:T(8,128)(2,1)S(1)}, bf16[2048,512]{1,0:T(8,128)(2,1)}, bf16[2048,512]{1,0:T(8,128)(2,1)}) custom-call(s32[3]{0:T(128)S(1)} %pad_add_fusion.refs_0_, bf16[1024,1024]{1,0:T(8,128)(2,1)S(1)} %pad_maximum_fusion.refs_1_, bf16[1024,1024]{1,0:T(8,128)(2,1)} %collective-permute-done.9.refs_2_, ...), custom_call_target="tpu_custom_call" | custom-call | flops 4294967296 | bytes 8388608 | tf_op jit(solution)/shard_map/hidden/pallas_call | solution.py:111
  188.6 2.0 collective-permute-start.26
  191.8 1.5 collective-permute-start.28
  194.5 13.9 %collective-permute-done.26.refs_4_ = bf16[4,64,512]{2,1,0:T(8,128)(2,1)S(1)} collective-permute-done((bf16[4,64,512]{2,1,0:T(8,128)(2,1)S(1)}, bf16[4,64,512]{2,1,0:T(8,128)(2,1)S(1)}, u32[]{:S(2)}, u32[]{:S(2)}) %collective-permute-start.26) | collective-permute-done | bytes 262176 | tf_op jit(solution)/shard_map/ppermute | solution.py:199
  208.4 3.8 %collective-permute-start.35 = (bf16[4,64,256]{2,1,0:T(8,128)(2,1)S(1)}, bf16[4,64,256]{2,1,0:T(8,128)(2,1)S(1)}, u32[]{:S(2)}, u32[]{:S(2)}) collective-permute-start(bf16[4,64,256]{2,1,0:T(8,128)(2,1)S(1)} %get-tuple-element.87), channel_id=1, source_target_pairs={{0,16},{2,18},{4,20},{6,22},{8,24},{10,26},{12,28},{14,30},{16,0},... | collective-permute-start | bytes 393224 | tf_op jit(solution)/shard_map/ppermute | solution.py:199
  212.2 11.5 %collective-permute-done.27.refs_5_ = bf16[4,64,512]{2,1,0:T(8,128)(2,1)S(1)} collective-permute-done((bf16[4,64,512]{2,1,0:T(8,128)(2,1)S(1)}, bf16[4,64,512]{2,1,0:T(8,128)(2,1)S(1)}, u32[]{:S(2)}, u32[]{:S(2)}) %collective-permute-start.27) | collective-permute-done | bytes 262176 | tf_op jit(solution)/shard_map/ppermute | solution.py:199
  224.8 2.6 shard_map.102
  227.4 2.5 collective-permute-start.31
  233.2 1.7 collective-permute-start.46
  234.9 1.8 shard_map.103
  236.8 3.2 %collective-permute-done.45.refs_5_ = bf16[4,64,256]{2,1,0:T(8,128)(2,1)S(1)} collective-permute-done((bf16[4,64,256]{2,1,0:T(8,128)(2,1)S(1)}, bf16[4,64,256]{2,1,0:T(8,128)(2,1)S(1)}, u32[]{:S(2)}, u32[]{:S(2)}) %collective-permute-start.45) | collective-permute-done | bytes 131104 | tf_op jit(solution)/shard_map/ppermute | solution.py:199
  240.1 1.8 shard_map.104
  242.0 2.0 collective-permute-start.49
  244.5 2.0 collective-permute-start.40
  248.9 3.3 %collective-permute-done.40 = bf16[256,256]{1,0:T(8,128)(2,1)S(1)} collective-permute-done((bf16[256,256]{1,0:T(8,128)(2,1)S(1)}, bf16[256,256]{1,0:T(8,128)(2,1)S(1)}, u32[]{:S(2)}, u32[]{:S(2)}) %collective-permute-start.40) | collective-permute-done | bytes 131104 | tf_op jit(solution)/shard_map/ppermute | solution.py:196
  252.8 3.8 %collective-permute-done.39 = bf16[256,256]{1,0:T(8,128)(2,1)S(1)} collective-permute-done((bf16[256,256]{1,0:T(8,128)(2,1)S(1)}, bf16[256,256]{1,0:T(8,128)(2,1)S(1)}, u32[]{:S(2)}, u32[]{:S(2)}) %collective-permute-start.39) | collective-permute-done | bytes 131104 | tf_op jit(solution)/shard_map/ppermute | solution.py:196
  260.5 2.1 collective-permute-start.50
  262.7 1.2 collective-permute-start.42
  264.0 3.0 %collective-permute-start.41 = (bf16[128,256]{1,0:T(8,128)(2,1)S(1)}, bf16[128,256]{1,0:T(8,128)(2,1)S(1)}, u32[]{:S(2)}, u32[]{:S(2)}) collective-permute-start(bf16[128,256]{1,0:T(8,128)(2,1)S(1)} %get-tuple-element.99), channel_id=1, source_target_pairs={{0,16},{2,18},{4,20},{6,22},{8,24},{10,26},{12,28},{14,30},{16,0},... | collective-permute-start | bytes 196616 | tf_op jit(solution)/shard_map/ppermute | solution.py:199
  267.0 2.3 collective-permute-done.50
  269.6 4.8 %collective-permute-start.32 = (bf16[128,512]{1,0:T(8,128)(2,1)S(1)}, bf16[128,512]{1,0:T(8,128)(2,1)S(1)}, u32[]{:S(2)}, u32[]{:S(2)}) collective-permute-start(bf16[128,512]{1,0:T(8,128)(2,1)S(1)} %get-tuple-element.84), channel_id=1, source_target_pairs={{0,16},{2,18},{4,20},{6,22},{8,24},{10,26},{12,28},{14,30},{16,0},... | collective-permute-start | bytes 393224 | tf_op jit(solution)/shard_map/ppermute | solution.py:199
  275.5 6.7 %collective-permute-done.33 = bf16[128,512]{1,0:T(8,128)(2,1)S(1)} collective-permute-done((bf16[128,512]{1,0:T(8,128)(2,1)S(1)}, bf16[128,512]{1,0:T(8,128)(2,1)S(1)}, u32[]{:S(2)}, u32[]{:S(2)}) %collective-permute-start.33) | collective-permute-done | bytes 131104 | tf_op jit(solution)/shard_map/ppermute | solution.py:199
  (128 shorter events, 37.5 us)
Async XLA Ops:
  0.6 10.8 %copy-start.11 = (f32[128]{0:T(128)S(1)}, f32[128]{0:T(128)}, u32[]{:S(2)}) copy-start(f32[128]{0:T(128)} %param.8) | copy-start | bytes 1540
  3.0 22.9 %collective-permute-start = (bf16[136,1024]{1,0:T(8,128)(2,1)S(1)}, bf16[136,1024]{1,0:T(8,128)(2,1)S(1)}, u32[]{:S(2)}, u32[]{:S(2)}) collective-permute-start(bf16[136,1024]{1,0:T(8,128)(2,1)S(1)} %pad_maximum_fusion.6), channel_id=1, source_target_pairs={{8,0},{10,2},{12,4},{14,6},{16,8},{18,10},{20,12},{22,14},{24,16},... | collective-permute-start | bytes 835592 | tf_op jit(solution)/shard_map/ppermute | solution.py:212
  5.4 33.0 %collective-permute-start.1 = (bf16[136,1024]{1,0:T(8,128)(2,1)S(1)}, bf16[136,1024]{1,0:T(8,128)(2,1)S(1)}, u32[]{:S(2)}, u32[]{:S(2)}) collective-permute-start(bf16[136,1024]{1,0:T(8,128)(2,1)S(1)} %pad_maximum_fusion.6), channel_id=1, source_target_pairs={{0,8},{2,10},{4,12},{6,14},{8,16},{10,18},{12,20},{14,22},{16,24},... | collective-permute-start | bytes 835592 | tf_op jit(solution)/shard_map/ppermute | solution.py:212
  11.0 71.1 %collective-permute-start.10 = (bf16[4,128,512]{2,1,0:T(8,128)(2,1)}, bf16[4,128,512]{2,1,0:T(8,128)(2,1)S(1)}, u32[]{:S(2)}, u32[]{:S(2)}) collective-permute-start(bf16[4,128,512]{2,1,0:T(8,128)(2,1)} %fusion.17), channel_id=1, source_target_pairs={{0,16},{2,18},{4,20},{6,22},{8,24},{10,26},{12,28},{14,30},{16,0},... | collective-permute-start | bytes 1572872 | tf_op jit(solution)/shard_map/ppermute | solution.py:199
  20.1 83.7 %collective-permute-start.11 = (bf16[4,128,512]{2,1,0:T(8,128)(2,1)}, bf16[4,128,512]{2,1,0:T(8,128)(2,1)}, u32[]{:S(2)}, u32[]{:S(2)}) collective-permute-start(bf16[4,128,512]{2,1,0:T(8,128)(2,1)} %fusion.13), channel_id=1, source_target_pairs={{0,24},{2,26},{4,28},{6,30},{8,16},{10,18},{12,20},{14,22},{16,8},... | collective-permute-start | bytes 1572872 | tf_op jit(solution)/shard_map/ppermute | solution.py:199
  21.6 44.7 %copy-start.6 = (bf16[128,1024]{1,0:T(8,128)(2,1)S(1)}, bf16[128,1024]{1,0:T(8,128)(2,1)}, u32[]{:S(2)}) copy-start(bf16[128,1024]{1,0:T(8,128)(2,1)} %param.7) | copy-start | bytes 786436
  25.9 38.3 %collective-permute-start.2 = (bf16[136,1024]{1,0:T(8,128)(2,1)S(1)}, bf16[136,1024]{1,0:T(8,128)(2,1)S(1)}, u32[]{:S(2)}, u32[]{:S(2)}) collective-permute-start(bf16[136,1024]{1,0:T(8,128)(2,1)S(1)} %collective-permute-done), channel_id=1, source_target_pairs={{8,0},{10,2},{12,4},{14,6},{16,8},{18,10},{20,12},{22,14},{9,1},{1... | collective-permute-start | bytes 835592 | tf_op jit(solution)/shard_map/ppermute | solution.py:212
  38.4 27.2 %collective-permute-start.3 = (bf16[136,1024]{1,0:T(8,128)(2,1)S(1)}, bf16[136,1024]{1,0:T(8,128)(2,1)S(1)}, u32[]{:S(2)}, u32[]{:S(2)}) collective-permute-start(bf16[136,1024]{1,0:T(8,128)(2,1)S(1)} %collective-permute-done.1), channel_id=1, source_target_pairs={{8,16},{10,18},{12,20},{14,22},{16,24},{18,26},{20,28},{22,30},{9,... | collective-permute-start | bytes 835592 | tf_op jit(solution)/shard_map/ppermute | solution.py:212
  64.3 6.6 %collective-permute-start.4 = (bf16[136,1024]{1,0:T(8,128)(2,1)S(1)}, bf16[136,1024]{1,0:T(8,128)(2,1)S(1)}, u32[]{:S(2)}, u32[]{:S(2)}) collective-permute-start(bf16[136,1024]{1,0:T(8,128)(2,1)S(1)} %collective-permute-done.2), channel_id=1, source_target_pairs={{8,0},{10,2},{12,4},{14,6},{9,1},{11,3},{13,5},{15,7}} | collective-permute-start | bytes 835592 | tf_op jit(solution)/shard_map/ppermute | solution.py:212
  65.6 5.3 %collective-permute-start.5 = (bf16[136,1024]{1,0:T(8,128)(2,1)S(1)}, bf16[136,1024]{1,0:T(8,128)(2,1)S(1)}, u32[]{:S(2)}, u32[]{:S(2)}) collective-permute-start(bf16[136,1024]{1,0:T(8,128)(2,1)S(1)} %collective-permute-done.3), channel_id=1, source_target_pairs={{16,24},{18,26},{20,28},{22,30},{17,25},{19,27},{21,29},{23,31}} | collective-permute-start | bytes 835592 | tf_op jit(solution)/shard_map/ppermute | solution.py:212
  73.4 16.0 %collective-permute-start.8 = (bf16[256,1024]{1,0:T(8,128)(2,1)}, bf16[256,1024]{1,0:T(8,128)(2,1)}, u32[]{:S(2)}, u32[]{:S(2)}) collective-permute-start(bf16[256,1024]{1,0:T(8,128)(2,1)} %bitcast.16), channel_id=1, source_target_pairs={{0,6},{2,4},{4,2},{6,0},{8,14},{10,12},{12,10},{14,8},{16,22},{18,... | collective-permute-start | bytes 1572872 | tf_op jit(solution)/shard_map/ppermute | solution.py:196
  74.8 23.3 %collective-permute-start.7 = (bf16[256,1024]{1,0:T(8,128)(2,1)}, bf16[256,1024]{1,0:T(8,128)(2,1)}, u32[]{:S(2)}, u32[]{:S(2)}) collective-permute-start(bf16[256,1024]{1,0:T(8,128)(2,1)} %bitcast.15), channel_id=1, source_target_pairs={{0,4},{2,6},{4,0},{6,2},{8,12},{10,14},{12,8},{14,10},{16,20},{18,... | collective-permute-start | bytes 1572872 | tf_op jit(solution)/shard_map/ppermute | solution.py:196
  76.3 23.6 %collective-permute-start.6 = (bf16[256,1024]{1,0:T(8,128)(2,1)}, bf16[256,1024]{1,0:T(8,128)(2,1)}, u32[]{:S(2)}, u32[]{:S(2)}) collective-permute-start(bf16[256,1024]{1,0:T(8,128)(2,1)} %bitcast.14), channel_id=1, source_target_pairs={{0,2},{2,0},{4,6},{6,4},{8,10},{10,8},{12,14},{14,12},{16,18},{18,... | collective-permute-start | bytes 1572872 | tf_op jit(solution)/shard_map/ppermute | solution.py:196
  82.1 23.1 %collective-permute-start.12 = (bf16[4,128,512]{2,1,0:T(8,128)(2,1)}, bf16[4,128,512]{2,1,0:T(8,128)(2,1)S(1)}, u32[]{:S(2)}, u32[]{:S(2)}) collective-permute-start(bf16[4,128,512]{2,1,0:T(8,128)(2,1)} %fusion.12), channel_id=1, source_target_pairs={{0,8},{2,10},{4,12},{6,14},{8,0},{10,2},{12,4},{14,6},{16,24},{18,... | collective-permute-start | bytes 1572872 | tf_op jit(solution)/shard_map/ppermute | solution.py:199
  84.7 17.5 %copy-start.4 = (bf16[4,4,128,512]{3,2,0,1:T(8,128)(2,1)}, bf16[4,4,128,512]{3,2,0,1:T(8,128)(2,1)S(1)}, u32[]{:S(2)}) copy-start(bf16[4,4,128,512]{3,2,0,1:T(8,128)(2,1)S(1)} %bitcast_dynamic-update-slice_fusion.4) | copy-start | bytes 6291460
  89.4 21.7 %collective-permute-start.16 = (bf16[4,128,512]{2,1,0:T(8,128)(2,1)}, bf16[4,128,512]{2,1,0:T(8,128)(2,1)S(1)}, u32[]{:S(2)}, u32[]{:S(2)}) collective-permute-start(bf16[4,128,512]{2,1,0:T(8,128)(2,1)} %fusion.16), channel_id=1, source_target_pairs={{0,2},{2,0},{4,6},{6,4},{8,10},{10,8},{12,14},{14,12},{16,18},{18,... | collective-permute-start | bytes 1572872 | tf_op jit(solution)/shard_map/ppermute | solution.py:196
  98.1 25.3 %collective-permute-start.17 = (bf16[4,128,512]{2,1,0:T(8,128)(2,1)}, bf16[4,128,512]{2,1,0:T(8,128)(2,1)S(1)}, u32[]{:S(2)}, u32[]{:S(2)}) collective-permute-start(bf16[4,128,512]{2,1,0:T(8,128)(2,1)} %fusion.15), channel_id=1, source_target_pairs={{0,4},{2,6},{4,0},{6,2},{8,12},{10,14},{12,8},{14,10},{16,20},{18,... | collective-permute-start | bytes 1572872 | tf_op jit(solution)/shard_map/ppermute | solution.py:196
  99.9 25.2 %collective-permute-start.18 = (bf16[4,128,512]{2,1,0:T(8,128)(2,1)}, bf16[4,128,512]{2,1,0:T(8,128)(2,1)S(1)}, u32[]{:S(2)}, u32[]{:S(2)}) collective-permute-start(bf16[4,128,512]{2,1,0:T(8,128)(2,1)} %fusion.14), channel_id=1, source_target_pairs={{0,6},{2,4},{4,2},{6,0},{8,14},{10,12},{12,10},{14,8},{16,22},{18,... | collective-permute-start | bytes 1572872 | tf_op jit(solution)/shard_map/ppermute | solution.py:196
  102.1 2.1 copy-start.5
  103.8 75.0 %collective-permute-start.9 = (bf16[1024,1024]{1,0:T(8,128)(2,1)S(1)}, bf16[1024,1024]{1,0:T(8,128)(2,1)}, u32[]{:S(2)}, u32[]{:S(2)}) collective-permute-start(bf16[1024,1024]{1,0:T(8,128)(2,1)S(1)} %pad_maximum_fusion.refs_1_), channel_id=1, source_target_pairs={{0,1},{1,0},{2,3},{3,2},{4,5},{5,4},{6,7},{7,6},{8,9},{9,8},{10,11... | collective-permute-start | bytes 6291464 | tf_op jit(solution)/shard_map/ppermute | solution.py:54
  105.3 28.3 %collective-permute-start.23 = (bf16[4,64,1024]{2,1,0:T(8,128)(2,1)}, bf16[4,64,1024]{2,1,0:T(8,128)(2,1)S(1)}, u32[]{:S(2)}, u32[]{:S(2)}) collective-permute-start(bf16[4,64,1024]{2,1,0:T(8,128)(2,1)} %fusion.22), channel_id=1, source_target_pairs={{0,2},{2,0},{4,6},{6,4},{8,10},{10,8},{12,14},{14,12},{16,18},{18,... | collective-permute-start | bytes 1572872 | tf_op jit(solution)/shard_map/ppermute | solution.py:196
  111.0 33.8 %collective-permute-start.13 = (bf16[4,128,512]{2,1,0:T(8,128)(2,1)S(1)}, bf16[4,128,512]{2,1,0:T(8,128)(2,1)S(1)}, u32[]{:S(2)}, u32[]{:S(2)}) collective-permute-start(bf16[4,128,512]{2,1,0:T(8,128)(2,1)S(1)} %get-tuple-element.70), channel_id=1, source_target_pairs={{0,2},{2,0},{4,6},{6,4},{8,10},{10,8},{12,14},{14,12},{16,18},{18,... | collective-permute-start | bytes 1572872 | tf_op jit(solution)/shard_map/ppermute | solution.py:196
  123.4 25.4 %collective-permute-start.14 = (bf16[4,128,512]{2,1,0:T(8,128)(2,1)S(1)}, bf16[4,128,512]{2,1,0:T(8,128)(2,1)S(1)}, u32[]{:S(2)}, u32[]{:S(2)}) collective-permute-start(bf16[4,128,512]{2,1,0:T(8,128)(2,1)S(1)} %get-tuple-element.69), channel_id=1, source_target_pairs={{0,4},{2,6},{4,0},{6,2},{8,12},{10,14},{12,8},{14,10},{16,20},{18,... | collective-permute-start | bytes 1572872 | tf_op jit(solution)/shard_map/ppermute | solution.py:196
  125.1 29.6 %collective-permute-start.15 = (bf16[4,128,512]{2,1,0:T(8,128)(2,1)}, bf16[4,128,512]{2,1,0:T(8,128)(2,1)}, u32[]{:S(2)}, u32[]{:S(2)}) collective-permute-start(bf16[4,128,512]{2,1,0:T(8,128)(2,1)} %get-tuple-element.68), channel_id=1, source_target_pairs={{0,6},{2,4},{4,2},{6,0},{8,14},{10,12},{12,10},{14,8},{16,22},{18,... | collective-permute-start | bytes 1572872 | tf_op jit(solution)/shard_map/ppermute | solution.py:196
  133.6 15.2 %copy-start.9 = (bf16[4,64,1024]{2,1,0:T(8,128)(2,1)}, bf16[4,64,1024]{2,1,0:T(8,128)(2,1)S(1)}, u32[]{:S(2)}) copy-start(bf16[4,64,1024]{2,1,0:T(8,128)(2,1)S(1)} %collective-permute-done.23) | copy-start | bytes 1572868
  133.6 33.7 %collective-permute-start.19 = (bf16[4,128,512]{2,1,0:T(8,128)(2,1)}, bf16[4,128,512]{2,1,0:T(8,128)(2,1)}, u32[]{:S(2)}, u32[]{:S(2)}) collective-permute-start(bf16[4,128,512]{2,1,0:T(8,128)(2,1)} %get-tuple-element.66), channel_id=1, source_target_pairs={{0,16},{2,18},{4,20},{6,22},{8,24},{10,26},{12,28},{14,30},{16,0},... | collective-permute-start | bytes 1572872 | tf_op jit(solution)/shard_map/ppermute | solution.py:199
  145.6 33.2 %collective-permute-start.20 = (bf16[4,128,512]{2,1,0:T(8,128)(2,1)}, bf16[4,128,512]{2,1,0:T(8,128)(2,1)}, u32[]{:S(2)}, u32[]{:S(2)}) collective-permute-start(bf16[4,128,512]{2,1,0:T(8,128)(2,1)} %get-tuple-element.65), channel_id=1, source_target_pairs={{0,24},{2,26},{4,28},{6,30},{8,16},{10,18},{12,20},{14,22},{16,8},... | collective-permute-start | bytes 1572872 | tf_op jit(solution)/shard_map/ppermute | solution.py:199
  148.7 0.8 copy-start.2
  149.5 29.3 %collective-permute-start.21 = (bf16[4,128,512]{2,1,0:T(8,128)(2,1)}, bf16[4,128,512]{2,1,0:T(8,128)(2,1)}, u32[]{:S(2)}, u32[]{:S(2)}) collective-permute-start(bf16[4,128,512]{2,1,0:T(8,128)(2,1)} %get-tuple-element.64), channel_id=1, source_target_pairs={{0,8},{2,10},{4,12},{6,14},{8,0},{10,2},{12,4},{14,6},{16,24},{18,... | collective-permute-start | bytes 1572872 | tf_op jit(solution)/shard_map/ppermute | solution.py:199
  152.9 1.8 copy-start.7
  152.9 3.4 %copy-start.10 = (bf16[4,64,1024]{2,1,0:T(8,128)(2,1)S(1)}, bf16[4,64,1024]{2,1,0:T(8,128)(2,1)}, u32[]{:S(2)}) copy-start(bf16[4,64,1024]{2,1,0:T(8,128)(2,1)} %copy-done.9) | copy-start | bytes 1572868
  153.0 14.2 %copy-start.8 = (bf16[4,64,1024]{2,1,0:T(8,128)(2,1)S(1)}, bf16[4,64,1024]{2,1,0:T(8,128)(2,1)}, u32[]{:S(2)}) copy-start(bf16[4,64,1024]{2,1,0:T(8,128)(2,1)} %fusion.24) | copy-start | bytes 1572868
  153.0 25.8 %copy-start.1 = (bf16[4,128,512]{2,1,0:T(8,128)(2,1)S(1)}, bf16[4,128,512]{2,1,0:T(8,128)(2,1)}, u32[]{:S(2)}) copy-start(bf16[4,128,512]{2,1,0:T(8,128)(2,1)} %copy-done) | copy-start | bytes 1572868
  153.0 25.8 %copy-start.3 = (bf16[4,128,512]{2,1,0:T(8,128)(2,1)S(1)}, bf16[4,128,512]{2,1,0:T(8,128)(2,1)}, u32[]{:S(2)}) copy-start(bf16[4,128,512]{2,1,0:T(8,128)(2,1)} %copy-done.2) | copy-start | bytes 1572868
  154.8 33.5 %collective-permute-start.24 = (bf16[4,64,1024]{2,1,0:T(8,128)(2,1)S(1)}, bf16[4,64,1024]{2,1,0:T(8,128)(2,1)S(1)}, u32[]{:S(2)}, u32[]{:S(2)}) collective-permute-start(bf16[4,64,1024]{2,1,0:T(8,128)(2,1)S(1)} %copy-done.7), channel_id=1, source_target_pairs={{0,4},{2,6},{4,0},{6,2},{8,12},{10,14},{12,8},{14,10},{16,20},{18,... | collective-permute-start | bytes 1572872 | tf_op jit(solution)/shard_map/ppermute | solution.py:196
  167.2 21.1 %collective-permute-start.25 = (bf16[4,64,1024]{2,1,0:T(8,128)(2,1)S(1)}, bf16[4,64,1024]{2,1,0:T(8,128)(2,1)S(1)}, u32[]{:S(2)}, u32[]{:S(2)}) collective-permute-start(bf16[4,64,1024]{2,1,0:T(8,128)(2,1)S(1)} %copy-done.8), channel_id=1, source_target_pairs={{0,6},{2,4},{4,2},{6,0},{8,14},{10,12},{12,10},{14,8},{16,22},{18,... | collective-permute-start | bytes 1572872 | tf_op jit(solution)/shard_map/ppermute | solution.py:196
  188.2 36.6 %collective-permute-start.22 = (bf16[1024,512]{1,0:T(8,128)(2,1)S(1)}, bf16[1024,512]{1,0:T(8,128)(2,1)S(1)}, u32[]{:S(2)}, u32[]{:S(2)}) collective-permute-start(bf16[1024,512]{1,0:T(8,128)(2,1)S(1)} %get-tuple-element.42.refs_1_), channel_id=1, source_target_pairs={{0,1},{1,0},{2,3},{3,2},{4,5},{5,4},{6,7},{7,6},{8,9},{9,8},{10,11... | collective-permute-start | bytes 3145736 | tf_op jit(solution)/shard_map/ppermute | solution.py:54
  188.6 19.7 %collective-permute-start.26 = (bf16[4,64,512]{2,1,0:T(8,128)(2,1)S(1)}, bf16[4,64,512]{2,1,0:T(8,128)(2,1)S(1)}, u32[]{:S(2)}, u32[]{:S(2)}) collective-permute-start(bf16[4,64,512]{2,1,0:T(8,128)(2,1)S(1)} %get-tuple-element.78), channel_id=1, source_target_pairs={{0,16},{2,18},{4,20},{6,22},{8,24},{10,26},{12,28},{14,30},{16,0},... | collective-permute-start | bytes 786440 | tf_op jit(solution)/shard_map/ppermute | solution.py:199
  190.8 32.9 %collective-permute-start.27 = (bf16[4,64,512]{2,1,0:T(8,128)(2,1)S(1)}, bf16[4,64,512]{2,1,0:T(8,128)(2,1)S(1)}, u32[]{:S(2)}, u32[]{:S(2)}) collective-permute-start(bf16[4,64,512]{2,1,0:T(8,128)(2,1)S(1)} %get-tuple-element.77), channel_id=1, source_target_pairs={{0,24},{2,26},{4,28},{6,30},{8,16},{10,18},{12,20},{14,22},{16,8},... | collective-permute-start | bytes 786440 | tf_op jit(solution)/shard_map/ppermute | solution.py:199
  191.8 33.1 %collective-permute-start.28 = (bf16[4,64,512]{2,1,0:T(8,128)(2,1)S(1)}, bf16[4,64,512]{2,1,0:T(8,128)(2,1)S(1)}, u32[]{:S(2)}, u32[]{:S(2)}) collective-permute-start(bf16[4,64,512]{2,1,0:T(8,128)(2,1)S(1)} %get-tuple-element.76), channel_id=1, source_target_pairs={{0,8},{2,10},{4,12},{6,14},{8,0},{10,2},{12,4},{14,6},{16,24},{18,... | collective-permute-start | bytes 786440 | tf_op jit(solution)/shard_map/ppermute | solution.py:199
  193.3 36.7 %collective-permute-start.44 = (bf16[4,64,256]{2,1,0:T(8,128)(2,1)S(1)}, bf16[4,64,256]{2,1,0:T(8,128)(2,1)S(1)}, u32[]{:S(2)}, u32[]{:S(2)}) collective-permute-start(bf16[4,64,256]{2,1,0:T(8,128)(2,1)S(1)} %get-tuple-element.91), channel_id=1, source_target_pairs={{0,16},{2,18},{4,20},{6,22},{8,24},{10,26},{12,28},{14,30},{16,0},... | collective-permute-start | bytes 393224 | tf_op jit(solution)/shard_map/ppermute | solution.py:199
  208.4 22.1 %collective-permute-start.35 = (bf16[4,64,256]{2,1,0:T(8,128)(2,1)S(1)}, bf16[4,64,256]{2,1,0:T(8,128)(2,1)S(1)}, u32[]{:S(2)}, u32[]{:S(2)}) collective-permute-start(bf16[4,64,256]{2,1,0:T(8,128)(2,1)S(1)} %get-tuple-element.87), channel_id=1, source_target_pairs={{0,16},{2,18},{4,20},{6,22},{8,24},{10,26},{12,28},{14,30},{16,0},... | collective-permute-start | bytes 393224 | tf_op jit(solution)/shard_map/ppermute | solution.py:199
  223.7 8.3 %collective-permute-start.36 = (bf16[4,64,256]{2,1,0:T(8,128)(2,1)S(1)}, bf16[4,64,256]{2,1,0:T(8,128)(2,1)S(1)}, u32[]{:S(2)}, u32[]{:S(2)}) collective-permute-start(bf16[4,64,256]{2,1,0:T(8,128)(2,1)S(1)} %get-tuple-element.86), channel_id=1, source_target_pairs={{0,24},{2,26},{4,28},{6,30},{8,16},{10,18},{12,20},{14,22},{16,8},... | collective-permute-start | bytes 393224 | tf_op jit(solution)/shard_map/ppermute | solution.py:199
  224.8 8.3 %collective-permute-start.37 = (bf16[4,64,256]{2,1,0:T(8,128)(2,1)S(1)}, bf16[4,64,256]{2,1,0:T(8,128)(2,1)S(1)}, u32[]{:S(2)}, u32[]{:S(2)}) collective-permute-start(bf16[4,64,256]{2,1,0:T(8,128)(2,1)S(1)} %get-tuple-element.85), channel_id=1, source_target_pairs={{0,8},{2,10},{4,12},{6,14},{8,0},{10,2},{12,4},{14,6},{16,24},{18,... | collective-permute-start | bytes 393224 | tf_op jit(solution)/shard_map/ppermute | solution.py:199
  227.4 17.1 %collective-permute-start.31 = (bf16[256,512]{1,0:T(8,128)(2,1)S(1)}, bf16[256,512]{1,0:T(8,128)(2,1)S(1)}, u32[]{:S(2)}, u32[]{:S(2)}) collective-permute-start(bf16[256,512]{1,0:T(8,128)(2,1)S(1)} %get-tuple-element.46), channel_id=1, source_target_pairs={{0,6},{2,4},{4,2},{6,0},{8,14},{10,12},{12,10},{14,8},{16,22},{18,... | collective-permute-start | bytes 786440 | tf_op jit(solution)/shard_map/ppermute | solution.py:196
  230.0 16.5 %collective-permute-start.30 = (bf16[256,512]{1,0:T(8,128)(2,1)S(1)}, bf16[256,512]{1,0:T(8,128)(2,1)S(1)}, u32[]{:S(2)}, u32[]{:S(2)}) collective-permute-start(bf16[256,512]{1,0:T(8,128)(2,1)S(1)} %get-tuple-element.45), channel_id=1, source_target_pairs={{0,4},{2,6},{4,0},{6,2},{8,12},{10,14},{12,8},{14,10},{16,20},{18,... | collective-permute-start | bytes 786440 | tf_op jit(solution)/shard_map/ppermute | solution.py:196
  230.5 16.5 %collective-permute-start.29 = (bf16[256,512]{1,0:T(8,128)(2,1)S(1)}, bf16[256,512]{1,0:T(8,128)(2,1)S(1)}, u32[]{:S(2)}, u32[]{:S(2)}) collective-permute-start(bf16[256,512]{1,0:T(8,128)(2,1)S(1)} %get-tuple-element.44), channel_id=1, source_target_pairs={{0,2},{2,0},{4,6},{6,4},{8,10},{10,8},{12,14},{14,12},{16,18},{18,... | collective-permute-start | bytes 786440 | tf_op jit(solution)/shard_map/ppermute | solution.py:196
  232.0 7.9 %collective-permute-start.45 = (bf16[4,64,256]{2,1,0:T(8,128)(2,1)S(1)}, bf16[4,64,256]{2,1,0:T(8,128)(2,1)S(1)}, u32[]{:S(2)}, u32[]{:S(2)}) collective-permute-start(bf16[4,64,256]{2,1,0:T(8,128)(2,1)S(1)} %get-tuple-element.90), channel_id=1, source_target_pairs={{0,24},{2,26},{4,28},{6,30},{8,16},{10,18},{12,20},{14,22},{16,8},... | collective-permute-start | bytes 393224 | tf_op jit(solution)/shard_map/ppermute | solution.py:199
  233.2 7.0 %collective-permute-start.46 = (bf16[4,64,256]{2,1,0:T(8,128)(2,1)S(1)}, bf16[4,64,256]{2,1,0:T(8,128)(2,1)S(1)}, u32[]{:S(2)}, u32[]{:S(2)}) collective-permute-start(bf16[4,64,256]{2,1,0:T(8,128)(2,1)S(1)} %get-tuple-element.89), channel_id=1, source_target_pairs={{0,8},{2,10},{4,12},{6,14},{8,0},{10,2},{12,4},{14,6},{16,24},{18,... | collective-permute-start | bytes 393224 | tf_op jit(solution)/shard_map/ppermute | solution.py:199
  242.0 15.4 %collective-permute-start.49 = (bf16[256,256]{1,0:T(8,128)(2,1)S(1)}, bf16[256,256]{1,0:T(8,128)(2,1)S(1)}, u32[]{:S(2)}, u32[]{:S(2)}) collective-permute-start(bf16[256,256]{1,0:T(8,128)(2,1)S(1)} %get-tuple-element.58), channel_id=1, source_target_pairs={{0,6},{2,4},{4,2},{6,0},{8,14},{10,12},{12,10},{14,8},{16,22},{18,... | collective-permute-start | bytes 393224 | tf_op jit(solution)/shard_map/ppermute | solution.py:196
  244.0 13.4 %collective-permute-start.48 = (bf16[256,256]{1,0:T(8,128)(2,1)S(1)}, bf16[256,256]{1,0:T(8,128)(2,1)S(1)}, u32[]{:S(2)}, u32[]{:S(2)}) collective-permute-start(bf16[256,256]{1,0:T(8,128)(2,1)S(1)} %get-tuple-element.57), channel_id=1, source_target_pairs={{0,4},{2,6},{4,0},{6,2},{8,12},{10,14},{12,8},{14,10},{16,20},{18,... | collective-permute-start | bytes 393224 | tf_op jit(solution)/shard_map/ppermute | solution.py:196
  244.5 7.6 %collective-permute-start.40 = (bf16[256,256]{1,0:T(8,128)(2,1)S(1)}, bf16[256,256]{1,0:T(8,128)(2,1)S(1)}, u32[]{:S(2)}, u32[]{:S(2)}) collective-permute-start(bf16[256,256]{1,0:T(8,128)(2,1)S(1)} %get-tuple-element.52), channel_id=1, source_target_pairs={{0,6},{2,4},{4,2},{6,0},{8,14},{10,12},{12,10},{14,8},{16,22},{18,... | collective-permute-start | bytes 393224 | tf_op jit(solution)/shard_map/ppermute | solution.py:196
  246.5 10.1 %collective-permute-start.39 = (bf16[256,256]{1,0:T(8,128)(2,1)S(1)}, bf16[256,256]{1,0:T(8,128)(2,1)S(1)}, u32[]{:S(2)}, u32[]{:S(2)}) collective-permute-start(bf16[256,256]{1,0:T(8,128)(2,1)S(1)} %get-tuple-element.51), channel_id=1, source_target_pairs={{0,4},{2,6},{4,0},{6,2},{8,12},{10,14},{12,8},{14,10},{16,20},{18,... | collective-permute-start | bytes 393224 | tf_op jit(solution)/shard_map/ppermute | solution.py:196
  247.0 9.6 %collective-permute-start.38 = (bf16[256,256]{1,0:T(8,128)(2,1)S(1)}, bf16[256,256]{1,0:T(8,128)(2,1)S(1)}, u32[]{:S(2)}, u32[]{:S(2)}) collective-permute-start(bf16[256,256]{1,0:T(8,128)(2,1)S(1)} %get-tuple-element.50), channel_id=1, source_target_pairs={{0,2},{2,0},{4,6},{6,4},{8,10},{10,8},{12,14},{14,12},{16,18},{18,... | collective-permute-start | bytes 393224 | tf_op jit(solution)/shard_map/ppermute | solution.py:196
  252.1 5.2 %collective-permute-start.47 = (bf16[256,256]{1,0:T(8,128)(2,1)S(1)}, bf16[256,256]{1,0:T(8,128)(2,1)S(1)}, u32[]{:S(2)}, u32[]{:S(2)}) collective-permute-start(bf16[256,256]{1,0:T(8,128)(2,1)S(1)} %get-tuple-element.56), channel_id=1, source_target_pairs={{0,2},{2,0},{4,6},{6,4},{8,10},{10,8},{12,14},{14,12},{16,18},{18,... | collective-permute-start | bytes 393224 | tf_op jit(solution)/shard_map/ppermute | solution.py:196
  258.2 5.8 %collective-permute-start.52 = (bf16[128,256]{1,0:T(8,128)(2,1)S(1)}, bf16[128,256]{1,0:T(8,128)(2,1)S(1)}, u32[]{:S(2)}, u32[]{:S(2)}) collective-permute-start(bf16[128,256]{1,0:T(8,128)(2,1)S(1)} %get-tuple-element.95), channel_id=1, source_target_pairs={{0,8},{2,10},{4,12},{6,14},{8,0},{10,2},{12,4},{14,6},{16,24},{18,... | collective-permute-start | bytes 196616 | tf_op jit(solution)/shard_map/ppermute | solution.py:199
  259.2 7.8 %collective-permute-start.51 = (bf16[128,256]{1,0:T(8,128)(2,1)S(1)}, bf16[128,256]{1,0:T(8,128)(2,1)S(1)}, u32[]{:S(2)}, u32[]{:S(2)}) collective-permute-start(bf16[128,256]{1,0:T(8,128)(2,1)S(1)} %get-tuple-element.96), channel_id=1, source_target_pairs={{0,24},{2,26},{4,28},{6,30},{8,16},{10,18},{12,20},{14,22},{16,8},... | collective-permute-start | bytes 196616 | tf_op jit(solution)/shard_map/ppermute | solution.py:199
  260.5 8.8 %collective-permute-start.50 = (bf16[128,256]{1,0:T(8,128)(2,1)S(1)}, bf16[128,256]{1,0:T(8,128)(2,1)S(1)}, u32[]{:S(2)}, u32[]{:S(2)}) collective-permute-start(bf16[128,256]{1,0:T(8,128)(2,1)S(1)} %get-tuple-element.94), channel_id=1, source_target_pairs={{0,16},{2,18},{4,20},{6,22},{8,24},{10,26},{12,28},{14,30},{16,0},... | collective-permute-start | bytes 196616 | tf_op jit(solution)/shard_map/ppermute | solution.py:199
  262.6 7.0 %collective-permute-start.43 = (bf16[128,256]{1,0:T(8,128)(2,1)S(1)}, bf16[128,256]{1,0:T(8,128)(2,1)S(1)}, u32[]{:S(2)}, u32[]{:S(2)}) collective-permute-start(bf16[128,256]{1,0:T(8,128)(2,1)S(1)} %get-tuple-element.98), channel_id=1, source_target_pairs={{0,8},{2,10},{4,12},{6,14},{8,0},{10,2},{12,4},{14,6},{16,24},{18,... | collective-permute-start | bytes 196616 | tf_op jit(solution)/shard_map/ppermute | solution.py:199
  262.7 11.7 %collective-permute-start.42 = (bf16[128,256]{1,0:T(8,128)(2,1)S(1)}, bf16[128,256]{1,0:T(8,128)(2,1)S(1)}, u32[]{:S(2)}, u32[]{:S(2)}) collective-permute-start(bf16[128,256]{1,0:T(8,128)(2,1)S(1)} %get-tuple-element.97), channel_id=1, source_target_pairs={{0,24},{2,26},{4,28},{6,30},{8,16},{10,18},{12,20},{14,22},{16,8},... | collective-permute-start | bytes 196616 | tf_op jit(solution)/shard_map/ppermute | solution.py:199
  264.0 11.4 %collective-permute-start.41 = (bf16[128,256]{1,0:T(8,128)(2,1)S(1)}, bf16[128,256]{1,0:T(8,128)(2,1)S(1)}, u32[]{:S(2)}, u32[]{:S(2)}) collective-permute-start(bf16[128,256]{1,0:T(8,128)(2,1)S(1)} %get-tuple-element.99), channel_id=1, source_target_pairs={{0,16},{2,18},{4,20},{6,22},{8,24},{10,26},{12,28},{14,30},{16,0},... | collective-permute-start | bytes 196616 | tf_op jit(solution)/shard_map/ppermute | solution.py:199
  267.0 8.4 %collective-permute-start.34 = (bf16[128,512]{1,0:T(8,128)(2,1)S(1)}, bf16[128,512]{1,0:T(8,128)(2,1)S(1)}, u32[]{:S(2)}, u32[]{:S(2)}) collective-permute-start(bf16[128,512]{1,0:T(8,128)(2,1)S(1)} %get-tuple-element.83), channel_id=1, source_target_pairs={{0,8},{2,10},{4,12},{6,14},{8,0},{10,2},{12,4},{14,6},{16,24},{18,... | collective-permute-start | bytes 393224 | tf_op jit(solution)/shard_map/ppermute | solution.py:199
  269.3 12.8 %collective-permute-start.33 = (bf16[128,512]{1,0:T(8,128)(2,1)S(1)}, bf16[128,512]{1,0:T(8,128)(2,1)S(1)}, u32[]{:S(2)}, u32[]{:S(2)}) collective-permute-start(bf16[128,512]{1,0:T(8,128)(2,1)S(1)} %get-tuple-element.82), channel_id=1, source_target_pairs={{0,24},{2,26},{4,28},{6,30},{8,16},{10,18},{12,20},{14,22},{16,8},... | collective-permute-start | bytes 393224 | tf_op jit(solution)/shard_map/ppermute | solution.py:199
  269.6 13.7 %collective-permute-start.32 = (bf16[128,512]{1,0:T(8,128)(2,1)S(1)}, bf16[128,512]{1,0:T(8,128)(2,1)S(1)}, u32[]{:S(2)}, u32[]{:S(2)}) collective-permute-start(bf16[128,512]{1,0:T(8,128)(2,1)S(1)} %get-tuple-element.84), channel_id=1, source_target_pairs={{0,16},{2,18},{4,20},{6,22},{8,24},{10,26},{12,28},{14,30},{16,0},... | collective-permute-start | bytes 393224 | tf_op jit(solution)/shard_map/ppermute | solution.py:199
  (1 other events, 0.8 us)
